TPU v7x, 256 devices: a 4x2x16 block of a 4x16x16 slice. The times are simulated.
256 devices in a mesh: grp: 2 (over y), ep: 32 (over z, core), tp: 4 (over x).
Axes of the slice: x: 4, y: 2, z: 16, core: 2. Of those that a mesh axis runs over, the one named last changes fastest.
The devices are a block of a 4x16x16 slice.
Arguments:
- conv_input: bfloat16 [40960, 2048], P(('grp', 'ep')), parts along dimension 0, may hold values from -6 to 6
- conv_taps: float32 [31, 2048], replicated, may hold values from -1 to 1
- conv_gain: float32 [2048], replicated, may hold values from 0.1 to 1.9
- conv_weight: bfloat16 [2048, 2048], P(None, 'tp'), may hold values from -0.125 to 0.125
- moe_input: bfloat16 [40960, 2048], P(('grp', 'ep')), parts along dimension 0, may hold values from -6 to 6
- moe_gain: float32 [2048], replicated, may hold values from 0.1 to 1.9
- expert_ids: int32 [40960, 2], P(('grp', 'ep')), parts along dimension 0, may hold values from 0 to 31, as said below
- route_weights: float32 [40960, 2], P(('grp', 'ep')), parts along dimension 0, may hold values from 0.1 to 1
- gate_weight: bfloat16 [32, 2048, 1024], P('ep', None, 'tp'), may hold values from -0.125 to 0.125
- up_weight: bfloat16 [32, 2048, 1024], P('ep', None, 'tp'), may hold values from -0.125 to 0.125
- down_weight: bfloat16 [32, 1024, 2048], P('ep', 'tp'), may hold values from -0.1875 to 0.1875
- post_gain: float32 [2048], replicated, may hold values from 0.1 to 1.9
Outputs:
- conv_out: bfloat16 [40960, 2048], P(('grp', 'ep'), 'tp'), parts along dimension 0
- moe_out: bfloat16 [40960, 2048], P(('grp', 'ep', 'tp')), parts along dimension 0
There are 2 independent parts, one for each index of `grp`. A program takes and returns all parts, laid end to end along the dimension named above; an argument that names none is the same for every part. Nothing has to cross between parts.
Inputs may be any that keep to these rules, and one draw needn't show every extreme that they name: `expert_ids`: in each aligned block of 160 tokens, every expert is named exactly 10 times; a token's two experts differ and lie in one group of 4 consecutive experts.
All inputs are finite; a program needn't handle non-finite values.
Results may differ from a plain program's by a relative error of at most 0.012.
Values may be sent and summed in bfloat16 or wider, within the bound.
No kernel may reach another device: no remote copies, remote signals or barrier semaphores. Data moves between devices by JAX's collectives and lax.ppermute only.
A program may use at most 128 MiB of HBM per device.

v0:
```python
import jax
import jax.numpy as jnp
from jax import lax
from jax.sharding import Mesh
from jax.sharding import PartitionSpec as P

EP = ("ep_0", "ep_1")
GRP_EP = ("grp", "ep_0", "ep_1")
GRP_EP_TP = ("grp", "ep_0", "ep_1", "tp")


EPSILON = 1e-06


def shifted(shard, axis, by):
    size = lax.axis_size(axis)
    pairs = [(i, i + by) for i in range(size) if 0 <= i + by < size]
    return lax.ppermute(shard, axis, pairs)


def gather_turned(arrays, axis, dims):
    turned = [jnp.moveaxis(a, dim, 0) for a, dim in zip(arrays, dims)]
    both = jnp.concatenate([t.reshape(len(t), -1) for t in turned], axis=1)
    out, at, outs = (lax.all_gather(both, axis, axis=0, tiled=True), 0, [])
    for t, dim in zip(turned, dims):
        slab = out[:, at : at + t[0].size].reshape(-1, *t.shape[1:])
        outs.append(jnp.moveaxis(slab, 0, dim))
        at += t[0].size
    return tuple(outs)


def in_blocks(shard, dim, size):
    dims = shard.shape
    pieces = shard.reshape(*dims[:dim], size, dims[dim] // size, *dims[dim + 1 :])
    return jnp.moveaxis(pieces, dim, 0)


def in_order(pieces, dim):
    pieces = jnp.moveaxis(pieces, 0, dim)
    dims = pieces.shape
    return pieces.reshape(*dims[:dim], dims[dim] * dims[dim + 1], *dims[dim + 2 :])


def moved_by_axis(pieces, axes, sequence):
    inside = pieces.shape[1:]
    out = pieces.reshape(*(lax.axis_size(a) for a in axes), *inside)
    for k in sequence:
        out = lax.all_to_all(out, axes[k], k, k, tiled=True)
    return out.reshape(-1, *inside)


def core_and_chips(shard, groups, sequence, split_dim, concat_dim):
    size = lax.axis_size(groups[0]) * lax.axis_size(groups[1])
    pieces = in_blocks(shard, split_dim, size)
    return in_order(moved_by_axis(pieces, groups, sequence), concat_dim)


def channel_norm(values, scales):
    mean_square = jnp.mean(values * values, axis=-1, keepdims=True)
    return values * lax.rsqrt(mean_square + EPSILON) * scales


def body(
    conv_input,
    conv_taps,
    conv_gain,
    conv_weight,
    moe_input,
    moe_gain,
    expert_ids,
    route_weights,
    gate_weight,
    up_weight,
    down_weight,
    post_gain,
):
    row_count = conv_input.shape[0]
    reach = conv_taps.shape[0] - 1
    carried = shifted(conv_input[row_count - reach :], EP, 1)
    extended = jnp.concatenate([carried, conv_input], axis=0).astype(jnp.float32)
    conv_sum = extended[0:row_count] * conv_taps[0]
    for offset in range(1, reach + 1):
        conv_sum = conv_sum + extended[offset : offset + row_count] * conv_taps[offset]
    activated = jax.nn.silu(channel_norm(conv_sum, conv_gain)).astype(jnp.bfloat16)
    conv_out = jnp.dot(activated, conv_weight, preferred_element_type=jnp.float32).astype(
        jnp.bfloat16
    )
    model_width = moe_input.shape[1]
    quarters = lax.axis_size("tp")
    ep_count = lax.axis_size(EP)
    block_rows = moe_input.shape[0] // quarters
    local_experts = gate_weight.shape[0]
    experts_all = ep_count * local_experts
    capacity = 2 * block_rows // experts_all
    slot_rows = 2 * block_rows
    own_quarter = lax.axis_index("tp")
    entries = expert_ids.reshape(quarters, slot_rows)
    onehot = (
        entries[:, :, None] == jnp.arange(experts_all, dtype=jnp.int32)[None, None, :]
    ).astype(jnp.int32)
    position = jnp.sum((jnp.cumsum(onehot, axis=1) - 1) * onehot, axis=2)
    target = entries * capacity + position
    quarter_index = jnp.arange(quarters, dtype=jnp.int32)[:, None]
    entry_index = jnp.broadcast_to(
        jnp.arange(slot_rows, dtype=jnp.int32)[None, :], (quarters, slot_rows)
    )
    source_entry = (
        jnp.zeros((quarters, slot_rows), jnp.int32).at[quarter_index, target].set(entry_index)
    )
    own_input = lax.dynamic_slice_in_dim(moe_input, own_quarter * block_rows, block_rows, 0)
    normed = channel_norm(own_input.astype(jnp.float32), moe_gain).astype(jnp.bfloat16)
    own_source = lax.dynamic_index_in_dim(source_entry, own_quarter, 0, keepdims=False)
    arrived = lax.all_to_all(
        normed[own_source // 2].reshape(1, ep_count, local_experts * capacity, model_width),
        EP,
        split_axis=1,
        concat_axis=1,
        tiled=True,
    )
    gate_full, up_full, down_full = gather_turned(
        (gate_weight, up_weight, down_weight), "tp", (2, 2, 1)
    )
    count = arrived.shape[0]
    shaped = arrived.reshape(count, ep_count, local_experts, capacity, model_width)
    gate_value = jnp.einsum(
        "qsjcd,jdf->qsjcf", shaped, gate_full, preferred_element_type=jnp.float32
    )
    up_value = jnp.einsum("qsjcd,jdf->qsjcf", shaped, up_full, preferred_element_type=jnp.float32)
    hidden = (jax.nn.silu(gate_value) * up_value).astype(jnp.bfloat16)
    hidden_units = down_full.shape[1]
    part_units = hidden_units // quarters
    pieces = hidden.reshape(ep_count, local_experts, capacity, quarters, part_units)
    down_pieces = down_full.reshape(local_experts, quarters, part_units, model_width)
    partial_value = jnp.einsum(
        "sjctf,jtfd->sjctd", pieces, down_pieces, preferred_element_type=jnp.float32
    )
    summed = jnp.sum(partial_value.astype(jnp.bfloat16).astype(jnp.float32), axis=3).astype(
        jnp.bfloat16
    )
    summed = summed.reshape(slot_rows, model_width)
    returned = core_and_chips(
        summed.reshape(ep_count, local_experts * capacity, model_width),
        ("ep_0", "ep_1"),
        (1, 0),
        0,
        0,
    )
    flat_back = returned.reshape(slot_rows, model_width)
    own_target = lax.dynamic_index_in_dim(target, own_quarter, 0, keepdims=False)
    gathered = flat_back[own_target].reshape(block_rows, 2, model_width).astype(jnp.float32)
    weights = lax.dynamic_slice_in_dim(route_weights, own_quarter * block_rows, block_rows, 0)
    mixed_rows = jnp.sum(gathered * weights[:, :, None], axis=1)
    moe_out = channel_norm(mixed_rows, post_gain).astype(jnp.bfloat16)
    return (conv_out, moe_out)


def solution(mesh):
    split = Mesh(
        mesh.devices.reshape(mesh.shape["grp"], 16, 2, mesh.shape["tp"]),
        ("grp", "ep_0", "ep_1", "tp"),
    )
    return jax.shard_map(
        body,
        mesh=split,
        in_specs=(
            P(GRP_EP, None),
            P(),
            P(),
            P(None, "tp"),
            P(GRP_EP, None),
            P(),
            P(GRP_EP, None),
            P(GRP_EP, None),
            P(EP, None, "tp"),
            P(EP, None, "tp"),
            P(EP, "tp", None),
            P(),
        ),
        out_specs=(P(GRP_EP, "tp"), P(GRP_EP_TP, None)),
        check_vma=False,
    )
```

profile of v0, /device:TPU:33, one launch (start us, length us, event | category | flops | bytes accessed | tf_op | source)
XLA Modules:
  0.0 306.5 jit_solution(14852747243465150614)
XLA Ops:
  8.9 3.1 %pad_maximum_fusion = bf16[256,6144]{0,1:T(8,128)(2,1)} fusion(bf16[256,2048]{0,1:T(8,128)(2,1)S(1)} %bitcast.133, bf16[256,2048]{0,1:T(8,128)(2,1)} %bitcast.135, bf16[256,2048]{0,1:T(8,128)(2,1)} %bitcast.136), kind=kLoop, calls=%fused_computation.71 | loop fusion | flops 9437184 | bytes 6291456 | tf_op jit(solution)/shard_map/concatenate | solution.py:23
  12.5 3.5 %reduce-window.6 = s32[4,32,3,128]{3,1,2,0:T(8,128)S(1)} reduce-window(s32[4,32,3,128]{3,1,2,0:T(8,128)S(1)} %copy_bitcast_fusion, s32[]{:T(128)} %constant.58.clone.1), window={size=1x1x1x128 pad=0_0x0_0x0_0x127_0}, to_apply=%region_2.3 | reduce-window | flops 6242304 | bytes 393220 | tf_op jit(solution)/shard_map/reduce-window
  17.3 5.2 %scatter_custom_fusion = s32[1280]{0:T(1024)S(1)} fusion(s32[1280]{0:T(1024)S(1)} %reshape.262, s32[1280]{0:T(1024)S(1)} %reshape.264, s32[]{:T(128)} %constant.58.clone.1), kind=kCustom, calls=%fused_computation.113 | custom fusion | bytes 5124
  25.3 3.0 gather_fusion
  28.3 3.4 %reshape.235 = bf16[1,32,10,2048]{3,2,1,0:T(8,128)(2,1)} reshape(bf16[320,2048]{1,0:T(8,128)(2,1)} %gather_fusion) | data formatting | bytes 2621440 | tf_op jit(solution)/shard_map/reshape | solution.py:114
  31.7 25.7 %all-to-all-start = ((bf16[1,32,10,2048]{3,2,0,1:T(8,128)(2,1)}), bf16[1,32,10,2048]{3,2,0,1:T(8,128)(2,1)}, u32[]{:S(2)}, u32[]{:S(2)}) async-start(bf16[1,32,10,2048]{3,2,0,1:T(8,128)(2,1)} %bitcast.131), calls=%async_computation | async-start | bytes 4194304 | tf_op jit(solution)/shard_map/all_to_all | solution.py:113
  58.4 3.8 %collective-permute-start = (bf16[30,2048]{1,0:T(8,128)(2,1)S(1)}, bf16[30,2048]{1,0:T(8,128)(2,1)S(1)}, u32[]{:S(2)}, u32[]{:S(2)}) collective-permute-start(bf16[30,2048]{1,0:T(8,128)(2,1)S(1)} %slice.207), channel_id=1, source_target_pairs={{0,4},{4,8},{8,12},{12,16},{16,20},{20,24},{24,28},{28,32},{32,36}... | collective-permute-start | bytes 368648 | tf_op jit(solution)/shard_map/ppermute | solution.py:18
  65.1 81.0 %collective-permute-done = bf16[30,2048]{1,0:T(8,128)(2,1)S(1)} collective-permute-done((bf16[30,2048]{1,0:T(8,128)(2,1)S(1)}, bf16[30,2048]{1,0:T(8,128)(2,1)S(1)}, u32[]{:S(2)}, u32[]{:S(2)}) %collective-permute-start) | collective-permute-done | bytes 122912 | tf_op jit(solution)/shard_map/ppermute | solution.py:18
  146.1 4.9 %maximum_convert_fusion = f32[670,2048]{1,0:T(8,128)} fusion(bf16[640,2048]{1,0:T(8,128)(2,1)} %param.12, bf16[30,2048]{1,0:T(8,128)(2,1)S(1)} %collective-permute-done), kind=kLoop, calls=%fused_computation.72 | loop fusion | flops 5488640 | bytes 8232960 | tf_op jit(solution)/shard_map/convert_element_type | solution.py:80
  151.0 5.1 %all-to-all-done = bf16[1,32,10,2048]{3,2,0,1:T(8,128)(2,1)} async-done(((bf16[1,32,10,2048]{3,2,0,1:T(8,128)(2,1)}), bf16[1,32,10,2048]{3,2,0,1:T(8,128)(2,1)}, u32[]{:S(2)}, u32[]{:S(2)}) %all-to-all-start) | async-done | bytes 1310752 | tf_op jit(solution)/shard_map/all_to_all | solution.py:113
  156.2 4.6 %fusion.33 = f32[1,32,1,10,1024]{4,1,3,0,2:T(8,128)S(1)} fusion(bf16[1024,6144]{0,1:T(8,128)(2,1)} %all-gather.2.cloned.1.call-done, bf16[1,32,10,2048]{3,2,0,1:T(8,128)(2,1)} %all-to-all-done), kind=kOutput, calls=%fused_computation.77 | convolution fusion | flops 1342177280 | bytes 7602176 | tf_op jit(solution)/shard_map/qsjcd,jdf->qsjcf/dot_general | solution.py:125
  162.6 3.4 %fusion.36 = bf16[1,32,1,10,1024]{4,1,3,0,2:T(8,128)(2,1)S(1)} fusion(bf16[1024,6144]{0,1:T(8,128)(2,1)S(1)} %copy-done.1, f32[1,32,1,10,1024]{4,1,3,0,2:T(8,128)S(1)} %fusion.33, bf16[1,32,10,2048]{3,2,0,1:T(8,128)(2,1)} %all-to-all-done), kind=kOutput, calls=%fused_computation.80 | convolution fusion | flops 1344143360 | bytes 7471104 | tf_op jit(solution)/shard_map/qsjcd,jdf->qsjcf/dot_general | solution.py:128
  166.5 4.6 %slice.311 = bf16[1024,2048]{0,1:T(8,128)(2,1)} slice(bf16[1024,6144]{0,1:T(8,128)(2,1)} %all-gather.2.cloned.1.call-done), slice={[0:1024], [4096:6144]} | slice | bytes 8388608 | tf_op jit(solution)/shard_map/slice | solution.py:26
  171.1 6.5 %copy.45 = bf16[1024,2048]{1,0:T(8,128)(2,1)} copy(bf16[1024,2048]{0,1:T(8,128)(2,1)} %slice.311) | data formatting | bytes 8388608 | tf_op jit(solution)/shard_map/reshape.22
  177.6 5.1 %convert_reduce_fusion = bf16[2048,32,10]{0,1,2:T(8,128)(2,1)} fusion(bf16[4,256,2048,1]{2,1,3,0:T(8,128)(2,1)} %bitcast.132, bf16[32,10,4,256]{3,2,0,1:T(4,128)(2,1)S(1)} %reshape.239), kind=kOutput, calls=%fused_computation.64 | convolution fusion | flops 1346764800 | bytes 6160384 | tf_op jit(solution)/shard_map/sjctf,jtfd->sjctd/dot_general | solution.py:134
  182.7 3.1 %reshape_reshape_reshape_reshape.3 = bf16[16,2,1,10,2048]{4,1,0,3,2:T(2,128)(2,1)S(1)} reshape(bf16[32,10,2048]{2,0,1:T(8,128)(2,1)} %bitcast.134) | data formatting | bytes 2621440 | tf_op jit(solution)/shard_map/reshape;reshape;reshape;reshape | solution.py:46
  186.3 7.0 %all_to_all.15 = bf16[16,2,1,10,2048]{4,0,3,2,1:T(8,128)(2,1)S(1)} all-to-all(bf16[16,2,1,10,2048]{4,0,3,2,1:T(8,128)(2,1)S(1)} %copy.40), channel_id=1, replica_groups=mesh['grp'=2,'ep_0'=16,'ep_1'=2,'tp'=4] {'ep_1'}, dimensions={1} | all-to-all | bytes 2621440 | tf_op jit(solution)/shard_map/all_to_all | solution.py:48
  195.7 9.2 %all-to-all-start.2 = ((bf16[16,2,1,10,2048]{4,1,3,2,0:T(2,128)(2,1)}), bf16[16,2,1,10,2048]{4,1,3,2,0:T(2,128)(2,1)S(1)}, u32[]{:S(2)}, u32[]{:S(2)}) async-start(bf16[16,2,1,10,2048]{4,1,3,2,0:T(2,128)(2,1)} %copy.41), calls=%async_computation.2 | async-start | bytes 2621440 | tf_op jit(solution)/shard_map/all_to_all | solution.py:48
  205.0 73.5 %multiply_reduce_fusion = (f32[640]{0:T(1024)S(1)}, f32[640,2048]{1,0:T(8,128)S(1)}) fusion(f32[2048]{0:T(1024)} %bitcast.147, f32[670,2048]{1,0:T(8,128)} %maximum_convert_fusion, f32[2048]{0:T(1024)} %bitcast.148, f32[2048]{0:T(1024)} %bitcast.150, f32[2048]{0:T(1024)} %bitcast.151, f32[2048]{0:T(1024)} %bitcast.152, f32[2048]{0:T(1024)} %bitcast.153, ...), kind=kLoop, calls=%fused_computation.66 | loop fusion | flops 82574720 | bytes 168028672 | tf_op jit(solution)/shard_map/reduce_sum | solution.py:59
  278.5 2.5 fusion.37
  282.9 2.5 reshape_reshape_reshape.3
  285.5 3.0 gather_fusion.1
  288.5 4.1 %reshape.245 = f32[160,2,2048]{2,1,0:T(2,128)} reshape(bf16[320,2048]{1,0:T(8,128)(2,1)} %gather_fusion.1) | data formatting | bytes 3932160 | tf_op jit(solution)/shard_map/convert_element_type | solution.py:150
  292.6 5.8 %multiply_reduce_fusion.1 = f32[160,2048]{1,0:T(8,128)S(1)} fusion(f32[160,2,2048]{2,1,0:T(2,128)} %reshape.245, f32[160,2]{1,0:T(8,128)S(1)} %copy.43), kind=kLoop, calls=%fused_computation.73 | loop fusion | flops 983040 | bytes 3933440 | tf_op jit(solution)/shard_map/reduce_sum | solution.py:152
  (68 shorter events, 18.4 us)
Async XLA Ops:
  7.2 271.3 %copy-start = (bf16[2048,512]{1,0:T(8,128)(2,1)S(1)}, bf16[2048,512]{1,0:T(8,128)(2,1)}, u32[]{:S(2)}) copy-start(bf16[2048,512]{1,0:T(8,128)(2,1)} %param.15) | copy-start | bytes 6291460
  7.2 149.0 %all-gather.2.cloned.1.call-start = ((), (), s32[]{:S(2)}) async-start(), calls=%async_computation.3 | async-start | bytes 15728640 | tf_op jit(solution)/shard_map/all_gather | solution.py:24
  8.9 3.2 %copy-start.3 = (s32[640,2]{0,1:T(2,128)S(1)}, s32[640,2]{0,1:T(2,128)}, u32[]{:S(2)}) copy-start(s32[640,2]{0,1:T(2,128)} %param.18) | copy-start | bytes 15364
  8.9 8.0 %copy-start.8 = (s32[2]{0:T(128)S(1)}, s32[2]{0:T(128)}, u32[]{:S(2)}) copy-start(s32[2]{0:T(128)} %constant.72) | copy-start | bytes 28
  8.9 8.1 %copy-start.7 = (s32[2]{0:T(128)S(1)}, s32[2]{0:T(128)}, u32[]{:S(2)}) copy-start(s32[2]{0:T(128)} %constant.75) | copy-start | bytes 28
  8.9 15.0 %copy-start.5 = (f32[2048]{0:T(1024)S(1)}, f32[2048]{0:T(1024)}, u32[]{:S(2)}) copy-start(f32[2048]{0:T(1024)} %param.17) | copy-start | bytes 24580
  28.3 33.9 %copy-start.2 = (f32[31,2048]{1,0:T(8,128)S(1)}, f32[31,2048]{1,0:T(8,128)}, u32[]{:S(2)}) copy-start(f32[31,2048]{1,0:T(8,128)} %param.13) | copy-start | bytes 761860
  31.7 124.4 %all-to-all-start = ((bf16[1,32,10,2048]{3,2,0,1:T(8,128)(2,1)}), bf16[1,32,10,2048]{3,2,0,1:T(8,128)(2,1)}, u32[]{:S(2)}, u32[]{:S(2)}) async-start(bf16[1,32,10,2048]{3,2,0,1:T(8,128)(2,1)} %bitcast.131), calls=%async_computation | async-start | bytes 4194304 | tf_op jit(solution)/shard_map/all_to_all | solution.py:113
  58.4 87.7 %collective-permute-start = (bf16[30,2048]{1,0:T(8,128)(2,1)S(1)}, bf16[30,2048]{1,0:T(8,128)(2,1)S(1)}, u32[]{:S(2)}, u32[]{:S(2)}) collective-permute-start(bf16[30,2048]{1,0:T(8,128)(2,1)S(1)} %slice.207), channel_id=1, source_target_pairs={{0,4},{4,8},{8,12},{12,16},{16,20},{20,24},{24,28},{28,32},{32,36}... | collective-permute-start | bytes 368648 | tf_op jit(solution)/shard_map/ppermute | solution.py:18
  156.2 6.4 %copy-start.1 = (bf16[1024,6144]{0,1:T(8,128)(2,1)S(1)}, bf16[1024,6144]{0,1:T(8,128)(2,1)}, u32[]{:S(2)}) copy-start(bf16[1024,6144]{0,1:T(8,128)(2,1)} %all-gather.2.cloned.1.call-done) | copy-start | bytes 37748740
  195.7 85.2 %all-to-all-start.2 = ((bf16[16,2,1,10,2048]{4,1,3,2,0:T(2,128)(2,1)}), bf16[16,2,1,10,2048]{4,1,3,2,0:T(2,128)(2,1)S(1)}, u32[]{:S(2)}, u32[]{:S(2)}) async-start(bf16[16,2,1,10,2048]{4,1,3,2,0:T(2,128)(2,1)} %copy.41), calls=%async_computation.2 | async-start | bytes 2621440 | tf_op jit(solution)/shard_map/all_to_all | solution.py:48
  204.9 73.5 %copy-start.9 = (f32[2048]{0:T(1024)S(1)}, f32[2048]{0:T(1024)}, u32[]{:S(2)}) copy-start(f32[2048]{0:T(1024)} %param.14) | copy-start | bytes 24580
  280.9 4.5 %copy-start.4 = (s32[1024]{0:T(1024)S(1)}, s32[1024]{0:T(1024)}, u32[]{:S(2)}) copy-start(s32[1024]{0:T(1024)} %pad_clamp_fusion) | copy-start | bytes 12292
  288.5 10.1 %copy-start.6 = (f32[2048]{0:T(1024)S(1)}, f32[2048]{0:T(1024)}, u32[]{:S(2)}) copy-start(f32[2048]{0:T(1024)} %param.23) | copy-start | bytes 24580
Sparse Core Ops, SparseCore 0:
  12.2 140.7 all-gather.1
where the time goes:
time: 307 us; the launch traced here: 306 us
  other arithmetic  95.7 us (31%)
  waiting for transfers between devices  86.2 us (28%)
  local copies, waits for them, and re-layouts  48.8 us (16%)
  starting transfers between devices  38.7 us (13%)
  matrix products  15.6 us (5%)
  between operations  14.4 us (5%)
  blocking collectives  7.04 us (2%)
    ppermute x1, waiting for transfers between devices, shifted(): return lax.ppermute(shard, axis, pairs)  81 us
    reduce_sum x3, other arithmetic, channel_norm(): mean_square = jnp.mean(values * values, axis=-1, keepdims=True)  74.9 us
    all_to_all x1, starting transfers between devices, body(): lax.all_to_all(normed[own_source // 2].reshape(1, ep_count, local_experts...  25.7 us
    all_to_all x1, starting transfers between devices, moved_by_axis(): out = lax.all_to_all(out, axes[k], k, k, tiled=True)  9.21 us
    unnamed x24, local copies, waits for them, and re-layouts  8.95 us
    all_to_all x1, blocking collectives, moved_by_axis(): out = lax.all_to_all(out, axes[k], k, k, tiled=True)  7.04 us
    another operation x4, local copies, waits for them, and re-layouts  6.98 us
  transfers between devices with their start and end apart: 4, of which 2 were waited for; matrix products, arithmetic and copies ran while one was open for 34% of the time, Pallas kernels for 0%

commit v1 on v0

v1 whole, which is shorter than its diff:
```python
import jax
import jax.numpy as jnp
from jax import lax
from jax.experimental import pallas as pl
from jax.experimental.pallas import tpu as pltpu
from jax.sharding import PartitionSpec as P

EPSILON = 1e-06
LANES = 128
F32 = jnp.float32
BF16 = jnp.bfloat16


def whole():
    return pl.BlockSpec(memory_space=pltpu.VMEM)


def dot(a, b):
    return jnp.dot(a, b, preferred_element_type=F32)


def split_rows(capacity):
    main = capacity // 8 * 8
    return main, capacity - main


def col(ref_or_value, c):
    return ref_or_value[:, c * LANES : (c + 1) * LANES]


def selection(index, first, count, dim):
    shape = (count, index.shape[1]) if dim == 0 else (index.shape[0], count)
    return index == first + lax.broadcasted_iota(jnp.int32, shape, dim)


def put_message(out_ref, head_of, tail_of, peers, head, tail, blocks):
    for c in range(0, blocks, 2):
        pair = [head_of(c + i).reshape(peers, head, LANES) for i in range(2)]
        out_ref[:, c * head : (c + 2) * head, :] = jnp.concatenate(pair, axis=1).astype(BF16)
    per = 8 // tail
    base = blocks * head
    for j in range(0, blocks // per, 2):
        pair = [tail_of(j + i).reshape(peers, 8, LANES) for i in range(2)]
        out_ref[:, base + j * 8 : base + (j + 2) * 8, :] = jnp.concatenate(pair, axis=1).astype(BF16)


def dispatch_kernel(own_ref, rows_ref, gain_ref, ids_ref, out_ref, target_ref, *, experts, capacity):
    del own_ref
    tokens, width = rows_ref.shape
    blocks = width // LANES
    head, tail = split_rows(capacity)
    per = 8 // tail
    rows = rows_ref[...].astype(F32)
    mean_square = jnp.mean(rows * rows, axis=-1, keepdims=True)
    normed = (rows * lax.rsqrt(mean_square + EPSILON) * gain_ref[...]).astype(BF16)
    ids = ids_ref[...]
    onehot = [
        (ids[k : k + 1, :] == lax.broadcasted_iota(jnp.int32, (experts, tokens), 0)).astype(F32)
        for k in range(2)
    ]
    before = lax.broadcasted_iota(jnp.int32, (tokens, tokens), 0) < lax.broadcasted_iota(
        jnp.int32, (tokens, tokens), 1
    )
    before = before.astype(F32).astype(BF16)
    counts = [dot(h.astype(BF16), before) for h in onehot]
    counts[1] = counts[1] + jnp.sum(onehot[0], axis=1, keepdims=True)
    place = [jnp.sum(c * h, axis=0, keepdims=True).astype(jnp.int32) for c, h in zip(counts, onehot)]
    place = jnp.concatenate(place, axis=0)
    target_ref[...] = ids * capacity + place
    in_head = jnp.where(place < head, ids * head + place, -64)
    in_tail = jnp.where(place < head, -64, ids * 8 + place - head)
    pick = jnp.zeros((experts * head, tokens), F32)
    picks = [jnp.zeros((experts * 8, tokens), F32) for _ in range(per)]
    for k in range(2):
        pick = pick + selection(in_head[k : k + 1], 0, experts * head, 0).astype(F32)
        for q in range(per):
            picks[q] = picks[q] + selection(in_tail[k : k + 1], -q * tail, experts * 8, 0).astype(F32)
    pick = pick.astype(BF16)
    picks = jnp.concatenate(picks, axis=1).astype(BF16)

    def tail_of(j):
        stack = [col(normed, per * j + q) for q in range(per)]
        return dot(picks, jnp.concatenate(stack, axis=0))

    put_message(
        out_ref, lambda c: dot(pick, col(normed, c)), tail_of, experts, head, tail, blocks
    )


def dispatch(own, rows, gain, ids, experts, capacity):
    tokens = ids.shape[1]
    width = rows.shape[1]
    grid_spec = pltpu.PrefetchScalarGridSpec(
        num_scalar_prefetch=1,
        grid=(1,),
        in_specs=[
            pl.BlockSpec((tokens, width), lambda i, own: (own[0], 0)),
            pl.BlockSpec((1, width), lambda i, own: (0, 0)),
            pl.BlockSpec((2, tokens), lambda i, own: (0, 0)),
        ],
        out_specs=[
            pl.BlockSpec((experts, capacity * width // LANES, LANES), lambda i, own: (0, 0, 0)),
            pl.BlockSpec((2, tokens), lambda i, own: (0, 0)),
        ],
    )

    def kernel(*refs):
        dispatch_kernel(*refs, experts=experts, capacity=capacity)

    return pl.pallas_call(
        kernel,
        grid_spec=grid_spec,
        out_shape=[
            jax.ShapeDtypeStruct((experts, capacity * width // LANES, LANES), BF16),
            jax.ShapeDtypeStruct((2, tokens), jnp.int32),
        ],
        compiler_params=pltpu.CompilerParams(vmem_limit_bytes=24 << 20),
        name="dispatch",
    )(own, rows, gain, ids)


def expert_kernel(*refs, sources, peers, capacity, blocks):
    count = len(refs) // 2 - 2
    message_ref, out_ref = refs[0], refs[count + 1]
    remote = refs[1 : count + 1]
    rows_ref, hidden_ref, signals = refs[count + 2], refs[count + 3], refs[-1]
    weights = refs[count + 4 : -1]
    copies = [
        pltpu.make_async_copy(far, near, signals.at[i])
        for i, (far, near) in enumerate(zip(remote, weights))
    ]
    for copy in copies:
        copy.start()
    head, tail = split_rows(capacity)
    per = 8 // tail
    heads = peers * head
    for c in range(0, blocks, 2):
        both = message_ref[:, c * head : (c + 2) * head, :].astype(F32)
        for i in range(2):
            part = both[:, i * head : (i + 1) * head, :].reshape(heads, LANES)
            rows_ref[0:heads, (c + i) * LANES : (c + i + 1) * LANES] = part.astype(BF16)
    base = blocks * head
    slot = lax.broadcasted_iota(jnp.int32, (peers * tail, peers * 8), 0)
    lane = lax.broadcasted_iota(jnp.int32, (peers * tail, peers * 8), 1)
    gathers = [
        (lane == slot // tail * 8 + q * tail + slot % tail).astype(F32).astype(BF16)
        for q in range(per)
    ]
    for j in range(0, blocks // per, 2):
        both = message_ref[:, base + j * 8 : base + (j + 2) * 8, :].astype(F32)
        for i in range(2):
            part = both[:, i * 8 : (i + 1) * 8, :].reshape(peers * 8, LANES).astype(BF16)
            for q in range(per):
                c = per * (j + i) + q
                rows_ref[heads:, c * LANES : (c + 1) * LANES] = dot(gathers[q], part).astype(BF16)
    at = 0
    downs = []
    for gates, ups, down_parts in sources:
        rows = rows_ref[...]
        values = []
        for group in (gates, ups):
            value = None
            begin = 0
            for g in group:
                copies[g].wait()
                size = weights[g].shape[0]
                part = dot(rows[:, begin : begin + size], weights[g][...])
                value = part if value is None else value + part
                begin += size
            values.append(value)
        gate_value, up_value = values
        hidden = gate_value / (1.0 + jnp.exp(-gate_value)) * up_value
        hidden_ref[:, at : at + hidden.shape[1]] = hidden.astype(BF16)
        for d in down_parts:
            downs.append((at, d))
            at += weights[d].shape[0]
    for _, d in downs:
        copies[d].wait()
    slot = lax.broadcasted_iota(jnp.int32, (peers * 8, peers * tail), 1)
    lane = lax.broadcasted_iota(jnp.int32, (peers * 8, peers * tail), 0)
    spreads = [
        (lane == slot // tail * 8 + q * tail + slot % tail).astype(F32).astype(BF16)
        for q in range(per)
    ]
    step = 2 * per
    for first in range(0, blocks, step):
        cols = slice(first * LANES, (first + step) * LANES)
        total = None
        for begin, d in downs:
            size = weights[d].shape[0]
            part = dot(hidden_ref[:, begin : begin + size], weights[d][:, cols])
            total = part if total is None else total + part
        for c in range(0, step, 2):
            pair = [col(total, c + i)[0:heads].reshape(peers, head, LANES) for i in range(2)]
            at_row = (first + c) * head
            out_ref[:, at_row : at_row + 2 * head, :] = jnp.concatenate(pair, axis=1).astype(BF16)
        last = total[heads:].astype(BF16)
        pair = []
        for i in range(2):
            spread = None
            for q in range(per):
                part = dot(spreads[q], col(last, per * i + q))
                spread = part if spread is None else spread + part
            pair.append(spread.reshape(peers, 8, LANES))
        at_row = base + first // per * 8
        out_ref[:, at_row : at_row + 16, :] = jnp.concatenate(pair, axis=1).astype(BF16)


def experts_apply(message, weights, sources, capacity):
    peers, lines, _ = message.shape
    blocks = lines // capacity
    units = sum(weights[d].shape[0] for s in sources for d in s[2])

    def kernel(*refs):
        expert_kernel(*refs, sources=sources, peers=peers, capacity=capacity, blocks=blocks)

    return pl.pallas_call(
        kernel,
        in_specs=[whole()] + [pl.BlockSpec(memory_space=pltpu.HBM)] * len(weights),
        out_specs=whole(),
        out_shape=jax.ShapeDtypeStruct(message.shape, BF16),
        scratch_shapes=[
            pltpu.VMEM((peers * capacity, blocks * LANES), BF16),
            pltpu.VMEM((peers * capacity, units), BF16),
            *(pltpu.VMEM(w.shape, BF16) for w in weights),
            pltpu.SemaphoreType.DMA((len(weights),)),
        ],
        compiler_params=pltpu.CompilerParams(vmem_limit_bytes=60 << 20),
        name="experts",
    )(message, *weights)


def combine_kernel(message_ref, target_ref, weight_ref, gain_ref, out_ref, mixed_ref, *, capacity):
    peers = message_ref.shape[0]
    tokens, width = out_ref.shape
    blocks = width // LANES
    head, tail = split_rows(capacity)
    per = 8 // tail
    heads = peers * head
    target = target_ref[...]
    peer = target // capacity
    place = target - peer * capacity
    in_head = jnp.where(place < head, peer * head + place, -64)
    in_tail = jnp.where(place < head, -64, peer * 8 + place - head)
    pick = [selection(in_head[:, k : k + 1], 0, heads, 1).astype(F32) for k in range(2)]
    pick = jnp.concatenate(pick, axis=0).astype(BF16)
    picks = []
    for q in range(per):
        both = [selection(in_tail[:, k : k + 1], -q * tail, peers * 8, 1).astype(F32) for k in range(2)]
        picks.append(jnp.concatenate(both, axis=0).astype(BF16))
    weight = [weight_ref[:, k : k + 1] for k in range(2)]
    base = blocks * head
    square = jnp.zeros((tokens, LANES), F32)
    for c in range(0, blocks, 2):
        both = message_ref[:, c * head : (c + 2) * head, :].astype(F32)
        for i in range(2):
            part = both[:, i * head : (i + 1) * head, :].reshape(heads, LANES).astype(BF16)
            j = (c + i) // per
            rest = message_ref[:, base + j // 2 * 16 : base + j // 2 * 16 + 16, :].astype(F32)
            rest = rest[:, j % 2 * 8 : j % 2 * 8 + 8, :].reshape(peers * 8, LANES).astype(BF16)
            rows = dot(pick, part) + dot(picks[(c + i) % per], rest)
            mixed = rows[:tokens] * weight[0] + rows[tokens:] * weight[1]
            mixed_ref[:, (c + i) * LANES : (c + i + 1) * LANES] = mixed
            square = square + mixed * mixed
    scale = lax.rsqrt(jnp.sum(square, axis=1, keepdims=True) * (1.0 / width) + EPSILON)
    out_ref[...] = (mixed_ref[...] * scale * gain_ref[...]).astype(BF16)


def combine(message, target, weight, gain, capacity):
    tokens = target.shape[0]
    width = gain.shape[1]

    def kernel(*refs):
        combine_kernel(*refs, capacity=capacity)

    return pl.pallas_call(
        kernel,
        in_specs=[whole()] * 4,
        out_specs=whole(),
        out_shape=jax.ShapeDtypeStruct((tokens, width), BF16),
        scratch_shapes=[pltpu.VMEM((tokens, width), F32)],
        compiler_params=pltpu.CompilerParams(vmem_limit_bytes=24 << 20),
        name="combine",
    )(message, target, weight, gain)


def conv_kernel(rows_ref, carried_ref, taps_ref, gain_ref, weight_ref, out_ref, line_ref, sum_ref):
    block, width = rows_ref.shape
    blocks = width // LANES
    reach = taps_ref.shape[0] - 1
    halo = line_ref.shape[1] - block
    step = pl.program_id(0)

    @pl.when(step == 0)
    def _():
        for c in range(blocks):
            line_ref[c, 0:halo, :] = col(carried_ref, c).astype(F32)

    @pl.when(step > 0)
    def _():
        for c in range(blocks):
            line_ref[c, 0:halo, :] = line_ref[c, block : block + halo, :]

    for c in range(blocks):
        line_ref[c, halo:, :] = col(rows_ref, c).astype(F32)

    strip = 64

    def column(c, square):
        parts = []
        for first in range(0, block, strip):
            total = jnp.zeros((strip, LANES), F32)
            for k in range(reach + 1):
                at = first + halo - reach + k
                total = total + line_ref[c, at : at + strip, :] * taps_ref[k, pl.ds(c, 1), :]
            sum_ref[c, first : first + strip, :] = total
            parts.append(total * total)
        return square + jnp.concatenate(parts, axis=0)

    square = lax.fori_loop(0, blocks, column, jnp.zeros((block, LANES), F32))
    scale = lax.rsqrt(jnp.sum(square, axis=1, keepdims=True) * (1.0 / width) + EPSILON)
    result = jnp.zeros((block, out_ref.shape[1]), F32)
    for c in range(0, blocks, 4):
        group = []
        for i in range(4):
            value = sum_ref[c + i] * scale * col(gain_ref, c + i)
            group.append((value / (1.0 + jnp.exp(-value))).astype(BF16))
        part = jnp.concatenate(group, axis=1)
        result = result + dot(part, weight_ref[c * LANES : (c + 4) * LANES, :])
    out_ref[...] = result.astype(BF16)


def conv_module(rows, carried, taps, gain, weight, block=128):
    count, width = rows.shape
    blocks = width // LANES
    halo = carried.shape[0]
    return pl.pallas_call(
        conv_kernel,
        grid=(count // block,),
        in_specs=[
            pl.BlockSpec((block, width), lambda i: (i, 0)),
            pl.BlockSpec((halo, width), lambda i: (0, 0)),
            pl.BlockSpec((taps.shape[0], blocks, LANES), lambda i: (0, 0, 0)),
            pl.BlockSpec((1, width), lambda i: (0, 0)),
            pl.BlockSpec(weight.shape, lambda i: (0, 0)),
        ],
        out_specs=pl.BlockSpec((block, weight.shape[1]), lambda i: (i, 0)),
        out_shape=jax.ShapeDtypeStruct((count, weight.shape[1]), BF16),
        scratch_shapes=[
            pltpu.VMEM((blocks, block + halo, LANES), F32),
            pltpu.VMEM((blocks, block, LANES), F32),
        ],
        compiler_params=pltpu.CompilerParams(vmem_limit_bytes=24 << 20),
        name="conv",
    )(rows, carried, taps.reshape(taps.shape[0], blocks, LANES), gain, weight)


EP = "ep"
GRP_EP = ("grp", "ep")
GRP_EP_TP = ("grp", "ep", "tp")
HALO = 32


def run(
    conv_input,
    conv_taps,
    conv_gain,
    conv_weight,
    moe_input,
    moe_gain,
    expert_ids,
    route_weights,
    gate_weight,
    up_weight,
    down_weight,
    post_gain,
):
    quarters = lax.axis_size("tp")
    ep_count = lax.axis_size(EP)
    width = moe_input.shape[1]
    tokens = moe_input.shape[0] // quarters
    capacity = 2 * tokens // ep_count
    own = lax.axis_index("tp").astype(jnp.int32)

    right = [(i, (i + 1) % quarters) for i in range(quarters)]
    left = [(i, (i - 1) % quarters) for i in range(quarters)]
    gate, up, down = gate_weight[0], up_weight[0], down_weight[0]
    half = down.shape[0] // 2
    down_a, down_b = down[:half], down[half:]

    def send(array, pairs):
        return lax.ppermute(array, "tp", pairs)

    gate_r, up_l = send(gate, right), send(up, left)
    own_ids = lax.dynamic_slice_in_dim(expert_ids, own * tokens, tokens, 0).T
    message, target = dispatch(
        own.reshape(1), moe_input, moe_gain.reshape(1, width), own_ids, ep_count, capacity
    )
    arrived = lax.all_to_all(message, EP, 0, 0, tiled=True)
    down_r, down_l = send(down_a, right), send(down_b, left)
    up_r, gate_l = send(up, right), send(gate, left)
    rest_r, rest_l = send(down_b, right), send(down_a, left)
    gate_far, up_far = send(gate_r, right), send(up_l, left)
    down_far, rest_far = send(down_r, right), send(down_l, left)

    pairs = [(i, i + 1) for i in range(ep_count - 1)]
    carried = lax.ppermute(conv_input[conv_input.shape[0] - HALO :], EP, pairs)
    conv_out = conv_module(conv_input, carried, conv_taps, conv_gain.reshape(1, width), conv_weight)

    weights = [gate, up, down]
    sources = [((0,), (1,), (2,))]
    for arrays in (
        (gate_r, up_r, down_r, rest_r),
        (gate_l, up_l, rest_l, down_l),
        (gate_far, up_far, down_far, rest_far),
    ):
        at = len(weights)
        weights.extend(arrays)
        sources.append(((at,), (at + 1,), (at + 2, at + 3)))
    results = experts_apply(arrived, weights, tuple(sources), capacity)
    returned = lax.all_to_all(results, EP, 0, 0, tiled=True)
    own_weights = lax.dynamic_slice_in_dim(route_weights, own * tokens, tokens, 0)
    moe_out = combine(returned, target.T, own_weights, post_gain.reshape(1, width), capacity)
    return (conv_out, moe_out)


def solution(mesh):
    return jax.shard_map(
        run,
        mesh=mesh,
        in_specs=(
            P(GRP_EP, None),
            P(),
            P(),
            P(None, "tp"),
            P(GRP_EP, None),
            P(),
            P(GRP_EP, None),
            P(GRP_EP, None),
            P(EP, None, "tp"),
            P(EP, None, "tp"),
            P(EP, "tp", None),
            P(),
        ),
        out_specs=(P(GRP_EP, "tp"), P(GRP_EP_TP, None)),
        check_vma=False,
    )
```

time: 307 us -> 250 us (0.81)
  other arithmetic: 95.7 us -> 0 us
  waiting for transfers between devices: 86.2 us -> 139 us
  Pallas kernels: 0 us -> 36.6 us
  local copies, waits for them, and re-layouts: 48.8 us -> 14.5 us
  starting transfers between devices: 38.7 us -> 58.2 us
  matrix products: 15.6 us -> 0 us
  between operations: 14.4 us -> 0.84 us
  blocking collectives: 7.04 us -> 0 us
    reduce_sum x5 -> x0, other arithmetic: 80.8 us -> none  [the longest x3 74.9 us: channel_norm(): mean_square = jnp.mean(values * values, axis=-1, keepdims=True)]
    ppermute x1 -> x13, waiting for transfers between devices: 81 us -> 139 us  [the longest x12 91.5 us: send(): return lax.ppermute(array, 'tp', pairs)]
    pallas_call x0 -> x4, Pallas kernels: none -> 36.6 us  [the longest x1 17.6 us: conv_module(): pl.pallas_call(conv_kernel, grid=(count // block,), in_specs=[pl.BlockSpe...]
    dot_general x4 -> x0, matrix products: 15.6 us -> none  [the longest x1 5.09 us: body(): jnp.einsum('sjctf,jtfd->sjctd', pieces, down_pieces, preferred_element_ty...]
    ppermute x1 -> x13, starting transfers between devices: 3.75 us -> 17.6 us  [the longest x12 14 us: send(): return lax.ppermute(array, 'tp', pairs)]
    another operation x7 -> x0, local copies, waits for them, and re-layouts: 13.1 us -> none
    convert_element_type x3 -> x0, other arithmetic: 7.26 us -> none  [the longest x1 4.93 us: body(): jnp.concatenate([carried, conv_input], axis=0).astype(jnp.float32)]
    all_to_all x1 -> x0, blocking collectives: 7.04 us -> none  [moved_by_axis(): out = lax.all_to_all(out, axes[k], k, k, tiled=True)]
  transfers between devices with their start and end apart: 4 -> 15, of which waited for: 2 -> 6; matrix products, arithmetic and copies ran while one was open for 34% -> 2% of each run, Pallas kernels for 0% -> 7%
where the time goes in v1:
time: 250 us; the launch traced here: 249 us
  waiting for transfers between devices  139 us (56%)
  starting transfers between devices  58.2 us (23%)
  Pallas kernels  36.6 us (15%)
  local copies, waits for them, and re-layouts  14.5 us (6%)
    ppermute x12, waiting for transfers between devices, send(): return lax.ppermute(array, 'tp', pairs)  91.5 us
    ppermute x1, waiting for transfers between devices, run(): carried = lax.ppermute(conv_input[conv_input.shape[0] - HALO:], EP, pairs)  47.6 us
    all_to_all x1, starting transfers between devices, run(): arrived = lax.all_to_all(message, EP, 0, 0, tiled=True)  25.6 us
    pallas_call x1, Pallas kernels, conv_module(): pl.pallas_call(conv_kernel, grid=(count // block,), in_specs=[pl.BlockSpe...  17.6 us
    all_to_all x1, starting transfers between devices, run(): returned = lax.all_to_all(results, EP, 0, 0, tiled=True)  15 us
    ppermute x12, starting transfers between devices, send(): return lax.ppermute(array, 'tp', pairs)  14 us
    pallas_call x1, Pallas kernels, experts_apply(): pl.pallas_call(kernel, in_specs=[whole()] + [pl.BlockSpec(memory_space=pl...  14 us
    unnamed x46, local copies, waits for them, and re-layouts  11.9 us
  transfers between devices with their start and end apart: 15, of which 6 were waited for; matrix products, arithmetic and copies ran while one was open for 2% of the time, Pallas kernels for 7%

profile of v1, /device:TPU:33, one launch (start us, length us, event | category | flops | bytes accessed | tf_op | source)
XLA Modules:
  0.0 249.3 jit_solution(12487013718510454974)
XLA Ops:
  1.4 1.7 copy-done.2
  3.8 2.5 dispatch.1
  6.3 25.6 %all-to-all-start = ((bf16[32,160,128]{2,1,0:T(8,128)(2,1)}), bf16[32,160,128]{2,1,0:T(8,128)(2,1)S(1)}, u32[]{:S(2)}, u32[]{:S(2)}) async-start(bf16[32,160,128]{2,1,0:T(8,128)(2,1)} %get-tuple-element.4), calls=%async_computation | async-start | bytes 2621440 | tf_op jit(solution)/shard_map/all_to_all | solution.py:399
  32.0 1.5 collective-permute-start.3
  33.5 2.5 %collective-permute-start.6 = (bf16[2048,256]{1,0:T(8,128)(2,1)S(1)}, bf16[2048,256]{1,0:T(8,128)(2,1)S(1)}, u32[]{:S(2)}, u32[]{:S(2)}) collective-permute-start(bf16[2048,256]{1,0:T(8,128)(2,1)S(1)} %bitcast.26), channel_id=1, source_target_pairs={{0,3},{1,0},{2,1},{3,2},{4,7},{5,4},{6,5},{7,6},{8,11},{9,8},{10,9... | collective-permute-start | bytes 3145736 | tf_op jit(solution)/shard_map/ppermute | solution.py:392
  36.0 2.7 %collective-permute-start.8 = (bf16[128,2048]{1,0:T(8,128)(2,1)S(1)}, bf16[128,2048]{1,0:T(8,128)(2,1)S(1)}, u32[]{:S(2)}, u32[]{:S(2)}) collective-permute-start(bf16[128,2048]{1,0:T(8,128)(2,1)S(1)} %get-tuple-element.6), channel_id=1, source_target_pairs={{0,3},{1,0},{2,1},{3,2},{4,7},{5,4},{6,5},{7,6},{8,11},{9,8},{10,9... | collective-permute-start | bytes 1572872 | tf_op jit(solution)/shard_map/ppermute | solution.py:392
  38.7 7.9 %collective-permute-done.3.refs_6_ = bf16[128,2048]{1,0:T(8,128)(2,1)S(1)} collective-permute-done((bf16[128,2048]{1,0:T(8,128)(2,1)S(1)}, bf16[128,2048]{1,0:T(8,128)(2,1)S(1)}, u32[]{:S(2)}, u32[]{:S(2)}) %collective-permute-start.3) | collective-permute-done | bytes 524320 | tf_op jit(solution)/shard_map/ppermute | solution.py:392
  46.6 1.2 collective-permute-start.7
  47.8 21.3 %collective-permute-done.8.refs_11_ = bf16[128,2048]{1,0:T(8,128)(2,1)S(1)} collective-permute-done((bf16[128,2048]{1,0:T(8,128)(2,1)S(1)}, bf16[128,2048]{1,0:T(8,128)(2,1)S(1)}, u32[]{:S(2)}, u32[]{:S(2)}) %collective-permute-start.8) | collective-permute-done | bytes 524320 | tf_op jit(solution)/shard_map/ppermute | solution.py:392
  69.8 10.5 %collective-permute-done.4.refs_7_ = bf16[128,2048]{1,0:T(8,128)(2,1)S(1)} collective-permute-done((bf16[128,2048]{1,0:T(8,128)(2,1)S(1)}, bf16[128,2048]{1,0:T(8,128)(2,1)S(1)}, u32[]{:S(2)}, u32[]{:S(2)}) %collective-permute-start.4) | collective-permute-done | bytes 524320 | tf_op jit(solution)/shard_map/ppermute | solution.py:392
  81.1 2.7 %collective-permute-start.5 = (bf16[2048,256]{1,0:T(8,128)(2,1)S(1)}, bf16[2048,256]{1,0:T(8,128)(2,1)S(1)}, u32[]{:S(2)}, u32[]{:S(2)}) collective-permute-start(bf16[2048,256]{1,0:T(8,128)(2,1)S(1)} %bitcast.24), channel_id=1, source_target_pairs={{0,3},{1,0},{2,1},{3,2},{4,7},{5,4},{6,5},{7,6},{8,11},{9,8},{10,9... | collective-permute-start | bytes 3145736 | tf_op jit(solution)/shard_map/ppermute | solution.py:392
  84.0 1.3 collective-permute-start.9
  85.3 28.7 %collective-permute-done.11.refs_14_ = bf16[128,2048]{1,0:T(8,128)(2,1)S(1)} collective-permute-done((bf16[128,2048]{1,0:T(8,128)(2,1)S(1)}, bf16[128,2048]{1,0:T(8,128)(2,1)S(1)}, u32[]{:S(2)}, u32[]{:S(2)}) %collective-permute-start.11) | collective-permute-done | bytes 524320 | tf_op jit(solution)/shard_map/ppermute | solution.py:392
  114.0 1.2 collective-permute-start.12
  115.2 23.1 %collective-permute-done.12.refs_15_ = bf16[128,2048]{1,0:T(8,128)(2,1)S(1)} collective-permute-done((bf16[128,2048]{1,0:T(8,128)(2,1)S(1)}, bf16[128,2048]{1,0:T(8,128)(2,1)S(1)}, u32[]{:S(2)}, u32[]{:S(2)}) %collective-permute-start.12) | collective-permute-done | bytes 524320 | tf_op jit(solution)/shard_map/ppermute | solution.py:392
  140.9 1.1 copy-done.8
  142.0 14.0 %experts.1 = bf16[32,160,128]{2,1,0:T(8,128)(2,1)} custom-call(bf16[32,160,128]{2,1,0:T(8,128)(2,1)} %copy-done.8, bf16[2048,256]{1,0:T(8,128)(2,1)} %bitcast.22, bf16[2048,256]{1,0:T(8,128)(2,1)} %bitcast.25, bf16[256,2048]{1,0:T(8,128)(2,1)} %bitcast.21, bf16[2048,256]{1,0:T(8,128)(2,1)} %copy-done.13, bf16[2048,256]{1,0:T(8,128)(2,1)} %copy-done.14, ...), custom_call_target="tpu_custom_call" | custom-call | tf_op jit(solution)/shard_map/experts/pallas_call | solution.py:217
  156.0 15.0 %all-to-all-start.1 = ((bf16[32,160,128]{2,1,0:T(8,128)(2,1)}), bf16[32,160,128]{2,1,0:T(8,128)(2,1)S(1)}, u32[]{:S(2)}, u32[]{:S(2)}) async-start(bf16[32,160,128]{2,1,0:T(8,128)(2,1)} %experts.1), calls=%async_computation.1 | async-start | bytes 2621440 | tf_op jit(solution)/shard_map/all_to_all | solution.py:421
  171.0 1.6 slice.15
  172.6 3.6 %collective-permute-start = (bf16[32,2048]{1,0:T(8,128)(2,1)}, bf16[32,2048]{1,0:T(8,128)(2,1)}, u32[]{:S(2)}, u32[]{:S(2)}) collective-permute-start(bf16[32,2048]{1,0:T(8,128)(2,1)} %slice.15), channel_id=1, source_target_pairs={{0,4},{4,8},{8,12},{12,16},{16,20},{20,24},{24,28},{28,32},{32,36}... | collective-permute-start | bytes 393224 | tf_op jit(solution)/shard_map/ppermute | solution.py:407
  178.8 47.6 %collective-permute-done.carried_ref = bf16[32,2048]{1,0:T(8,128)(2,1)} collective-permute-done((bf16[32,2048]{1,0:T(8,128)(2,1)}, bf16[32,2048]{1,0:T(8,128)(2,1)}, u32[]{:S(2)}, u32[]{:S(2)}) %collective-permute-start) | collective-permute-done | bytes 131104 | tf_op jit(solution)/shard_map/ppermute | solution.py:407
  226.4 1.7 copy-done.1
  228.2 17.6 %conv.1 = bf16[640,512]{1,0:T(8,128)(2,1)} custom-call(bf16[640,2048]{1,0:T(8,128)(2,1)S(1)} %copy-done.1, bf16[32,2048]{1,0:T(8,128)(2,1)} %collective-permute-done.carried_ref, f32[31,16,128]{2,1,0:T(8,128)S(1)} %slice.20.taps_ref, f32[1,2048]{1,0:T(1,128)S(1)} %bitcast.19, bf16[2048,512]{1,0:T(8,128)(2,1)S(1)} %copy-done.3), custom_call_target="tpu_custom_call" | custom-call | tf_op jit(solution)/shard_map/conv/pallas_call | solution.py:337
  246.6 2.6 %combine.1 = bf16[160,2048]{1,0:T(8,128)(2,1)} custom-call(bf16[32,160,128]{2,1,0:T(8,128)(2,1)S(1)} %all-to-all-done.1.refs_0_, s32[160,2]{1,0:T(8,128)S(1)} %bitcast.17, f32[160,2]{1,0:T(8,128)S(1)} %copy-done.4, f32[1,2048]{1,0:T(1,128)S(1)} %bitcast.20), custom_call_target="tpu_custom_call" | custom-call | tf_op jit(solution)/shard_map/combine/pallas_call | solution.py:276
  (62 shorter events, 9.3 us)
Async XLA Ops:
  6.3 25.6 %copy-start.9 = (bf16[1,256,2048]{2,1,0:T(8,128)(2,1)S(1)}, bf16[1,256,2048]{2,1,0:T(8,128)(2,1)}, u32[]{:S(2)}) copy-start(bf16[1,256,2048]{2,1,0:T(8,128)(2,1)} %param.22) | copy-start | bytes 3145732
  6.3 134.6 %all-to-all-start = ((bf16[32,160,128]{2,1,0:T(8,128)(2,1)}), bf16[32,160,128]{2,1,0:T(8,128)(2,1)S(1)}, u32[]{:S(2)}, u32[]{:S(2)}) async-start(bf16[32,160,128]{2,1,0:T(8,128)(2,1)} %get-tuple-element.4), calls=%async_computation | async-start | bytes 2621440 | tf_op jit(solution)/shard_map/all_to_all | solution.py:399
  32.0 14.6 %collective-permute-start.3 = (bf16[128,2048]{1,0:T(8,128)(2,1)S(1)}, bf16[128,2048]{1,0:T(8,128)(2,1)S(1)}, u32[]{:S(2)}, u32[]{:S(2)}) collective-permute-start(bf16[128,2048]{1,0:T(8,128)(2,1)S(1)} %get-tuple-element.7), channel_id=1, source_target_pairs={{0,1},{1,2},{2,3},{3,0},{4,5},{5,6},{6,7},{7,4},{8,9},{9,10},{10,1... | collective-permute-start | bytes 1572872 | tf_op jit(solution)/shard_map/ppermute | solution.py:392
  33.5 50.3 %collective-permute-start.6 = (bf16[2048,256]{1,0:T(8,128)(2,1)S(1)}, bf16[2048,256]{1,0:T(8,128)(2,1)S(1)}, u32[]{:S(2)}, u32[]{:S(2)}) collective-permute-start(bf16[2048,256]{1,0:T(8,128)(2,1)S(1)} %bitcast.26), channel_id=1, source_target_pairs={{0,3},{1,0},{2,1},{3,2},{4,7},{5,4},{6,5},{7,6},{8,11},{9,8},{10,9... | collective-permute-start | bytes 3145736 | tf_op jit(solution)/shard_map/ppermute | solution.py:392
  36.0 47.9 %collective-permute-start.1 = (bf16[2048,256]{1,0:T(8,128)(2,1)S(1)}, bf16[2048,256]{1,0:T(8,128)(2,1)S(1)}, u32[]{:S(2)}, u32[]{:S(2)}) collective-permute-start(bf16[2048,256]{1,0:T(8,128)(2,1)S(1)} %bitcast.23), channel_id=1, source_target_pairs={{0,1},{1,2},{2,3},{3,0},{4,5},{5,6},{6,7},{7,4},{8,9},{9,10},{10,1... | collective-permute-start | bytes 3145736 | tf_op jit(solution)/shard_map/ppermute | solution.py:392
  36.0 33.0 %collective-permute-start.8 = (bf16[128,2048]{1,0:T(8,128)(2,1)S(1)}, bf16[128,2048]{1,0:T(8,128)(2,1)S(1)}, u32[]{:S(2)}, u32[]{:S(2)}) collective-permute-start(bf16[128,2048]{1,0:T(8,128)(2,1)S(1)} %get-tuple-element.6), channel_id=1, source_target_pairs={{0,3},{1,0},{2,1},{3,2},{4,7},{5,4},{6,5},{7,6},{8,11},{9,8},{10,9... | collective-permute-start | bytes 1572872 | tf_op jit(solution)/shard_map/ppermute | solution.py:392
  38.7 41.6 %collective-permute-start.4 = (bf16[128,2048]{1,0:T(8,128)(2,1)S(1)}, bf16[128,2048]{1,0:T(8,128)(2,1)S(1)}, u32[]{:S(2)}, u32[]{:S(2)}) collective-permute-start(bf16[128,2048]{1,0:T(8,128)(2,1)S(1)} %get-tuple-element.6), channel_id=1, source_target_pairs={{0,1},{1,2},{2,3},{3,0},{4,5},{5,6},{6,7},{7,4},{8,9},{9,10},{10,1... | collective-permute-start | bytes 1572872 | tf_op jit(solution)/shard_map/ppermute | solution.py:392
  46.6 91.8 %copy-start.17 = (bf16[128,2048]{1,0:T(8,128)(2,1)}, bf16[128,2048]{1,0:T(8,128)(2,1)S(1)}, u32[]{:S(2)}) copy-start(bf16[128,2048]{1,0:T(8,128)(2,1)S(1)} %collective-permute-done.3.refs_6_) | copy-start | bytes 1572868
  46.6 34.5 %collective-permute-start.7 = (bf16[128,2048]{1,0:T(8,128)(2,1)S(1)}, bf16[128,2048]{1,0:T(8,128)(2,1)}, u32[]{:S(2)}, u32[]{:S(2)}) collective-permute-start(bf16[128,2048]{1,0:T(8,128)(2,1)S(1)} %get-tuple-element.7), channel_id=1, source_target_pairs={{0,3},{1,0},{2,1},{3,2},{4,7},{5,4},{6,5},{7,6},{8,11},{9,8},{10,9... | collective-permute-start | bytes 1572872 | tf_op jit(solution)/shard_map/ppermute | solution.py:392
  69.1 69.3 %copy-start.18 = (bf16[128,2048]{1,0:T(8,128)(2,1)}, bf16[128,2048]{1,0:T(8,128)(2,1)S(1)}, u32[]{:S(2)}) copy-start(bf16[128,2048]{1,0:T(8,128)(2,1)S(1)} %collective-permute-done.8.refs_11_) | copy-start | bytes 1572868
  69.1 69.3 %collective-permute-start.2 = (bf16[2048,256]{1,0:T(8,128)(2,1)S(1)}, bf16[2048,256]{1,0:T(8,128)(2,1)S(1)}, u32[]{:S(2)}, u32[]{:S(2)}) collective-permute-start(bf16[2048,256]{1,0:T(8,128)(2,1)S(1)} %bitcast.27), channel_id=1, source_target_pairs={{0,1},{1,2},{2,3},{3,0},{4,5},{5,6},{6,7},{7,4},{8,9},{9,10},{10,1... | collective-permute-start | bytes 3145736 | tf_op jit(solution)/shard_map/ppermute | solution.py:392
  80.3 33.7 %collective-permute-start.11 = (bf16[128,2048]{1,0:T(8,128)(2,1)S(1)}, bf16[128,2048]{1,0:T(8,128)(2,1)S(1)}, u32[]{:S(2)}, u32[]{:S(2)}) collective-permute-start(bf16[128,2048]{1,0:T(8,128)(2,1)S(1)} %collective-permute-done.3.refs_6_), channel_id=1, source_target_pairs={{0,1},{1,2},{2,3},{3,0},{4,5},{5,6},{6,7},{7,4},{8,9},{9,10},{10,1... | collective-permute-start | bytes 1572872 | tf_op jit(solution)/shard_map/ppermute | solution.py:392
  81.1 57.2 %collective-permute-start.5 = (bf16[2048,256]{1,0:T(8,128)(2,1)S(1)}, bf16[2048,256]{1,0:T(8,128)(2,1)S(1)}, u32[]{:S(2)}, u32[]{:S(2)}) collective-permute-start(bf16[2048,256]{1,0:T(8,128)(2,1)S(1)} %bitcast.24), channel_id=1, source_target_pairs={{0,3},{1,0},{2,1},{3,2},{4,7},{5,4},{6,5},{7,6},{8,11},{9,8},{10,9... | collective-permute-start | bytes 3145736 | tf_op jit(solution)/shard_map/ppermute | solution.py:392
  83.8 57.1 %copy-start.12 = (bf16[2048,256]{1,0:T(8,128)(2,1)}, bf16[2048,256]{1,0:T(8,128)(2,1)S(1)}, u32[]{:S(2)}) copy-start(bf16[2048,256]{1,0:T(8,128)(2,1)S(1)} %collective-permute-done.6.refs_9_) | copy-start | bytes 3145732
  83.8 54.5 %collective-permute-start.10 = (bf16[2048,256]{1,0:T(8,128)(2,1)S(1)}, bf16[2048,256]{1,0:T(8,128)(2,1)S(1)}, u32[]{:S(2)}, u32[]{:S(2)}) collective-permute-start(bf16[2048,256]{1,0:T(8,128)(2,1)S(1)} %collective-permute-done.6.refs_9_), channel_id=1, source_target_pairs={{0,3},{1,0},{2,1},{3,2},{4,7},{5,4},{6,5},{7,6},{8,11},{9,8},{10,9... | collective-permute-start | bytes 3145736 | tf_op jit(solution)/shard_map/ppermute | solution.py:392
  84.0 54.4 %copy-start.13 = (bf16[2048,256]{1,0:T(8,128)(2,1)}, bf16[2048,256]{1,0:T(8,128)(2,1)S(1)}, u32[]{:S(2)}) copy-start(bf16[2048,256]{1,0:T(8,128)(2,1)S(1)} %collective-permute-done.1.refs_4_) | copy-start | bytes 3145732
  84.0 56.9 %collective-permute-start.9 = (bf16[2048,256]{1,0:T(8,128)(2,1)S(1)}, bf16[2048,256]{1,0:T(8,128)(2,1)}, u32[]{:S(2)}, u32[]{:S(2)}) collective-permute-start(bf16[2048,256]{1,0:T(8,128)(2,1)S(1)} %collective-permute-done.1.refs_4_), channel_id=1, source_target_pairs={{0,1},{1,2},{2,3},{3,0},{4,5},{5,6},{6,7},{7,4},{8,9},{9,10},{10,1... | collective-permute-start | bytes 3145736 | tf_op jit(solution)/shard_map/ppermute | solution.py:392
  114.0 24.4 %copy-start.20 = (bf16[128,2048]{1,0:T(8,128)(2,1)}, bf16[128,2048]{1,0:T(8,128)(2,1)S(1)}, u32[]{:S(2)}) copy-start(bf16[128,2048]{1,0:T(8,128)(2,1)S(1)} %collective-permute-done.11.refs_14_) | copy-start | bytes 1572868
  114.0 24.3 %collective-permute-start.12 = (bf16[128,2048]{1,0:T(8,128)(2,1)S(1)}, bf16[128,2048]{1,0:T(8,128)(2,1)S(1)}, u32[]{:S(2)}, u32[]{:S(2)}) collective-permute-start(bf16[128,2048]{1,0:T(8,128)(2,1)S(1)} %collective-permute-done.8.refs_11_), channel_id=1, source_target_pairs={{0,3},{1,0},{2,1},{3,2},{4,7},{5,4},{6,5},{7,6},{8,11},{9,8},{10,9... | collective-permute-start | bytes 1572872 | tf_op jit(solution)/shard_map/ppermute | solution.py:392
  156.0 70.5 %copy-start.3 = (bf16[2048,512]{1,0:T(8,128)(2,1)S(1)}, bf16[2048,512]{1,0:T(8,128)(2,1)}, u32[]{:S(2)}) copy-start(bf16[2048,512]{1,0:T(8,128)(2,1)} %weight_ref.1) | copy-start | bytes 6291460
  156.0 89.8 %all-to-all-start.1 = ((bf16[32,160,128]{2,1,0:T(8,128)(2,1)}), bf16[32,160,128]{2,1,0:T(8,128)(2,1)S(1)}, u32[]{:S(2)}, u32[]{:S(2)}) async-start(bf16[32,160,128]{2,1,0:T(8,128)(2,1)} %experts.1), calls=%async_computation.1 | async-start | bytes 2621440 | tf_op jit(solution)/shard_map/all_to_all | solution.py:421
  171.0 55.4 %copy-start.6 = (f32[2048]{0:T(1024)S(1)}, f32[2048]{0:T(1024)}, u32[]{:S(2)}) copy-start(f32[2048]{0:T(1024)} %param.14) | copy-start | bytes 24580
  172.6 53.8 %collective-permute-start = (bf16[32,2048]{1,0:T(8,128)(2,1)}, bf16[32,2048]{1,0:T(8,128)(2,1)}, u32[]{:S(2)}, u32[]{:S(2)}) collective-permute-start(bf16[32,2048]{1,0:T(8,128)(2,1)} %slice.15), channel_id=1, source_target_pairs={{0,4},{4,8},{8,12},{12,16},{16,20},{20,24},{24,28},{28,32},{32,36}... | collective-permute-start | bytes 393224 | tf_op jit(solution)/shard_map/ppermute | solution.py:407
  228.2 17.6 %copy-start.7 = (f32[2048]{0:T(1024)S(1)}, f32[2048]{0:T(1024)}, u32[]{:S(2)}) copy-start(f32[2048]{0:T(1024)} %param.23) | copy-start | bytes 24580
  (13 other events, 17.8 us)

commit v2 on v1

--- a/solution.py
+++ b/solution.py
@@ -44,15 +44,17 @@
         out_ref[:, base + j * 8 : base + (j + 2) * 8, :] = jnp.concatenate(pair, axis=1).astype(BF16)
 
 
-def dispatch_kernel(own_ref, rows_ref, gain_ref, ids_ref, out_ref, target_ref, *, experts, capacity):
-    del own_ref
+def dispatch_kernel(
+    own_ref, all_ref, gain_ref, ids_ref, out_ref, target_ref, rows_ref, signal, *, experts, capacity
+):
     tokens, width = rows_ref.shape
+    copy = pltpu.make_async_copy(
+        all_ref.at[pl.ds(pl.multiple_of(own_ref[0] * tokens, 16), tokens), :], rows_ref, signal
+    )
+    copy.start()
     blocks = width // LANES
     head, tail = split_rows(capacity)
     per = 8 // tail
-    rows = rows_ref[...].astype(F32)
-    mean_square = jnp.mean(rows * rows, axis=-1, keepdims=True)
-    normed = (rows * lax.rsqrt(mean_square + EPSILON) * gain_ref[...]).astype(BF16)
     ids = ids_ref[...]
     onehot = [
         (ids[k : k + 1, :] == lax.broadcasted_iota(jnp.int32, (experts, tokens), 0)).astype(F32)
@@ -77,6 +79,10 @@
             picks[q] = picks[q] + selection(in_tail[k : k + 1], -q * tail, experts * 8, 0).astype(F32)
     pick = pick.astype(BF16)
     picks = jnp.concatenate(picks, axis=1).astype(BF16)
+    copy.wait()
+    rows = rows_ref[...].astype(F32)
+    mean_square = jnp.mean(rows * rows, axis=-1, keepdims=True)
+    normed = (rows * lax.rsqrt(mean_square + EPSILON) * gain_ref[...]).astype(BF16)
 
     def tail_of(j):
         stack = [col(normed, per * j + q) for q in range(per)]
@@ -90,41 +96,37 @@
 def dispatch(own, rows, gain, ids, experts, capacity):
     tokens = ids.shape[1]
     width = rows.shape[1]
-    grid_spec = pltpu.PrefetchScalarGridSpec(
-        num_scalar_prefetch=1,
-        grid=(1,),
-        in_specs=[
-            pl.BlockSpec((tokens, width), lambda i, own: (own[0], 0)),
-            pl.BlockSpec((1, width), lambda i, own: (0, 0)),
-            pl.BlockSpec((2, tokens), lambda i, own: (0, 0)),
-        ],
-        out_specs=[
-            pl.BlockSpec((experts, capacity * width // LANES, LANES), lambda i, own: (0, 0, 0)),
-            pl.BlockSpec((2, tokens), lambda i, own: (0, 0)),
-        ],
-    )
 
     def kernel(*refs):
         dispatch_kernel(*refs, experts=experts, capacity=capacity)
 
     return pl.pallas_call(
         kernel,
-        grid_spec=grid_spec,
+        in_specs=[
+            pl.BlockSpec(memory_space=pltpu.SMEM),
+            pl.BlockSpec(memory_space=pltpu.HBM),
+            whole(),
+            whole(),
+        ],
+        out_specs=[whole(), whole()],
+        scratch_shapes=[pltpu.VMEM((tokens, width), BF16), pltpu.SemaphoreType.DMA],
         out_shape=[
             jax.ShapeDtypeStruct((experts, capacity * width // LANES, LANES), BF16),
             jax.ShapeDtypeStruct((2, tokens), jnp.int32),
         ],
         compiler_params=pltpu.CompilerParams(vmem_limit_bytes=24 << 20),
         name="dispatch",
-    )(own, rows, gain, ids)
+    )(own, pltpu.with_memory_space_constraint(rows, pltpu.HBM), gain, ids)
 
 
 def expert_kernel(*refs, sources, peers, capacity, blocks):
-    count = len(refs) // 2 - 2
-    message_ref, out_ref = refs[0], refs[count + 1]
-    remote = refs[1 : count + 1]
-    rows_ref, hidden_ref, signals = refs[count + 2], refs[count + 3], refs[-1]
-    weights = refs[count + 4 : -1]
+    odd_ref, message_ref = refs[0], refs[1]
+    count = (len(refs) - 6) // 2
+    remote = refs[2 : count + 2]
+    out_ref, rows_ref, hidden_ref = refs[count + 2 : count + 5]
+    weights = refs[count + 5 : -1]
+    signals = refs[-1]
+    odd = odd_ref[0] == 1
     copies = [
         pltpu.make_async_copy(far, near, signals.at[i])
         for i, (far, near) in enumerate(zip(remote, weights))
@@ -155,7 +157,7 @@
                 rows_ref[heads:, c * LANES : (c + 1) * LANES] = dot(gathers[q], part).astype(BF16)
     at = 0
     downs = []
-    for gates, ups, down_parts in sources:
+    for gates, ups, down_parts, swapped in sources:
         rows = rows_ref[...]
         values = []
         for group in (gates, ups):
@@ -169,6 +171,11 @@
                 begin += size
             values.append(value)
         gate_value, up_value = values
+        if swapped:
+            gate_value, up_value = (
+                jnp.where(odd, up_value, gate_value),
+                jnp.where(odd, gate_value, up_value),
+            )
         hidden = gate_value / (1.0 + jnp.exp(-gate_value)) * up_value
         hidden_ref[:, at : at + hidden.shape[1]] = hidden.astype(BF16)
         for d in down_parts:
@@ -206,7 +213,7 @@
         out_ref[:, at_row : at_row + 16, :] = jnp.concatenate(pair, axis=1).astype(BF16)
 
 
-def experts_apply(message, weights, sources, capacity):
+def experts_apply(odd, message, weights, sources, capacity):
     peers, lines, _ = message.shape
     blocks = lines // capacity
     units = sum(weights[d].shape[0] for s in sources for d in s[2])
@@ -216,7 +223,8 @@
 
     return pl.pallas_call(
         kernel,
-        in_specs=[whole()] + [pl.BlockSpec(memory_space=pltpu.HBM)] * len(weights),
+        in_specs=[pl.BlockSpec(memory_space=pltpu.SMEM), whole()]
+        + [pl.BlockSpec(memory_space=pltpu.HBM)] * len(weights),
         out_specs=whole(),
         out_shape=jax.ShapeDtypeStruct(message.shape, BF16),
         scratch_shapes=[
@@ -225,9 +233,9 @@
             *(pltpu.VMEM(w.shape, BF16) for w in weights),
             pltpu.SemaphoreType.DMA((len(weights),)),
         ],
-        compiler_params=pltpu.CompilerParams(vmem_limit_bytes=60 << 20),
+        compiler_params=pltpu.CompilerParams(vmem_limit_bytes=40 << 20),
         name="experts",
-    )(message, *weights)
+    )(odd, message, *(pltpu.with_memory_space_constraint(w, pltpu.HBM) for w in weights))
 
 
 def combine_kernel(message_ref, target_ref, weight_ref, gain_ref, out_ref, mixed_ref, *, capacity):
@@ -382,42 +390,53 @@
     capacity = 2 * tokens // ep_count
     own = lax.axis_index("tp").astype(jnp.int32)
 
+    odd = (lax.axis_index("grp") % 2).astype(jnp.int32)
+
     right = [(i, (i + 1) % quarters) for i in range(quarters)]
     left = [(i, (i - 1) % quarters) for i in range(quarters)]
+    across = [(i, i ^ 1) for i in range(lax.axis_size("grp"))]
     gate, up, down = gate_weight[0], up_weight[0], down_weight[0]
-    half = down.shape[0] // 2
-    down_a, down_b = down[:half], down[half:]
+    rows, units = gate.shape[0] // 2, down.shape[0] // 2
+    down_a, down_b = down[:units], down[units:]
+    mine_a = jnp.where(odd == 1, up[:rows], gate[:rows])
+    mine_b = jnp.where(odd == 1, up[rows:], gate[rows:])
 
     def send(array, pairs):
         return lax.ppermute(array, "tp", pairs)
 
-    gate_r, up_l = send(gate, right), send(up, left)
+    def swap(array):
+        return lax.ppermute(array, "grp", across)
+
+    mine_a_r, mine_b_l = send(mine_a, right), send(mine_b, left)
     own_ids = lax.dynamic_slice_in_dim(expert_ids, own * tokens, tokens, 0).T
     message, target = dispatch(
         own.reshape(1), moe_input, moe_gain.reshape(1, width), own_ids, ep_count, capacity
     )
     arrived = lax.all_to_all(message, EP, 0, 0, tiled=True)
-    down_r, down_l = send(down_a, right), send(down_b, left)
-    up_r, gate_l = send(up, right), send(gate, left)
-    rest_r, rest_l = send(down_b, right), send(down_a, left)
-    gate_far, up_far = send(gate_r, right), send(up_l, left)
-    down_far, rest_far = send(down_r, right), send(down_l, left)
-
     pairs = [(i, i + 1) for i in range(ep_count - 1)]
     carried = lax.ppermute(conv_input[conv_input.shape[0] - HALO :], EP, pairs)
+    mine_b_r, mine_a_l = send(mine_b, right), send(mine_a, left)
+    mine_a_far, mine_b_far = send(mine_a_r, right), send(mine_b_l, left)
+    other_a_r, other_b_l = swap(mine_a_r), swap(mine_b_l)
+    down_a_r, down_b_l = send(down_a, right), send(down_b, left)
+    other_b_r, other_a_l = swap(mine_b_r), swap(mine_a_l)
+    down_b_r, down_a_l = send(down_b, right), send(down_a, left)
+    other_a_far, other_b_far = swap(mine_a_far), swap(mine_b_far)
+    down_a_far, down_b_far = send(down_a_r, right), send(down_b_l, left)
+
     conv_out = conv_module(conv_input, carried, conv_taps, conv_gain.reshape(1, width), conv_weight)
 
     weights = [gate, up, down]
-    sources = [((0,), (1,), (2,))]
+    sources = [((0,), (1,), (2,), False)]
     for arrays in (
-        (gate_r, up_r, down_r, rest_r),
-        (gate_l, up_l, rest_l, down_l),
-        (gate_far, up_far, down_far, rest_far),
+        (mine_a_r, mine_b_r, other_a_r, other_b_r, down_a_r, down_b_r),
+        (mine_a_l, mine_b_l, other_a_l, other_b_l, down_a_l, down_b_l),
+        (mine_a_far, mine_b_far, other_a_far, other_b_far, down_a_far, down_b_far),
     ):
         at = len(weights)
         weights.extend(arrays)
-        sources.append(((at,), (at + 1,), (at + 2, at + 3)))
-    results = experts_apply(arrived, weights, tuple(sources), capacity)
+        sources.append(((at, at + 1), (at + 2, at + 3), (at + 4, at + 5), True))
+    results = experts_apply(odd.reshape(1), arrived, weights, tuple(sources), capacity)
     returned = lax.all_to_all(results, EP, 0, 0, tiled=True)
     own_weights = lax.dynamic_slice_in_dim(route_weights, own * tokens, tokens, 0)
     moe_out = combine(returned, target.T, own_weights, post_gain.reshape(1, width), capacity)

time: 250 us -> 245 us (0.980)
  waiting for transfers between devices: 139 us -> 132 us
  starting transfers between devices: 58.2 us -> 64.9 us
  local copies, waits for them, and re-layouts: 14.5 us -> 9.3 us
    ppermute x12, waiting for transfers between devices: 91.5 us -> 44.4 us  [send(): return lax.ppermute(array, 'tp', pairs)]
    ppermute x0 -> x6, waiting for transfers between devices: none -> 40.5 us  [swap(): return lax.ppermute(array, 'grp', across)]
    ppermute x0 -> x6, starting transfers between devices: none -> 7.62 us  [swap(): return lax.ppermute(array, 'grp', across)]
    unnamed x46 -> x56, local copies, waits for them, and re-layouts: 11.9 us -> 6.69 us
  transfers between devices with their start and end apart: 15 -> 21, of which waited for: 6 -> 10; matrix products, arithmetic and copies ran while one was open for 2% -> 2% of each run, Pallas kernels for 7% -> 7%
where the time goes in v2:
time: 245 us
  waiting for transfers between devices  132 us (54%)
  starting transfers between devices  64.9 us (26%)
  Pallas kernels  36.8 us (15%)
  local copies, waits for them, and re-layouts  9.3 us (4%)
    ppermute x1, waiting for transfers between devices, run(): carried = lax.ppermute(conv_input[conv_input.shape[0] - HALO:], EP, pairs)  47.6 us
    ppermute x12, waiting for transfers between devices, send(): return lax.ppermute(array, 'tp', pairs)  44.4 us
    ppermute x6, waiting for transfers between devices, swap(): return lax.ppermute(array, 'grp', across)  40.5 us
    all_to_all x1, starting transfers between devices, run(): arrived = lax.all_to_all(message, EP, 0, 0, tiled=True)  25.6 us
    pallas_call x1, Pallas kernels, conv_module(): pl.pallas_call(conv_kernel, grid=(count // block,), in_specs=[pl.BlockSpe...  17.6 us
    all_to_all x1, starting transfers between devices, run(): returned = lax.all_to_all(results, EP, 0, 0, tiled=True)  14.7 us
    ppermute x12, starting transfers between devices, send(): return lax.ppermute(array, 'tp', pairs)  13.4 us
    pallas_call x1, Pallas kernels, experts_apply(): pl.pallas_call(kernel, in_specs=[pl.BlockSpec(memory_space=pltpu.SMEM), w...  13.1 us
  transfers between devices with their start and end apart: 21, of which 10 were waited for; matrix products, arithmetic and copies ran while one was open for 2% of the time, Pallas kernels for 7%

profile of v2, /device:TPU:33, one launch (start us, length us, event | category | flops | bytes accessed | tf_op | source)
XLA Modules:
  0.0 244.5 jit_solution(17674212170591419397)
XLA Ops:
  2.1 3.4 %dispatch.1 = (bf16[32,160,128]{2,1,0:T(8,128)(2,1)}, s32[2,160]{1,0:T(2,128)S(1)}) custom-call(s32[1]{0:T(128)} %bitcast.2.refs_0_, bf16[640,2048]{1,0:T(8,128)(2,1)} %refs_1_.1, f32[1,2048]{1,0:T(1,128)S(1)} %bitcast.23, s32[2,160]{1,0:T(2,128)S(1)} %dynamic-slice_bitcast_fusion.refs_3_), custom_call_target="tpu_custom_call" | custom-call | tf_op jit(solution)/shard_map/dispatch/pallas_call | solution.py:103
  5.6 25.6 %all-to-all-start = ((bf16[32,160,128]{2,1,0:T(8,128)(2,1)}), bf16[32,160,128]{2,1,0:T(8,128)(2,1)S(1)}, u32[]{:S(2)}, u32[]{:S(2)}) async-start(bf16[32,160,128]{2,1,0:T(8,128)(2,1)} %get-tuple-element.4), calls=%async_computation | async-start | bytes 2621440 | tf_op jit(solution)/shard_map/all_to_all | solution.py:415
  32.8 1.7 collective-permute-start.8
  34.5 2.7 %collective-permute-start.7 = (bf16[1024,256]{1,0:T(8,128)(2,1)S(1)}, bf16[1024,256]{1,0:T(8,128)(2,1)S(1)}, u32[]{:S(2)}, u32[]{:S(2)}) collective-permute-start(bf16[1024,256]{1,0:T(8,128)(2,1)S(1)} %get-tuple-element.7), channel_id=1, source_target_pairs={{0,3},{1,0},{2,1},{3,2},{4,7},{5,4},{6,5},{7,6},{8,11},{9,8},{10,9... | collective-permute-start | bytes 1572872 | tf_op jit(solution)/shard_map/ppermute | solution.py:405
  37.4 8.5 %collective-permute-done.1.refs_5_ = bf16[1024,256]{1,0:T(8,128)(2,1)S(1)} collective-permute-done((bf16[1024,256]{1,0:T(8,128)(2,1)S(1)}, bf16[1024,256]{1,0:T(8,128)(2,1)S(1)}, u32[]{:S(2)}, u32[]{:S(2)}) %collective-permute-start.1) | collective-permute-done | bytes 524320 | tf_op jit(solution)/shard_map/ppermute | solution.py:405
  48.5 8.7 %collective-permute-done.2.refs_6_ = bf16[1024,256]{1,0:T(8,128)(2,1)S(1)} collective-permute-done((bf16[1024,256]{1,0:T(8,128)(2,1)S(1)}, bf16[1024,256]{1,0:T(8,128)(2,1)S(1)}, u32[]{:S(2)}, u32[]{:S(2)}) %collective-permute-start.2) | collective-permute-done | bytes 524320 | tf_op jit(solution)/shard_map/ppermute | solution.py:405
  58.2 10.2 %collective-permute-done.5.refs_9_ = bf16[128,2048]{1,0:T(8,128)(2,1)S(1)} collective-permute-done((bf16[128,2048]{1,0:T(8,128)(2,1)S(1)}, bf16[128,2048]{1,0:T(8,128)(2,1)S(1)}, u32[]{:S(2)}, u32[]{:S(2)}) %collective-permute-start.5) | collective-permute-done | bytes 524320 | tf_op jit(solution)/shard_map/ppermute | solution.py:405
  69.6 1.8 collective-permute-start.10
  71.4 7.6 %collective-permute-done.11.refs_15_ = bf16[128,2048]{1,0:T(8,128)(2,1)S(1)} collective-permute-done((bf16[128,2048]{1,0:T(8,128)(2,1)S(1)}, bf16[128,2048]{1,0:T(8,128)(2,1)S(1)}, u32[]{:S(2)}, u32[]{:S(2)}) %collective-permute-start.11) | collective-permute-done | bytes 524320 | tf_op jit(solution)/shard_map/ppermute | solution.py:405
  79.0 1.8 collective-permute-start.3
  81.5 9.4 %collective-permute-done.13.refs_17_ = bf16[1024,256]{1,0:T(8,128)(2,1)S(1)} collective-permute-done((bf16[1024,256]{1,0:T(8,128)(2,1)S(1)}, bf16[1024,256]{1,0:T(8,128)(2,1)S(1)}, u32[]{:S(2)}, u32[]{:S(2)}) %collective-permute-start.13) | collective-permute-done | bytes 524320 | tf_op jit(solution)/shard_map/ppermute | solution.py:405
  90.8 1.8 collective-permute-start.9
  92.7 2.7 %collective-permute-start.18 = (bf16[128,2048]{1,0:T(8,128)(2,1)S(1)}, bf16[128,2048]{1,0:T(8,128)(2,1)S(1)}, u32[]{:S(2)}, u32[]{:S(2)}) collective-permute-start(bf16[128,2048]{1,0:T(8,128)(2,1)S(1)} %collective-permute-done.12.refs_16_), channel_id=1, source_target_pairs={{0,3},{1,0},{2,1},{3,2},{4,7},{5,4},{6,5},{7,6},{8,11},{9,8},{10,9... | collective-permute-start | bytes 1572872 | tf_op jit(solution)/shard_map/ppermute | solution.py:405
  95.5 9.1 %collective-permute-done.4.refs_8_ = bf16[1024,256]{1,0:T(8,128)(2,1)S(1)} collective-permute-done((bf16[1024,256]{1,0:T(8,128)(2,1)S(1)}, bf16[1024,256]{1,0:T(8,128)(2,1)S(1)}, u32[]{:S(2)}, u32[]{:S(2)}) %collective-permute-start.4) | collective-permute-done | bytes 524320 | tf_op jit(solution)/shard_map/ppermute | solution.py:408
  105.9 9.9 %collective-permute-done.9.refs_13_ = bf16[1024,256]{1,0:T(8,128)(2,1)S(1)} collective-permute-done((bf16[1024,256]{1,0:T(8,128)(2,1)S(1)}, bf16[1024,256]{1,0:T(8,128)(2,1)S(1)}, u32[]{:S(2)}, u32[]{:S(2)}) %collective-permute-start.9) | collective-permute-done | bytes 524320 | tf_op jit(solution)/shard_map/ppermute | solution.py:408
  115.8 11.2 %collective-permute-done.15.refs_19_ = bf16[1024,256]{1,0:T(8,128)(2,1)S(1)} collective-permute-done((bf16[1024,256]{1,0:T(8,128)(2,1)S(1)}, bf16[1024,256]{1,0:T(8,128)(2,1)S(1)}, u32[]{:S(2)}, u32[]{:S(2)}) %collective-permute-start.15) | collective-permute-done | bytes 524320 | tf_op jit(solution)/shard_map/ppermute | solution.py:408
  128.0 10.4 %collective-permute-done.16.refs_20_ = bf16[1024,256]{1,0:T(8,128)(2,1)} collective-permute-done((bf16[1024,256]{1,0:T(8,128)(2,1)S(1)}, bf16[1024,256]{1,0:T(8,128)(2,1)}, u32[]{:S(2)}, u32[]{:S(2)}) %collective-permute-start.16) | collective-permute-done | bytes 524320 | tf_op jit(solution)/shard_map/ppermute | solution.py:408
  138.4 13.1 %experts.1 = bf16[32,160,128]{2,1,0:T(8,128)(2,1)} custom-call(s32[1]{0:T(128)} %bitcast.1.refs_0_, bf16[32,160,128]{2,1,0:T(8,128)(2,1)S(1)} %all-to-all-done.refs_1_, bf16[2048,256]{1,0:T(8,128)(2,1)} %bitcast.26, bf16[2048,256]{1,0:T(8,128)(2,1)} %bitcast.27, bf16[256,2048]{1,0:T(8,128)(2,1)} %bitcast.28, bf16[1024,256]{1,0:T(8,128)(2,1)} %copy-done.10, ...), custom_call_target="tpu_custom_call" | custom-call | tf_op jit(solution)/shard_map/experts/pallas_call | solution.py:224
  151.6 14.7 %all-to-all-start.1 = ((bf16[32,160,128]{2,1,0:T(8,128)(2,1)}), bf16[32,160,128]{2,1,0:T(8,128)(2,1)S(1)}, u32[]{:S(2)}, u32[]{:S(2)}) async-start(bf16[32,160,128]{2,1,0:T(8,128)(2,1)} %experts.1), calls=%async_computation.1 | async-start | bytes 2621440 | tf_op jit(solution)/shard_map/all_to_all | solution.py:440
  167.9 3.6 %collective-permute-start = (bf16[32,2048]{1,0:T(8,128)(2,1)}, bf16[32,2048]{1,0:T(8,128)(2,1)}, u32[]{:S(2)}, u32[]{:S(2)}) collective-permute-start(bf16[32,2048]{1,0:T(8,128)(2,1)} %slice.31), channel_id=1, source_target_pairs={{0,4},{4,8},{8,12},{12,16},{16,20},{20,24},{24,28},{28,32},{32,36}... | collective-permute-start | bytes 393224 | tf_op jit(solution)/shard_map/ppermute | solution.py:417
  174.1 47.6 %collective-permute-done.carried_ref = bf16[32,2048]{1,0:T(8,128)(2,1)} collective-permute-done((bf16[32,2048]{1,0:T(8,128)(2,1)}, bf16[32,2048]{1,0:T(8,128)(2,1)}, u32[]{:S(2)}, u32[]{:S(2)}) %collective-permute-start) | collective-permute-done | bytes 131104 | tf_op jit(solution)/shard_map/ppermute | solution.py:417
  221.7 1.7 copy-done.1
  223.4 17.6 %conv.1 = bf16[640,512]{1,0:T(8,128)(2,1)} custom-call(bf16[640,2048]{1,0:T(8,128)(2,1)S(1)} %copy-done.1, bf16[32,2048]{1,0:T(8,128)(2,1)} %collective-permute-done.carried_ref, f32[31,16,128]{2,1,0:T(8,128)S(1)} %slice.40.taps_ref, f32[1,2048]{1,0:T(1,128)S(1)} %bitcast.24, bf16[2048,512]{1,0:T(8,128)(2,1)S(1)} %copy-done.2), custom_call_target="tpu_custom_call" | custom-call | tf_op jit(solution)/shard_map/conv/pallas_call | solution.py:345
  241.9 2.6 %combine.1 = bf16[160,2048]{1,0:T(8,128)(2,1)} custom-call(bf16[32,160,128]{2,1,0:T(8,128)(2,1)S(1)} %all-to-all-done.1.refs_0_, s32[160,2]{1,0:T(8,128)S(1)} %bitcast.22, f32[160,2]{1,0:T(8,128)S(1)} %copy-done.3, f32[1,2048]{1,0:T(1,128)S(1)} %bitcast.25), custom_call_target="tpu_custom_call" | custom-call | tf_op jit(solution)/shard_map/combine/pallas_call | solution.py:284
  (85 shorter events, 16.2 us)
Async XLA Ops:
  5.6 132.8 %all-to-all-start = ((bf16[32,160,128]{2,1,0:T(8,128)(2,1)}), bf16[32,160,128]{2,1,0:T(8,128)(2,1)S(1)}, u32[]{:S(2)}, u32[]{:S(2)}) async-start(bf16[32,160,128]{2,1,0:T(8,128)(2,1)} %get-tuple-element.4), calls=%async_computation | async-start | bytes 2621440 | tf_op jit(solution)/shard_map/all_to_all | solution.py:415
  31.3 14.6 %collective-permute-start.1 = (bf16[1024,256]{1,0:T(8,128)(2,1)S(1)}, bf16[1024,256]{1,0:T(8,128)(2,1)S(1)}, u32[]{:S(2)}, u32[]{:S(2)}) collective-permute-start(bf16[1024,256]{1,0:T(8,128)(2,1)S(1)} %get-tuple-element.7), channel_id=1, source_target_pairs={{0,1},{1,2},{2,3},{3,0},{4,5},{5,6},{6,7},{7,4},{8,9},{9,10},{10,1... | collective-permute-start | bytes 1572872 | tf_op jit(solution)/shard_map/ppermute | solution.py:405
  32.8 14.3 %collective-permute-start.8 = (bf16[1024,256]{1,0:T(8,128)(2,1)S(1)}, bf16[1024,256]{1,0:T(8,128)(2,1)S(1)}, u32[]{:S(2)}, u32[]{:S(2)}) collective-permute-start(bf16[1024,256]{1,0:T(8,128)(2,1)S(1)} %get-tuple-element.6), channel_id=1, source_target_pairs={{0,3},{1,0},{2,1},{3,2},{4,7},{5,4},{6,5},{7,6},{8,11},{9,8},{10,9... | collective-permute-start | bytes 1572872 | tf_op jit(solution)/shard_map/ppermute | solution.py:405
  34.5 22.7 %collective-permute-start.2 = (bf16[1024,256]{1,0:T(8,128)(2,1)S(1)}, bf16[1024,256]{1,0:T(8,128)(2,1)S(1)}, u32[]{:S(2)}, u32[]{:S(2)}) collective-permute-start(bf16[1024,256]{1,0:T(8,128)(2,1)S(1)} %get-tuple-element.6), channel_id=1, source_target_pairs={{0,1},{1,2},{2,3},{3,0},{4,5},{5,6},{6,7},{7,4},{8,9},{9,10},{10,1... | collective-permute-start | bytes 1572872 | tf_op jit(solution)/shard_map/ppermute | solution.py:405
  34.5 22.7 %collective-permute-start.7 = (bf16[1024,256]{1,0:T(8,128)(2,1)S(1)}, bf16[1024,256]{1,0:T(8,128)(2,1)S(1)}, u32[]{:S(2)}, u32[]{:S(2)}) collective-permute-start(bf16[1024,256]{1,0:T(8,128)(2,1)S(1)} %get-tuple-element.7), channel_id=1, source_target_pairs={{0,3},{1,0},{2,1},{3,2},{4,7},{5,4},{6,5},{7,6},{8,11},{9,8},{10,9... | collective-permute-start | bytes 1572872 | tf_op jit(solution)/shard_map/ppermute | solution.py:405
  37.2 31.1 %collective-permute-start.5 = (bf16[128,2048]{1,0:T(8,128)(2,1)S(1)}, bf16[128,2048]{1,0:T(8,128)(2,1)S(1)}, u32[]{:S(2)}, u32[]{:S(2)}) collective-permute-start(bf16[128,2048]{1,0:T(8,128)(2,1)S(1)} %get-tuple-element.9), channel_id=1, source_target_pairs={{0,1},{1,2},{2,3},{3,0},{4,5},{5,6},{6,7},{7,4},{8,9},{9,10},{10,1... | collective-permute-start | bytes 1572872 | tf_op jit(solution)/shard_map/ppermute | solution.py:405
  45.9 92.5 %copy-start.10 = (bf16[1024,256]{1,0:T(8,128)(2,1)}, bf16[1024,256]{1,0:T(8,128)(2,1)S(1)}, u32[]{:S(2)}) copy-start(bf16[1024,256]{1,0:T(8,128)(2,1)S(1)} %collective-permute-done.1.refs_5_) | copy-start | bytes 1572868
  45.9 23.7 %collective-permute-start.12 = (bf16[128,2048]{1,0:T(8,128)(2,1)S(1)}, bf16[128,2048]{1,0:T(8,128)(2,1)S(1)}, u32[]{:S(2)}, u32[]{:S(2)}) collective-permute-start(bf16[128,2048]{1,0:T(8,128)(2,1)S(1)} %get-tuple-element.8), channel_id=1, source_target_pairs={{0,3},{1,0},{2,1},{3,2},{4,7},{5,4},{6,5},{7,6},{8,11},{9,8},{10,9... | collective-permute-start | bytes 1572872 | tf_op jit(solution)/shard_map/ppermute | solution.py:405
  47.1 91.3 %copy-start.11 = (bf16[1024,256]{1,0:T(8,128)(2,1)}, bf16[1024,256]{1,0:T(8,128)(2,1)S(1)}, u32[]{:S(2)}) copy-start(bf16[1024,256]{1,0:T(8,128)(2,1)S(1)} %collective-permute-done.8.refs_12_) | copy-start | bytes 1572868
  47.1 31.9 %collective-permute-start.11 = (bf16[128,2048]{1,0:T(8,128)(2,1)S(1)}, bf16[128,2048]{1,0:T(8,128)(2,1)S(1)}, u32[]{:S(2)}, u32[]{:S(2)}) collective-permute-start(bf16[128,2048]{1,0:T(8,128)(2,1)S(1)} %get-tuple-element.9), channel_id=1, source_target_pairs={{0,3},{1,0},{2,1},{3,2},{4,7},{5,4},{6,5},{7,6},{8,11},{9,8},{10,9... | collective-permute-start | bytes 1572872 | tf_op jit(solution)/shard_map/ppermute | solution.py:405
  57.1 81.3 %copy-start.12 = (bf16[1024,256]{1,0:T(8,128)(2,1)}, bf16[1024,256]{1,0:T(8,128)(2,1)S(1)}, u32[]{:S(2)}) copy-start(bf16[1024,256]{1,0:T(8,128)(2,1)S(1)} %collective-permute-done.2.refs_6_) | copy-start | bytes 1572868
  57.1 23.7 %collective-permute-start.6 = (bf16[128,2048]{1,0:T(8,128)(2,1)S(1)}, bf16[128,2048]{1,0:T(8,128)(2,1)S(1)}, u32[]{:S(2)}, u32[]{:S(2)}) collective-permute-start(bf16[128,2048]{1,0:T(8,128)(2,1)S(1)} %get-tuple-element.8), channel_id=1, source_target_pairs={{0,1},{1,2},{2,3},{3,0},{4,5},{5,6},{6,7},{7,4},{8,9},{9,10},{10,1... | collective-permute-start | bytes 1572872 | tf_op jit(solution)/shard_map/ppermute | solution.py:405
  57.2 33.7 %collective-permute-start.13 = (bf16[1024,256]{1,0:T(8,128)(2,1)S(1)}, bf16[1024,256]{1,0:T(8,128)(2,1)S(1)}, u32[]{:S(2)}, u32[]{:S(2)}) collective-permute-start(bf16[1024,256]{1,0:T(8,128)(2,1)S(1)} %collective-permute-done.1.refs_5_), channel_id=1, source_target_pairs={{0,1},{1,2},{2,3},{3,0},{4,5},{5,6},{6,7},{7,4},{8,9},{9,10},{10,1... | collective-permute-start | bytes 1572872 | tf_op jit(solution)/shard_map/ppermute | solution.py:405
  68.4 24.3 %collective-permute-start.14 = (bf16[1024,256]{1,0:T(8,128)(2,1)S(1)}, bf16[1024,256]{1,0:T(8,128)(2,1)S(1)}, u32[]{:S(2)}, u32[]{:S(2)}) collective-permute-start(bf16[1024,256]{1,0:T(8,128)(2,1)S(1)} %collective-permute-done.8.refs_12_), channel_id=1, source_target_pairs={{0,3},{1,0},{2,1},{3,2},{4,7},{5,4},{6,5},{7,6},{8,11},{9,8},{10,9... | collective-permute-start | bytes 1572872 | tf_op jit(solution)/shard_map/ppermute | solution.py:405
  69.6 23.1 %collective-permute-start.10 = (bf16[1024,256]{1,0:T(8,128)(2,1)S(1)}, bf16[1024,256]{1,0:T(8,128)(2,1)S(1)}, u32[]{:S(2)}, u32[]{:S(2)}) collective-permute-start(bf16[1024,256]{1,0:T(8,128)(2,1)S(1)} %collective-permute-done.8.refs_12_), channel_id=1, source_target_pairs={{0,128},{128,0},{1,129},{129,1},{2,130},{130,2},{3,131},{131,3},{4... | collective-permute-start | bytes 1572872 | tf_op jit(solution)/shard_map/ppermute | solution.py:408
  79.0 16.4 %collective-permute-start.3 = (bf16[1024,256]{1,0:T(8,128)(2,1)S(1)}, bf16[1024,256]{1,0:T(8,128)(2,1)S(1)}, u32[]{:S(2)}, u32[]{:S(2)}) collective-permute-start(bf16[1024,256]{1,0:T(8,128)(2,1)S(1)} %collective-permute-done.1.refs_5_), channel_id=1, source_target_pairs={{0,128},{128,0},{1,129},{129,1},{2,130},{130,2},{3,131},{131,3},{4... | collective-permute-start | bytes 1572872 | tf_op jit(solution)/shard_map/ppermute | solution.py:408
  80.9 23.7 %collective-permute-start.4 = (bf16[1024,256]{1,0:T(8,128)(2,1)S(1)}, bf16[1024,256]{1,0:T(8,128)(2,1)S(1)}, u32[]{:S(2)}, u32[]{:S(2)}) collective-permute-start(bf16[1024,256]{1,0:T(8,128)(2,1)S(1)} %collective-permute-done.2.refs_6_), channel_id=1, source_target_pairs={{0,128},{128,0},{1,129},{129,1},{2,130},{130,2},{3,131},{131,3},{4... | collective-permute-start | bytes 1572872 | tf_op jit(solution)/shard_map/ppermute | solution.py:408
  90.8 25.0 %collective-permute-start.9 = (bf16[1024,256]{1,0:T(8,128)(2,1)S(1)}, bf16[1024,256]{1,0:T(8,128)(2,1)S(1)}, u32[]{:S(2)}, u32[]{:S(2)}) collective-permute-start(bf16[1024,256]{1,0:T(8,128)(2,1)S(1)} %collective-permute-done.7.refs_11_), channel_id=1, source_target_pairs={{0,128},{128,0},{1,129},{129,1},{2,130},{130,2},{3,131},{131,3},{4... | collective-permute-start | bytes 1572872 | tf_op jit(solution)/shard_map/ppermute | solution.py:408
  92.7 23.1 %collective-permute-start.17 = (bf16[128,2048]{1,0:T(8,128)(2,1)S(1)}, bf16[128,2048]{1,0:T(8,128)(2,1)S(1)}, u32[]{:S(2)}, u32[]{:S(2)}) collective-permute-start(bf16[128,2048]{1,0:T(8,128)(2,1)S(1)} %collective-permute-done.5.refs_9_), channel_id=1, source_target_pairs={{0,1},{1,2},{2,3},{3,0},{4,5},{5,6},{6,7},{7,4},{8,9},{9,10},{10,1... | collective-permute-start | bytes 1572872 | tf_op jit(solution)/shard_map/ppermute | solution.py:405
  92.7 23.1 %collective-permute-start.18 = (bf16[128,2048]{1,0:T(8,128)(2,1)S(1)}, bf16[128,2048]{1,0:T(8,128)(2,1)S(1)}, u32[]{:S(2)}, u32[]{:S(2)}) collective-permute-start(bf16[128,2048]{1,0:T(8,128)(2,1)S(1)} %collective-permute-done.12.refs_16_), channel_id=1, source_target_pairs={{0,3},{1,0},{2,1},{3,2},{4,7},{5,4},{6,5},{7,6},{8,11},{9,8},{10,9... | collective-permute-start | bytes 1572872 | tf_op jit(solution)/shard_map/ppermute | solution.py:405
  95.4 31.7 %collective-permute-start.15 = (bf16[1024,256]{1,0:T(8,128)(2,1)S(1)}, bf16[1024,256]{1,0:T(8,128)(2,1)S(1)}, u32[]{:S(2)}, u32[]{:S(2)}) collective-permute-start(bf16[1024,256]{1,0:T(8,128)(2,1)S(1)} %collective-permute-done.13.refs_17_), channel_id=1, source_target_pairs={{0,128},{128,0},{1,129},{129,1},{2,130},{130,2},{3,131},{131,3},{4... | collective-permute-start | bytes 1572872 | tf_op jit(solution)/shard_map/ppermute | solution.py:408
  104.6 33.8 %collective-permute-start.16 = (bf16[1024,256]{1,0:T(8,128)(2,1)S(1)}, bf16[1024,256]{1,0:T(8,128)(2,1)}, u32[]{:S(2)}, u32[]{:S(2)}) collective-permute-start(bf16[1024,256]{1,0:T(8,128)(2,1)S(1)} %collective-permute-done.14.refs_18_), channel_id=1, source_target_pairs={{0,128},{128,0},{1,129},{129,1},{2,130},{130,2},{3,131},{131,3},{4... | collective-permute-start | bytes 1572872 | tf_op jit(solution)/shard_map/ppermute | solution.py:408
  151.6 89.4 %all-to-all-start.1 = ((bf16[32,160,128]{2,1,0:T(8,128)(2,1)}), bf16[32,160,128]{2,1,0:T(8,128)(2,1)S(1)}, u32[]{:S(2)}, u32[]{:S(2)}) async-start(bf16[32,160,128]{2,1,0:T(8,128)(2,1)} %experts.1), calls=%async_computation.1 | async-start | bytes 2621440 | tf_op jit(solution)/shard_map/all_to_all | solution.py:440
  167.9 53.8 %collective-permute-start = (bf16[32,2048]{1,0:T(8,128)(2,1)}, bf16[32,2048]{1,0:T(8,128)(2,1)}, u32[]{:S(2)}, u32[]{:S(2)}) collective-permute-start(bf16[32,2048]{1,0:T(8,128)(2,1)} %slice.31), channel_id=1, source_target_pairs={{0,4},{4,8},{8,12},{12,16},{16,20},{20,24},{24,28},{28,32},{32,36}... | collective-permute-start | bytes 393224 | tf_op jit(solution)/shard_map/ppermute | solution.py:417
  (24 other events, 689.9 us)

commit v3 on v2

--- a/solution.py
+++ b/solution.py
@@ -238,7 +238,11 @@
     )(odd, message, *(pltpu.with_memory_space_constraint(w, pltpu.HBM) for w in weights))
 
 
-def combine_kernel(message_ref, target_ref, weight_ref, gain_ref, out_ref, mixed_ref, *, capacity):
+def combine_kernel(
+    message_ref, target_ref, far_ref, gain_ref, out_ref, mixed_ref, weight_ref, signal, *, capacity
+):
+    copy = pltpu.make_async_copy(far_ref, weight_ref, signal)
+    copy.start()
     peers = message_ref.shape[0]
     tokens, width = out_ref.shape
     blocks = width // LANES
@@ -256,6 +260,7 @@
     for q in range(per):
         both = [selection(in_tail[:, k : k + 1], -q * tail, peers * 8, 1).astype(F32) for k in range(2)]
         picks.append(jnp.concatenate(both, axis=0).astype(BF16))
+    copy.wait()
     weight = [weight_ref[:, k : k + 1] for k in range(2)]
     base = blocks * head
     square = jnp.zeros((tokens, LANES), F32)
@@ -283,13 +288,17 @@
 
     return pl.pallas_call(
         kernel,
-        in_specs=[whole()] * 4,
+        in_specs=[whole(), whole(), pl.BlockSpec(memory_space=pltpu.HBM), whole()],
         out_specs=whole(),
         out_shape=jax.ShapeDtypeStruct((tokens, width), BF16),
-        scratch_shapes=[pltpu.VMEM((tokens, width), F32)],
+        scratch_shapes=[
+            pltpu.VMEM((tokens, width), F32),
+            pltpu.VMEM(weight.shape, F32),
+            pltpu.SemaphoreType.DMA,
+        ],
         compiler_params=pltpu.CompilerParams(vmem_limit_bytes=24 << 20),
         name="combine",
-    )(message, target, weight, gain)
+    )(message, target, pltpu.with_memory_space_constraint(weight, pltpu.HBM), gain)
 
 
 def conv_kernel(rows_ref, carried_ref, taps_ref, gain_ref, weight_ref, out_ref, line_ref, sum_ref):
@@ -397,9 +406,6 @@
     across = [(i, i ^ 1) for i in range(lax.axis_size("grp"))]
     gate, up, down = gate_weight[0], up_weight[0], down_weight[0]
     rows, units = gate.shape[0] // 2, down.shape[0] // 2
-    down_a, down_b = down[:units], down[units:]
-    mine_a = jnp.where(odd == 1, up[:rows], gate[:rows])
-    mine_b = jnp.where(odd == 1, up[rows:], gate[rows:])
 
     def send(array, pairs):
         return lax.ppermute(array, "tp", pairs)
@@ -407,35 +413,37 @@
     def swap(array):
         return lax.ppermute(array, "grp", across)
 
-    mine_a_r, mine_b_l = send(mine_a, right), send(mine_b, left)
+    down_r, down_l = send(down, right), send(down, left)
     own_ids = lax.dynamic_slice_in_dim(expert_ids, own * tokens, tokens, 0).T
     message, target = dispatch(
         own.reshape(1), moe_input, moe_gain.reshape(1, width), own_ids, ep_count, capacity
     )
     arrived = lax.all_to_all(message, EP, 0, 0, tiled=True)
+    mine_a = jnp.where(odd == 1, up[:rows], gate[:rows])
+    mine_b = jnp.where(odd == 1, up[rows:], gate[rows:])
+    mine_a_r, mine_b_l = send(mine_a, right), send(mine_b, left)
+    mine_b_r, mine_a_l = send(mine_b, right), send(mine_a, left)
     pairs = [(i, i + 1) for i in range(ep_count - 1)]
     carried = lax.ppermute(conv_input[conv_input.shape[0] - HALO :], EP, pairs)
-    mine_b_r, mine_a_l = send(mine_b, right), send(mine_a, left)
+    down_a_far, down_b_far = send(down_r[:units], right), send(down_l[units:], left)
+    other_a_r, other_b_l = swap(mine_a_r), swap(mine_b_l)
     mine_a_far, mine_b_far = send(mine_a_r, right), send(mine_b_l, left)
-    other_a_r, other_b_l = swap(mine_a_r), swap(mine_b_l)
-    down_a_r, down_b_l = send(down_a, right), send(down_b, left)
     other_b_r, other_a_l = swap(mine_b_r), swap(mine_a_l)
-    down_b_r, down_a_l = send(down_b, right), send(down_a, left)
-    other_a_far, other_b_far = swap(mine_a_far), swap(mine_b_far)
-    down_a_far, down_b_far = send(down_a_r, right), send(down_b_l, left)
+    other_a_far, other_b_far = send(other_a_r, right), send(other_b_l, left)
 
     conv_out = conv_module(conv_input, carried, conv_taps, conv_gain.reshape(1, width), conv_weight)
 
     weights = [gate, up, down]
     sources = [((0,), (1,), (2,), False)]
     for arrays in (
-        (mine_a_r, mine_b_r, other_a_r, other_b_r, down_a_r, down_b_r),
-        (mine_a_l, mine_b_l, other_a_l, other_b_l, down_a_l, down_b_l),
+        (mine_a_r, mine_b_r, other_a_r, other_b_r, down_r),
+        (mine_a_l, mine_b_l, other_a_l, other_b_l, down_l),
         (mine_a_far, mine_b_far, other_a_far, other_b_far, down_a_far, down_b_far),
     ):
         at = len(weights)
         weights.extend(arrays)
-        sources.append(((at, at + 1), (at + 2, at + 3), (at + 4, at + 5), True))
+        parts = tuple(range(at + 4, len(weights)))
+        sources.append(((at, at + 1), (at + 2, at + 3), parts, True))
     results = experts_apply(odd.reshape(1), arrived, weights, tuple(sources), capacity)
     returned = lax.all_to_all(results, EP, 0, 0, tiled=True)
     own_weights = lax.dynamic_slice_in_dim(route_weights, own * tokens, tokens, 0)

time: 245 us -> 226 us (0.922)
  waiting for transfers between devices: 132 us -> 113 us
    ppermute x6 -> x4, waiting for transfers between devices: 40.5 us -> 24.5 us  [swap(): return lax.ppermute(array, 'grp', across)]
    ppermute x12, waiting for transfers between devices: 44.4 us -> 41.4 us  [send(): return lax.ppermute(array, 'tp', pairs)]
    ppermute x6 -> x4, starting transfers between devices: 7.62 us -> 5.27 us  [swap(): return lax.ppermute(array, 'grp', across)]
    unnamed x56 -> x50, local copies, waits for them, and re-layouts: 6.69 us -> 6.71 us
  transfers between devices with their start and end apart: 21 -> 19, of which waited for: 10 -> 10; matrix products, arithmetic and copies ran while one was open for 2% -> 2% of each run, Pallas kernels for 7% -> 8%
where the time goes in v3:
time: 226 us
  waiting for transfers between devices  113 us (50%)
  starting transfers between devices  64.8 us (29%)
  Pallas kernels  37.1 us (16%)
  local copies, waits for them, and re-layouts  9.33 us (4%)
    ppermute x1, waiting for transfers between devices, run(): carried = lax.ppermute(conv_input[conv_input.shape[0] - HALO:], EP, pairs)  47.6 us
    ppermute x12, waiting for transfers between devices, send(): return lax.ppermute(array, 'tp', pairs)  41.4 us
    all_to_all x1, starting transfers between devices, run(): arrived = lax.all_to_all(message, EP, 0, 0, tiled=True)  25.6 us
    ppermute x4, waiting for transfers between devices, swap(): return lax.ppermute(array, 'grp', across)  24.5 us
    pallas_call x1, Pallas kernels, conv_module(): pl.pallas_call(conv_kernel, grid=(count // block,), in_specs=[pl.BlockSpe...  17.6 us
    all_to_all x1, starting transfers between devices, run(): returned = lax.all_to_all(results, EP, 0, 0, tiled=True)  16.2 us
    ppermute x12, starting transfers between devices, send(): return lax.ppermute(array, 'tp', pairs)  14.2 us
    pallas_call x1, Pallas kernels, experts_apply(): pl.pallas_call(kernel, in_specs=[pl.BlockSpec(memory_space=pltpu.SMEM), w...  12.5 us
  transfers between devices with their start and end apart: 19, of which 10 were waited for; matrix products, arithmetic and copies ran while one was open for 2% of the time, Pallas kernels for 8%

profile of v3, /device:TPU:33, one launch (start us, length us, event | category | flops | bytes accessed | tf_op | source)
XLA Modules:
  0.0 225.8 jit_solution(12099427718490115064)
XLA Ops:
  2.1 3.5 %dispatch.1 = (bf16[32,160,128]{2,1,0:T(8,128)(2,1)}, s32[2,160]{1,0:T(2,128)S(1)}) custom-call(s32[1]{0:T(128)} %bitcast.2.refs_0_, bf16[640,2048]{1,0:T(8,128)(2,1)} %refs_1_.1, f32[1,2048]{1,0:T(1,128)S(1)} %bitcast.19, s32[2,160]{1,0:T(2,128)S(1)} %dynamic-slice_bitcast_fusion.refs_3_), custom_call_target="tpu_custom_call" | custom-call | tf_op jit(solution)/shard_map/dispatch/pallas_call | solution.py:103
  5.6 25.6 %all-to-all-start = ((bf16[32,160,128]{2,1,0:T(8,128)(2,1)}), bf16[32,160,128]{2,1,0:T(8,128)(2,1)S(1)}, u32[]{:S(2)}, u32[]{:S(2)}) async-start(bf16[32,160,128]{2,1,0:T(8,128)(2,1)} %get-tuple-element.4), calls=%async_computation | async-start | bytes 2621440 | tf_op jit(solution)/shard_map/all_to_all | solution.py:421
  31.4 1.5 collective-permute-start.1
  32.8 1.3 collective-permute-start.5
  34.2 1.3 collective-permute-start.10
  37.0 9.0 %collective-permute-done.1.refs_5_ = bf16[1024,256]{1,0:T(8,128)(2,1)S(1)} collective-permute-done((bf16[1024,256]{1,0:T(8,128)(2,1)S(1)}, bf16[1024,256]{1,0:T(8,128)(2,1)S(1)}, u32[]{:S(2)}, u32[]{:S(2)}) %collective-permute-start.1) | collective-permute-done | bytes 524320 | tf_op jit(solution)/shard_map/ppermute | solution.py:411
  47.2 21.7 %collective-permute-done.7.refs_11_ = bf16[1024,256]{1,0:T(8,128)(2,1)S(1)} collective-permute-done((bf16[1024,256]{1,0:T(8,128)(2,1)S(1)}, bf16[1024,256]{1,0:T(8,128)(2,1)S(1)}, u32[]{:S(2)}, u32[]{:S(2)}) %collective-permute-start.7) | collective-permute-done | bytes 524320 | tf_op jit(solution)/shard_map/ppermute | solution.py:411
  68.9 1.8 collective-permute-start.3
  70.7 8.9 %collective-permute-done.2.refs_6_ = bf16[1024,256]{1,0:T(8,128)(2,1)S(1)} collective-permute-done((bf16[1024,256]{1,0:T(8,128)(2,1)S(1)}, bf16[1024,256]{1,0:T(8,128)(2,1)S(1)}, u32[]{:S(2)}, u32[]{:S(2)}) %collective-permute-start.2) | collective-permute-done | bytes 524320 | tf_op jit(solution)/shard_map/ppermute | solution.py:411
  79.6 1.8 collective-permute-start.9
  81.5 2.7 %collective-permute-start.12 = (bf16[1024,256]{1,0:T(8,128)(2,1)S(1)}, bf16[1024,256]{1,0:T(8,128)(2,1)S(1)}, u32[]{:S(2)}, u32[]{:S(2)}) collective-permute-start(bf16[1024,256]{1,0:T(8,128)(2,1)S(1)} %collective-permute-done.7.refs_11_), channel_id=1, source_target_pairs={{0,3},{1,0},{2,1},{3,2},{4,7},{5,4},{6,5},{7,6},{8,11},{9,8},{10,9... | collective-permute-start | bytes 1572872 | tf_op jit(solution)/shard_map/ppermute | solution.py:411
  85.9 7.5 %collective-permute-done.9.refs_13_ = bf16[1024,256]{1,0:T(8,128)(2,1)S(1)} collective-permute-done((bf16[1024,256]{1,0:T(8,128)(2,1)S(1)}, bf16[1024,256]{1,0:T(8,128)(2,1)S(1)}, u32[]{:S(2)}, u32[]{:S(2)}) %collective-permute-start.9) | collective-permute-done | bytes 524320 | tf_op jit(solution)/shard_map/ppermute | solution.py:414
  95.0 2.3 collective-permute-start.14
  97.3 7.4 %collective-permute-done.4.refs_8_ = bf16[1024,256]{1,0:T(8,128)(2,1)S(1)} collective-permute-done((bf16[1024,256]{1,0:T(8,128)(2,1)S(1)}, bf16[1024,256]{1,0:T(8,128)(2,1)S(1)}, u32[]{:S(2)}, u32[]{:S(2)}) %collective-permute-start.4) | collective-permute-done | bytes 524320 | tf_op jit(solution)/shard_map/ppermute | solution.py:414
  104.6 1.8 collective-permute-start.16
  106.4 9.6 %collective-permute-done.8.refs_12_ = bf16[1024,256]{1,0:T(8,128)(2,1)S(1)} collective-permute-done((bf16[1024,256]{1,0:T(8,128)(2,1)S(1)}, bf16[1024,256]{1,0:T(8,128)(2,1)S(1)}, u32[]{:S(2)}, u32[]{:S(2)}) %collective-permute-start.8) | collective-permute-done | bytes 524320 | tf_op jit(solution)/shard_map/ppermute | solution.py:414
  118.7 12.5 %experts.1 = bf16[32,160,128]{2,1,0:T(8,128)(2,1)} custom-call(s32[1]{0:T(128)} %bitcast.1.refs_0_, bf16[32,160,128]{2,1,0:T(8,128)(2,1)S(1)} %all-to-all-done.refs_1_, bf16[2048,256]{1,0:T(8,128)(2,1)} %bitcast.22, bf16[2048,256]{1,0:T(8,128)(2,1)} %bitcast.23, bf16[256,2048]{1,0:T(8,128)(2,1)} %bitcast.24, bf16[1024,256]{1,0:T(8,128)(2,1)} %copy-done.11, ...), custom_call_target="tpu_custom_call" | custom-call | tf_op jit(solution)/shard_map/experts/pallas_call | solution.py:224
  131.2 16.2 %all-to-all-start.1 = ((bf16[32,160,128]{2,1,0:T(8,128)(2,1)}), bf16[32,160,128]{2,1,0:T(8,128)(2,1)S(1)}, u32[]{:S(2)}, u32[]{:S(2)}) async-start(bf16[32,160,128]{2,1,0:T(8,128)(2,1)} %experts.1), calls=%async_computation.1 | async-start | bytes 2621440 | tf_op jit(solution)/shard_map/all_to_all | solution.py:448
  147.4 1.6 slice.25
  149.0 3.6 %collective-permute-start = (bf16[32,2048]{1,0:T(8,128)(2,1)}, bf16[32,2048]{1,0:T(8,128)(2,1)}, u32[]{:S(2)}, u32[]{:S(2)}) collective-permute-start(bf16[32,2048]{1,0:T(8,128)(2,1)} %slice.25), channel_id=1, source_target_pairs={{0,4},{4,8},{8,12},{12,16},{16,20},{20,24},{24,28},{28,32},{32,36}... | collective-permute-start | bytes 393224 | tf_op jit(solution)/shard_map/ppermute | solution.py:427
  155.2 47.6 %collective-permute-done.carried_ref = bf16[32,2048]{1,0:T(8,128)(2,1)} collective-permute-done((bf16[32,2048]{1,0:T(8,128)(2,1)}, bf16[32,2048]{1,0:T(8,128)(2,1)}, u32[]{:S(2)}, u32[]{:S(2)}) %collective-permute-start) | collective-permute-done | bytes 131104 | tf_op jit(solution)/shard_map/ppermute | solution.py:427
  202.8 1.7 copy-done.1
  204.5 17.6 %conv.1 = bf16[640,512]{1,0:T(8,128)(2,1)} custom-call(bf16[640,2048]{1,0:T(8,128)(2,1)S(1)} %copy-done.1, bf16[32,2048]{1,0:T(8,128)(2,1)} %collective-permute-done.carried_ref, f32[31,16,128]{2,1,0:T(8,128)S(1)} %slice.34.taps_ref, f32[1,2048]{1,0:T(1,128)S(1)} %bitcast.20, bf16[2048,512]{1,0:T(8,128)(2,1)S(1)} %copy-done.2), custom_call_target="tpu_custom_call" | custom-call | tf_op jit(solution)/shard_map/conv/pallas_call | solution.py:354
  222.1 3.5 %combine.1 = bf16[160,2048]{1,0:T(8,128)(2,1)} custom-call(bf16[32,160,128]{2,1,0:T(8,128)(2,1)S(1)} %all-to-all-done.1.refs_0_, s32[160,2]{1,0:T(8,128)S(1)} %bitcast.18, f32[160,2]{1,0:T(8,128)} %copy.16.refs_2_, f32[1,2048]{1,0:T(1,128)S(1)} %bitcast.21), custom_call_target="tpu_custom_call" | custom-call | tf_op jit(solution)/shard_map/combine/pallas_call | solution.py:289
  (76 shorter events, 12.9 us)
Async XLA Ops:
  5.6 113.1 %all-to-all-start = ((bf16[32,160,128]{2,1,0:T(8,128)(2,1)}), bf16[32,160,128]{2,1,0:T(8,128)(2,1)S(1)}, u32[]{:S(2)}, u32[]{:S(2)}) async-start(bf16[32,160,128]{2,1,0:T(8,128)(2,1)} %get-tuple-element.4), calls=%async_computation | async-start | bytes 2621440 | tf_op jit(solution)/shard_map/all_to_all | solution.py:421
  31.4 14.6 %collective-permute-start.1 = (bf16[1024,256]{1,0:T(8,128)(2,1)S(1)}, bf16[1024,256]{1,0:T(8,128)(2,1)S(1)}, u32[]{:S(2)}, u32[]{:S(2)}) collective-permute-start(bf16[1024,256]{1,0:T(8,128)(2,1)S(1)} %get-tuple-element.7), channel_id=1, source_target_pairs={{0,1},{1,2},{2,3},{3,0},{4,5},{5,6},{6,7},{7,4},{8,9},{9,10},{10,1... | collective-permute-start | bytes 1572872 | tf_op jit(solution)/shard_map/ppermute | solution.py:411
  32.8 48.7 %collective-permute-start.5 = (bf16[256,2048]{1,0:T(8,128)(2,1)S(1)}, bf16[256,2048]{1,0:T(8,128)(2,1)S(1)}, u32[]{:S(2)}, u32[]{:S(2)}) collective-permute-start(bf16[256,2048]{1,0:T(8,128)(2,1)S(1)} %bitcast.25), channel_id=1, source_target_pairs={{0,1},{1,2},{2,3},{3,0},{4,5},{5,6},{6,7},{7,4},{8,9},{9,10},{10,1... | collective-permute-start | bytes 3145736 | tf_op jit(solution)/shard_map/ppermute | solution.py:411
  34.2 50.0 %collective-permute-start.10 = (bf16[256,2048]{1,0:T(8,128)(2,1)S(1)}, bf16[256,2048]{1,0:T(8,128)(2,1)S(1)}, u32[]{:S(2)}, u32[]{:S(2)}) collective-permute-start(bf16[256,2048]{1,0:T(8,128)(2,1)S(1)} %bitcast.26), channel_id=1, source_target_pairs={{0,3},{1,0},{2,1},{3,2},{4,7},{5,4},{6,5},{7,6},{8,11},{9,8},{10,9... | collective-permute-start | bytes 3145736 | tf_op jit(solution)/shard_map/ppermute | solution.py:411
  35.5 33.4 %collective-permute-start.7 = (bf16[1024,256]{1,0:T(8,128)(2,1)S(1)}, bf16[1024,256]{1,0:T(8,128)(2,1)S(1)}, u32[]{:S(2)}, u32[]{:S(2)}) collective-permute-start(bf16[1024,256]{1,0:T(8,128)(2,1)S(1)} %get-tuple-element.6), channel_id=1, source_target_pairs={{0,3},{1,0},{2,1},{3,2},{4,7},{5,4},{6,5},{7,6},{8,11},{9,8},{10,9... | collective-permute-start | bytes 1572872 | tf_op jit(solution)/shard_map/ppermute | solution.py:411
  36.8 42.8 %collective-permute-start.2 = (bf16[1024,256]{1,0:T(8,128)(2,1)S(1)}, bf16[1024,256]{1,0:T(8,128)(2,1)S(1)}, u32[]{:S(2)}, u32[]{:S(2)}) collective-permute-start(bf16[1024,256]{1,0:T(8,128)(2,1)S(1)} %get-tuple-element.6), channel_id=1, source_target_pairs={{0,1},{1,2},{2,3},{3,0},{4,5},{5,6},{6,7},{7,4},{8,9},{9,10},{10,1... | collective-permute-start | bytes 1572872 | tf_op jit(solution)/shard_map/ppermute | solution.py:411
  45.9 70.6 %copy-start.11 = (bf16[1024,256]{1,0:T(8,128)(2,1)}, bf16[1024,256]{1,0:T(8,128)(2,1)S(1)}, u32[]{:S(2)}) copy-start(bf16[1024,256]{1,0:T(8,128)(2,1)S(1)} %collective-permute-done.1.refs_5_) | copy-start | bytes 1572868
  45.9 35.6 %collective-permute-start.6 = (bf16[1024,256]{1,0:T(8,128)(2,1)S(1)}, bf16[1024,256]{1,0:T(8,128)(2,1)S(1)}, u32[]{:S(2)}, u32[]{:S(2)}) collective-permute-start(bf16[1024,256]{1,0:T(8,128)(2,1)S(1)} %get-tuple-element.7), channel_id=1, source_target_pairs={{0,3},{1,0},{2,1},{3,2},{4,7},{5,4},{6,5},{7,6},{8,11},{9,8},{10,9... | collective-permute-start | bytes 1572872 | tf_op jit(solution)/shard_map/ppermute | solution.py:411
  68.9 47.7 %copy-start.12 = (bf16[1024,256]{1,0:T(8,128)(2,1)}, bf16[1024,256]{1,0:T(8,128)(2,1)S(1)}, u32[]{:S(2)}) copy-start(bf16[1024,256]{1,0:T(8,128)(2,1)S(1)} %collective-permute-done.7.refs_11_) | copy-start | bytes 1572868
  68.9 15.9 %collective-permute-start.3 = (bf16[1024,256]{1,0:T(8,128)(2,1)S(1)}, bf16[1024,256]{1,0:T(8,128)(2,1)S(1)}, u32[]{:S(2)}, u32[]{:S(2)}) collective-permute-start(bf16[1024,256]{1,0:T(8,128)(2,1)S(1)} %collective-permute-done.1.refs_5_), channel_id=1, source_target_pairs={{0,128},{128,0},{1,129},{129,1},{2,130},{130,2},{3,131},{131,3},{4... | collective-permute-start | bytes 1572872 | tf_op jit(solution)/shard_map/ppermute | solution.py:414
  79.6 13.8 %collective-permute-start.9 = (bf16[1024,256]{1,0:T(8,128)(2,1)S(1)}, bf16[1024,256]{1,0:T(8,128)(2,1)S(1)}, u32[]{:S(2)}, u32[]{:S(2)}) collective-permute-start(bf16[1024,256]{1,0:T(8,128)(2,1)S(1)} %collective-permute-done.7.refs_11_), channel_id=1, source_target_pairs={{0,128},{128,0},{1,129},{129,1},{2,130},{130,2},{3,131},{131,3},{4... | collective-permute-start | bytes 1572872 | tf_op jit(solution)/shard_map/ppermute | solution.py:414
  81.5 13.1 %collective-permute-start.11 = (bf16[1024,256]{1,0:T(8,128)(2,1)S(1)}, bf16[1024,256]{1,0:T(8,128)(2,1)S(1)}, u32[]{:S(2)}, u32[]{:S(2)}) collective-permute-start(bf16[1024,256]{1,0:T(8,128)(2,1)S(1)} %collective-permute-done.1.refs_5_), channel_id=1, source_target_pairs={{0,1},{1,2},{2,3},{3,0},{4,5},{5,6},{6,7},{7,4},{8,9},{9,10},{10,1... | collective-permute-start | bytes 1572872 | tf_op jit(solution)/shard_map/ppermute | solution.py:411
  81.5 37.2 %copy-start.8 = (bf16[256,2048]{1,0:T(8,128)(2,1)}, bf16[256,2048]{1,0:T(8,128)(2,1)S(1)}, u32[]{:S(2)}) copy-start(bf16[256,2048]{1,0:T(8,128)(2,1)S(1)} %collective-permute-done.5.refs_9_) | copy-start | bytes 3145732
  81.5 13.5 %collective-permute-start.12 = (bf16[1024,256]{1,0:T(8,128)(2,1)S(1)}, bf16[1024,256]{1,0:T(8,128)(2,1)S(1)}, u32[]{:S(2)}, u32[]{:S(2)}) collective-permute-start(bf16[1024,256]{1,0:T(8,128)(2,1)S(1)} %collective-permute-done.7.refs_11_), channel_id=1, source_target_pairs={{0,3},{1,0},{2,1},{3,2},{4,7},{5,4},{6,5},{7,6},{8,11},{9,8},{10,9... | collective-permute-start | bytes 1572872 | tf_op jit(solution)/shard_map/ppermute | solution.py:411
  84.2 20.5 %collective-permute-start.4 = (bf16[1024,256]{1,0:T(8,128)(2,1)S(1)}, bf16[1024,256]{1,0:T(8,128)(2,1)S(1)}, u32[]{:S(2)}, u32[]{:S(2)}) collective-permute-start(bf16[1024,256]{1,0:T(8,128)(2,1)S(1)} %collective-permute-done.2.refs_6_), channel_id=1, source_target_pairs={{0,128},{128,0},{1,129},{129,1},{2,130},{130,2},{3,131},{131,3},{4... | collective-permute-start | bytes 1572872 | tf_op jit(solution)/shard_map/ppermute | solution.py:414
  84.8 31.2 %collective-permute-start.8 = (bf16[1024,256]{1,0:T(8,128)(2,1)S(1)}, bf16[1024,256]{1,0:T(8,128)(2,1)S(1)}, u32[]{:S(2)}, u32[]{:S(2)}) collective-permute-start(bf16[1024,256]{1,0:T(8,128)(2,1)S(1)} %collective-permute-done.6.refs_10_), channel_id=1, source_target_pairs={{0,128},{128,0},{1,129},{129,1},{2,130},{130,2},{3,131},{131,3},{4... | collective-permute-start | bytes 1572872 | tf_op jit(solution)/shard_map/ppermute | solution.py:414
  93.4 23.1 %collective-permute-start.15 = (bf16[128,2048]{1,0:T(8,128)(2,1)S(1)}, bf16[128,2048]{1,0:T(8,128)(2,1)S(1)}, u32[]{:S(2)}, u32[]{:S(2)}) collective-permute-start(bf16[128,2048]{1,0:T(8,128)(2,1)S(1)} %slice.32), channel_id=1, source_target_pairs={{0,1},{1,2},{2,3},{3,0},{4,5},{5,6},{6,7},{7,4},{8,9},{9,10},{10,1... | collective-permute-start | bytes 1572872 | tf_op jit(solution)/shard_map/ppermute | solution.py:411
  94.6 21.9 %collective-permute-start.13 = (bf16[1024,256]{1,0:T(8,128)(2,1)S(1)}, bf16[1024,256]{1,0:T(8,128)(2,1)S(1)}, u32[]{:S(2)}, u32[]{:S(2)}) collective-permute-start(bf16[1024,256]{1,0:T(8,128)(2,1)S(1)} %collective-permute-done.3.refs_7_), channel_id=1, source_target_pairs={{0,1},{1,2},{2,3},{3,0},{4,5},{5,6},{6,7},{7,4},{8,9},{9,10},{10,1... | collective-permute-start | bytes 1572872 | tf_op jit(solution)/shard_map/ppermute | solution.py:411
  95.0 21.5 %collective-permute-start.14 = (bf16[1024,256]{1,0:T(8,128)(2,1)S(1)}, bf16[1024,256]{1,0:T(8,128)(2,1)S(1)}, u32[]{:S(2)}, u32[]{:S(2)}) collective-permute-start(bf16[1024,256]{1,0:T(8,128)(2,1)S(1)} %collective-permute-done.9.refs_13_), channel_id=1, source_target_pairs={{0,3},{1,0},{2,1},{3,2},{4,7},{5,4},{6,5},{7,6},{8,11},{9,8},{10,9... | collective-permute-start | bytes 1572872 | tf_op jit(solution)/shard_map/ppermute | solution.py:411
  104.6 14.0 %collective-permute-start.16 = (bf16[128,2048]{1,0:T(8,128)(2,1)S(1)}, bf16[128,2048]{1,0:T(8,128)(2,1)}, u32[]{:S(2)}, u32[]{:S(2)}) collective-permute-start(bf16[128,2048]{1,0:T(8,128)(2,1)S(1)} %slice.33), channel_id=1, source_target_pairs={{0,3},{1,0},{2,1},{3,2},{4,7},{5,4},{6,5},{7,6},{8,11},{9,8},{10,9... | collective-permute-start | bytes 1572872 | tf_op jit(solution)/shard_map/ppermute | solution.py:411
  131.2 71.6 %copy-start.2 = (bf16[2048,512]{1,0:T(8,128)(2,1)S(1)}, bf16[2048,512]{1,0:T(8,128)(2,1)}, u32[]{:S(2)}) copy-start(bf16[2048,512]{1,0:T(8,128)(2,1)} %weight_ref.1) | copy-start | bytes 6291460
  131.2 90.9 %all-to-all-start.1 = ((bf16[32,160,128]{2,1,0:T(8,128)(2,1)}), bf16[32,160,128]{2,1,0:T(8,128)(2,1)S(1)}, u32[]{:S(2)}, u32[]{:S(2)}) async-start(bf16[32,160,128]{2,1,0:T(8,128)(2,1)} %experts.1), calls=%async_computation.1 | async-start | bytes 2621440 | tf_op jit(solution)/shard_map/all_to_all | solution.py:448
  147.4 55.4 %copy-start.4 = (f32[2048]{0:T(1024)S(1)}, f32[2048]{0:T(1024)}, u32[]{:S(2)}) copy-start(f32[2048]{0:T(1024)} %param.14) | copy-start | bytes 24580
  149.0 53.8 %collective-permute-start = (bf16[32,2048]{1,0:T(8,128)(2,1)}, bf16[32,2048]{1,0:T(8,128)(2,1)}, u32[]{:S(2)}, u32[]{:S(2)}) collective-permute-start(bf16[32,2048]{1,0:T(8,128)(2,1)} %slice.25), channel_id=1, source_target_pairs={{0,4},{4,8},{8,12},{12,16},{16,20},{20,24},{24,28},{28,32},{32,36}... | collective-permute-start | bytes 393224 | tf_op jit(solution)/shard_map/ppermute | solution.py:427
  (19 other events, 294.3 us)

commit v4 on v3

--- a/solution.py
+++ b/solution.py
@@ -119,20 +119,30 @@
     )(own, pltpu.with_memory_space_constraint(rows, pltpu.HBM), gain, ids)
 
 
-def expert_kernel(*refs, sources, peers, capacity, blocks):
+def expert_kernel(*refs, sources, far, peers, capacity, blocks):
     odd_ref, message_ref = refs[0], refs[1]
-    count = (len(refs) - 6) // 2
-    remote = refs[2 : count + 2]
-    out_ref, rows_ref, hidden_ref = refs[count + 2 : count + 5]
-    weights = refs[count + 5 : -1]
-    signals = refs[-1]
+    given = refs[2 : len(far) + 2]
+    out_ref, rows_ref, hidden_ref = refs[len(far) + 2 : len(far) + 5]
+    near, signals = list(refs[len(far) + 5 : -1]), refs[-1]
     odd = odd_ref[0] == 1
-    copies = [
-        pltpu.make_async_copy(far, near, signals.at[i])
-        for i, (far, near) in enumerate(zip(remote, weights))
-    ]
-    for copy in copies:
-        copy.start()
+    weights, copies = [], []
+    for ref, moved in zip(given, far):
+        weights.append(near.pop(0) if moved else ref)
+        copies.append(pltpu.make_async_copy(ref, weights[-1], signals.at[len(copies)]) if moved else None)
+    waves = [[*s[0], *s[1]] for s in sources] + [[d for s in sources for d in s[2]]]
+
+    def issue(wave):
+        for w in wave:
+            if copies[w] is not None:
+                copies[w].start()
+
+    def settle(wave):
+        for w in wave:
+            if copies[w] is not None:
+                copies[w].wait()
+
+    issue(waves[0])
+    issue(waves[1])
     head, tail = split_rows(capacity)
     per = 8 // tail
     heads = peers * head
@@ -157,14 +167,16 @@
                 rows_ref[heads:, c * LANES : (c + 1) * LANES] = dot(gathers[q], part).astype(BF16)
     at = 0
     downs = []
-    for gates, ups, down_parts, swapped in sources:
+    for n, (gates, ups, down_parts, swapped) in enumerate(sources):
+        settle(waves[n])
+        if n + 2 < len(waves):
+            issue(waves[n + 2])
         rows = rows_ref[...]
         values = []
         for group in (gates, ups):
             value = None
             begin = 0
             for g in group:
-                copies[g].wait()
                 size = weights[g].shape[0]
                 part = dot(rows[:, begin : begin + size], weights[g][...])
                 value = part if value is None else value + part
@@ -181,8 +193,7 @@
         for d in down_parts:
             downs.append((at, d))
             at += weights[d].shape[0]
-    for _, d in downs:
-        copies[d].wait()
+    settle(waves[-1])
     slot = lax.broadcasted_iota(jnp.int32, (peers * 8, peers * tail), 1)
     lane = lax.broadcasted_iota(jnp.int32, (peers * 8, peers * tail), 0)
     spreads = [
@@ -213,29 +224,33 @@
         out_ref[:, at_row : at_row + 16, :] = jnp.concatenate(pair, axis=1).astype(BF16)
 
 
-def experts_apply(odd, message, weights, sources, capacity):
+def experts_apply(odd, message, weights, far, sources, capacity):
     peers, lines, _ = message.shape
     blocks = lines // capacity
     units = sum(weights[d].shape[0] for s in sources for d in s[2])
 
     def kernel(*refs):
-        expert_kernel(*refs, sources=sources, peers=peers, capacity=capacity, blocks=blocks)
+        expert_kernel(*refs, sources=sources, far=far, peers=peers, capacity=capacity, blocks=blocks)
 
     return pl.pallas_call(
         kernel,
         in_specs=[pl.BlockSpec(memory_space=pltpu.SMEM), whole()]
-        + [pl.BlockSpec(memory_space=pltpu.HBM)] * len(weights),
+        + [pl.BlockSpec(memory_space=pltpu.HBM) if f else whole() for f in far],
         out_specs=whole(),
         out_shape=jax.ShapeDtypeStruct(message.shape, BF16),
         scratch_shapes=[
             pltpu.VMEM((peers * capacity, blocks * LANES), BF16),
             pltpu.VMEM((peers * capacity, units), BF16),
-            *(pltpu.VMEM(w.shape, BF16) for w in weights),
+            *(pltpu.VMEM(w.shape, BF16) for w, f in zip(weights, far) if f),
             pltpu.SemaphoreType.DMA((len(weights),)),
         ],
         compiler_params=pltpu.CompilerParams(vmem_limit_bytes=40 << 20),
         name="experts",
-    )(odd, message, *(pltpu.with_memory_space_constraint(w, pltpu.HBM) for w in weights))
+    )(
+        odd,
+        message,
+        *(pltpu.with_memory_space_constraint(w, pltpu.HBM) if f else w for w, f in zip(weights, far)),
+    )
 
 
 def combine_kernel(
@@ -444,7 +459,9 @@
         weights.extend(arrays)
         parts = tuple(range(at + 4, len(weights)))
         sources.append(((at, at + 1), (at + 2, at + 3), parts, True))
-    results = experts_apply(odd.reshape(1), arrived, weights, tuple(sources), capacity)
+    late = [id(w) for w in (other_b_r, other_a_l, other_a_far, other_b_far)]
+    far = tuple(id(w) not in late for w in weights)
+    results = experts_apply(odd.reshape(1), arrived, weights, far, tuple(sources), capacity)
     returned = lax.all_to_all(results, EP, 0, 0, tiled=True)
     own_weights = lax.dynamic_slice_in_dim(route_weights, own * tokens, tokens, 0)
     moe_out = combine(returned, target.T, own_weights, post_gain.reshape(1, width), capacity)

time: 226 us -> 223 us (0.987)
  Pallas kernels: 37.1 us -> 34.6 us
    pallas_call x1, Pallas kernels: 12.5 us -> 10 us  [experts_apply(): pl.pallas_call(kernel, in_specs=[pl.BlockSpec(memory_space=pltpu.SMEM), w...]
    unnamed x50 -> x42, local copies, waits for them, and re-layouts: 6.71 us -> 5.73 us
where the time goes in v4:
time: 223 us; the launch traced here: 222 us
  waiting for transfers between devices  114 us (51%)
  starting transfers between devices  63.9 us (29%)
  Pallas kernels  34.6 us (16%)
  local copies, waits for them, and re-layouts  8.35 us (4%)
    ppermute x1, waiting for transfers between devices, run(): carried = lax.ppermute(conv_input[conv_input.shape[0] - HALO:], EP, pairs)  47.6 us
    ppermute x12, waiting for transfers between devices, send(): return lax.ppermute(array, 'tp', pairs)  42.4 us
    all_to_all x1, starting transfers between devices, run(): arrived = lax.all_to_all(message, EP, 0, 0, tiled=True)  25.6 us
    ppermute x4, waiting for transfers between devices, swap(): return lax.ppermute(array, 'grp', across)  24.3 us
    pallas_call x1, Pallas kernels, conv_module(): pl.pallas_call(conv_kernel, grid=(count // block,), in_specs=[pl.BlockSpe...  17.6 us
    all_to_all x1, starting transfers between devices, run(): returned = lax.all_to_all(results, EP, 0, 0, tiled=True)  15.2 us
    ppermute x12, starting transfers between devices, send(): return lax.ppermute(array, 'tp', pairs)  14.3 us
    pallas_call x1, Pallas kernels, experts_apply(): pl.pallas_call(kernel, in_specs=[pl.BlockSpec(memory_space=pltpu.SMEM), w...  10 us
  transfers between devices with their start and end apart: 19, of which 10 were waited for; matrix products, arithmetic and copies ran while one was open for 2% of the time, Pallas kernels for 8%

profile of v4, /device:TPU:33, one launch (start us, length us, event | category | flops | bytes accessed | tf_op | source)
XLA Modules:
  0.0 222.3 jit_solution(11701542410139442725)
XLA Ops:
  2.1 3.4 %dispatch.1 = (bf16[32,160,128]{2,1,0:T(8,128)(2,1)}, s32[2,160]{1,0:T(2,128)S(1)}) custom-call(s32[1]{0:T(128)} %bitcast.2.refs_0_, bf16[640,2048]{1,0:T(8,128)(2,1)} %refs_1_.1, f32[1,2048]{1,0:T(1,128)S(1)} %bitcast.19, s32[2,160]{1,0:T(2,128)S(1)} %dynamic-slice_bitcast_fusion.refs_3_), custom_call_target="tpu_custom_call" | custom-call | tf_op jit(solution)/shard_map/dispatch/pallas_call | solution.py:103
  5.6 25.6 %all-to-all-start = ((bf16[32,160,128]{2,1,0:T(8,128)(2,1)}), bf16[32,160,128]{2,1,0:T(8,128)(2,1)S(1)}, u32[]{:S(2)}, u32[]{:S(2)}) async-start(bf16[32,160,128]{2,1,0:T(8,128)(2,1)} %get-tuple-element.4), calls=%async_computation | async-start | bytes 2621440 | tf_op jit(solution)/shard_map/all_to_all | solution.py:436
  31.4 1.5 collective-permute-start.1
  32.8 1.3 collective-permute-start.5
  34.2 1.3 collective-permute-start.10
  37.0 9.0 %collective-permute-done.1.refs_5_ = bf16[1024,256]{1,0:T(8,128)(2,1)S(1)} collective-permute-done((bf16[1024,256]{1,0:T(8,128)(2,1)S(1)}, bf16[1024,256]{1,0:T(8,128)(2,1)S(1)}, u32[]{:S(2)}, u32[]{:S(2)}) %collective-permute-start.1) | collective-permute-done | bytes 524320 | tf_op jit(solution)/shard_map/ppermute | solution.py:426
  47.1 21.7 %collective-permute-done.7.refs_11_ = bf16[1024,256]{1,0:T(8,128)(2,1)S(1)} collective-permute-done((bf16[1024,256]{1,0:T(8,128)(2,1)S(1)}, bf16[1024,256]{1,0:T(8,128)(2,1)S(1)}, u32[]{:S(2)}, u32[]{:S(2)}) %collective-permute-start.7) | collective-permute-done | bytes 524320 | tf_op jit(solution)/shard_map/ppermute | solution.py:426
  68.9 1.8 collective-permute-start.3
  70.7 8.9 %collective-permute-done.2.refs_6_ = bf16[1024,256]{1,0:T(8,128)(2,1)S(1)} collective-permute-done((bf16[1024,256]{1,0:T(8,128)(2,1)S(1)}, bf16[1024,256]{1,0:T(8,128)(2,1)S(1)}, u32[]{:S(2)}, u32[]{:S(2)}) %collective-permute-start.2) | collective-permute-done | bytes 524320 | tf_op jit(solution)/shard_map/ppermute | solution.py:426
  79.6 1.8 collective-permute-start.9
  81.5 2.7 %collective-permute-start.12 = (bf16[1024,256]{1,0:T(8,128)(2,1)S(1)}, bf16[1024,256]{1,0:T(8,128)(2,1)S(1)}, u32[]{:S(2)}, u32[]{:S(2)}) collective-permute-start(bf16[1024,256]{1,0:T(8,128)(2,1)S(1)} %collective-permute-done.7.refs_11_), channel_id=1, source_target_pairs={{0,3},{1,0},{2,1},{3,2},{4,7},{5,4},{6,5},{7,6},{8,11},{9,8},{10,9... | collective-permute-start | bytes 1572872 | tf_op jit(solution)/shard_map/ppermute | solution.py:426
  85.9 7.5 %collective-permute-done.9.refs_13_ = bf16[1024,256]{1,0:T(8,128)(2,1)S(1)} collective-permute-done((bf16[1024,256]{1,0:T(8,128)(2,1)S(1)}, bf16[1024,256]{1,0:T(8,128)(2,1)S(1)}, u32[]{:S(2)}, u32[]{:S(2)}) %collective-permute-start.9) | collective-permute-done | bytes 524320 | tf_op jit(solution)/shard_map/ppermute | solution.py:429
  95.0 2.4 %collective-permute-start.14 = (bf16[1024,256]{1,0:T(8,128)(2,1)S(1)}, bf16[1024,256]{1,0:T(8,128)(2,1)S(1)}, u32[]{:S(2)}, u32[]{:S(2)}) collective-permute-start(bf16[1024,256]{1,0:T(8,128)(2,1)S(1)} %collective-permute-done.9.refs_13_), channel_id=1, source_target_pairs={{0,3},{1,0},{2,1},{3,2},{4,7},{5,4},{6,5},{7,6},{8,11},{9,8},{10,9... | collective-permute-start | bytes 1572872 | tf_op jit(solution)/shard_map/ppermute | solution.py:426
  97.4 7.3 %collective-permute-done.4.refs_8_ = bf16[1024,256]{1,0:T(8,128)(2,1)S(1)} collective-permute-done((bf16[1024,256]{1,0:T(8,128)(2,1)S(1)}, bf16[1024,256]{1,0:T(8,128)(2,1)S(1)}, u32[]{:S(2)}, u32[]{:S(2)}) %collective-permute-start.4) | collective-permute-done | bytes 524320 | tf_op jit(solution)/shard_map/ppermute | solution.py:429
  104.6 1.8 collective-permute-start.16
  106.4 9.6 %collective-permute-done.8.refs_12_ = bf16[1024,256]{1,0:T(8,128)(2,1)S(1)} collective-permute-done((bf16[1024,256]{1,0:T(8,128)(2,1)S(1)}, bf16[1024,256]{1,0:T(8,128)(2,1)S(1)}, u32[]{:S(2)}, u32[]{:S(2)}) %collective-permute-start.8) | collective-permute-done | bytes 524320 | tf_op jit(solution)/shard_map/ppermute | solution.py:429
  118.7 10.0 %experts.1 = bf16[32,160,128]{2,1,0:T(8,128)(2,1)} custom-call(s32[1]{0:T(128)} %bitcast.1.refs_0_, bf16[32,160,128]{2,1,0:T(8,128)(2,1)S(1)} %all-to-all-done.refs_1_, bf16[2048,256]{1,0:T(8,128)(2,1)} %bitcast.22, bf16[2048,256]{1,0:T(8,128)(2,1)} %bitcast.23, bf16[256,2048]{1,0:T(8,128)(2,1)} %bitcast.24, bf16[1024,256]{1,0:T(8,128)(2,1)} %copy-done.11, ...), custom_call_target="tpu_custom_call" | custom-call | tf_op jit(solution)/shard_map/experts/pallas_call | solution.py:235
  128.7 15.2 %all-to-all-start.1 = ((bf16[32,160,128]{2,1,0:T(8,128)(2,1)}), bf16[32,160,128]{2,1,0:T(8,128)(2,1)S(1)}, u32[]{:S(2)}, u32[]{:S(2)}) async-start(bf16[32,160,128]{2,1,0:T(8,128)(2,1)} %experts.1), calls=%async_computation.1 | async-start | bytes 2621440 | tf_op jit(solution)/shard_map/all_to_all | solution.py:465
  143.9 1.6 slice.25
  145.5 3.6 %collective-permute-start = (bf16[32,2048]{1,0:T(8,128)(2,1)}, bf16[32,2048]{1,0:T(8,128)(2,1)}, u32[]{:S(2)}, u32[]{:S(2)}) collective-permute-start(bf16[32,2048]{1,0:T(8,128)(2,1)} %slice.25), channel_id=1, source_target_pairs={{0,4},{4,8},{8,12},{12,16},{16,20},{20,24},{24,28},{28,32},{32,36}... | collective-permute-start | bytes 393224 | tf_op jit(solution)/shard_map/ppermute | solution.py:442
  151.7 47.6 %collective-permute-done.carried_ref = bf16[32,2048]{1,0:T(8,128)(2,1)} collective-permute-done((bf16[32,2048]{1,0:T(8,128)(2,1)}, bf16[32,2048]{1,0:T(8,128)(2,1)}, u32[]{:S(2)}, u32[]{:S(2)}) %collective-permute-start) | collective-permute-done | bytes 131104 | tf_op jit(solution)/shard_map/ppermute | solution.py:442
  199.3 1.7 copy-done.1
  201.1 17.6 %conv.1 = bf16[640,512]{1,0:T(8,128)(2,1)} custom-call(bf16[640,2048]{1,0:T(8,128)(2,1)S(1)} %copy-done.1, bf16[32,2048]{1,0:T(8,128)(2,1)} %collective-permute-done.carried_ref, f32[31,16,128]{2,1,0:T(8,128)S(1)} %slice.34.taps_ref, f32[1,2048]{1,0:T(1,128)S(1)} %bitcast.20, bf16[2048,512]{1,0:T(8,128)(2,1)S(1)} %copy-done.2), custom_call_target="tpu_custom_call" | custom-call | tf_op jit(solution)/shard_map/conv/pallas_call | solution.py:369
  218.6 3.5 %combine.1 = bf16[160,2048]{1,0:T(8,128)(2,1)} custom-call(bf16[32,160,128]{2,1,0:T(8,128)(2,1)S(1)} %all-to-all-done.1.refs_0_, s32[160,2]{1,0:T(8,128)S(1)} %bitcast.18, f32[160,2]{1,0:T(8,128)} %copy.16.refs_2_, f32[1,2048]{1,0:T(1,128)S(1)} %bitcast.21), custom_call_target="tpu_custom_call" | custom-call | tf_op jit(solution)/shard_map/combine/pallas_call | solution.py:304
  (68 shorter events, 12.9 us)
Async XLA Ops:
  5.6 113.1 %all-to-all-start = ((bf16[32,160,128]{2,1,0:T(8,128)(2,1)}), bf16[32,160,128]{2,1,0:T(8,128)(2,1)S(1)}, u32[]{:S(2)}, u32[]{:S(2)}) async-start(bf16[32,160,128]{2,1,0:T(8,128)(2,1)} %get-tuple-element.4), calls=%async_computation | async-start | bytes 2621440 | tf_op jit(solution)/shard_map/all_to_all | solution.py:436
  31.4 14.6 %collective-permute-start.1 = (bf16[1024,256]{1,0:T(8,128)(2,1)S(1)}, bf16[1024,256]{1,0:T(8,128)(2,1)S(1)}, u32[]{:S(2)}, u32[]{:S(2)}) collective-permute-start(bf16[1024,256]{1,0:T(8,128)(2,1)S(1)} %get-tuple-element.7), channel_id=1, source_target_pairs={{0,1},{1,2},{2,3},{3,0},{4,5},{5,6},{6,7},{7,4},{8,9},{9,10},{10,1... | collective-permute-start | bytes 1572872 | tf_op jit(solution)/shard_map/ppermute | solution.py:426
  32.8 48.7 %collective-permute-start.5 = (bf16[256,2048]{1,0:T(8,128)(2,1)S(1)}, bf16[256,2048]{1,0:T(8,128)(2,1)S(1)}, u32[]{:S(2)}, u32[]{:S(2)}) collective-permute-start(bf16[256,2048]{1,0:T(8,128)(2,1)S(1)} %bitcast.25), channel_id=1, source_target_pairs={{0,1},{1,2},{2,3},{3,0},{4,5},{5,6},{6,7},{7,4},{8,9},{9,10},{10,1... | collective-permute-start | bytes 3145736 | tf_op jit(solution)/shard_map/ppermute | solution.py:426
  34.2 50.0 %collective-permute-start.10 = (bf16[256,2048]{1,0:T(8,128)(2,1)S(1)}, bf16[256,2048]{1,0:T(8,128)(2,1)S(1)}, u32[]{:S(2)}, u32[]{:S(2)}) collective-permute-start(bf16[256,2048]{1,0:T(8,128)(2,1)S(1)} %bitcast.26), channel_id=1, source_target_pairs={{0,3},{1,0},{2,1},{3,2},{4,7},{5,4},{6,5},{7,6},{8,11},{9,8},{10,9... | collective-permute-start | bytes 3145736 | tf_op jit(solution)/shard_map/ppermute | solution.py:426
  35.5 33.4 %collective-permute-start.7 = (bf16[1024,256]{1,0:T(8,128)(2,1)S(1)}, bf16[1024,256]{1,0:T(8,128)(2,1)S(1)}, u32[]{:S(2)}, u32[]{:S(2)}) collective-permute-start(bf16[1024,256]{1,0:T(8,128)(2,1)S(1)} %get-tuple-element.6), channel_id=1, source_target_pairs={{0,3},{1,0},{2,1},{3,2},{4,7},{5,4},{6,5},{7,6},{8,11},{9,8},{10,9... | collective-permute-start | bytes 1572872 | tf_op jit(solution)/shard_map/ppermute | solution.py:426
  36.8 42.8 %collective-permute-start.2 = (bf16[1024,256]{1,0:T(8,128)(2,1)S(1)}, bf16[1024,256]{1,0:T(8,128)(2,1)S(1)}, u32[]{:S(2)}, u32[]{:S(2)}) collective-permute-start(bf16[1024,256]{1,0:T(8,128)(2,1)S(1)} %get-tuple-element.6), channel_id=1, source_target_pairs={{0,1},{1,2},{2,3},{3,0},{4,5},{5,6},{6,7},{7,4},{8,9},{9,10},{10,1... | collective-permute-start | bytes 1572872 | tf_op jit(solution)/shard_map/ppermute | solution.py:426
  45.9 49.1 %copy-start.11 = (bf16[1024,256]{1,0:T(8,128)(2,1)}, bf16[1024,256]{1,0:T(8,128)(2,1)S(1)}, u32[]{:S(2)}) copy-start(bf16[1024,256]{1,0:T(8,128)(2,1)S(1)} %collective-permute-done.1.refs_5_) | copy-start | bytes 1572868
  45.9 35.6 %collective-permute-start.6 = (bf16[1024,256]{1,0:T(8,128)(2,1)S(1)}, bf16[1024,256]{1,0:T(8,128)(2,1)S(1)}, u32[]{:S(2)}, u32[]{:S(2)}) collective-permute-start(bf16[1024,256]{1,0:T(8,128)(2,1)S(1)} %get-tuple-element.7), channel_id=1, source_target_pairs={{0,3},{1,0},{2,1},{3,2},{4,7},{5,4},{6,5},{7,6},{8,11},{9,8},{10,9... | collective-permute-start | bytes 1572872 | tf_op jit(solution)/shard_map/ppermute | solution.py:426
  68.9 47.7 %copy-start.12 = (bf16[1024,256]{1,0:T(8,128)(2,1)}, bf16[1024,256]{1,0:T(8,128)(2,1)S(1)}, u32[]{:S(2)}) copy-start(bf16[1024,256]{1,0:T(8,128)(2,1)S(1)} %collective-permute-done.7.refs_11_) | copy-start | bytes 1572868
  68.9 15.9 %collective-permute-start.3 = (bf16[1024,256]{1,0:T(8,128)(2,1)S(1)}, bf16[1024,256]{1,0:T(8,128)(2,1)S(1)}, u32[]{:S(2)}, u32[]{:S(2)}) collective-permute-start(bf16[1024,256]{1,0:T(8,128)(2,1)S(1)} %collective-permute-done.1.refs_5_), channel_id=1, source_target_pairs={{0,128},{128,0},{1,129},{129,1},{2,130},{130,2},{3,131},{131,3},{4... | collective-permute-start | bytes 1572872 | tf_op jit(solution)/shard_map/ppermute | solution.py:429
  79.6 36.9 %copy-start.13 = (bf16[1024,256]{1,0:T(8,128)(2,1)}, bf16[1024,256]{1,0:T(8,128)(2,1)S(1)}, u32[]{:S(2)}) copy-start(bf16[1024,256]{1,0:T(8,128)(2,1)S(1)} %collective-permute-done.2.refs_6_) | copy-start | bytes 1572868
  79.6 13.8 %collective-permute-start.9 = (bf16[1024,256]{1,0:T(8,128)(2,1)S(1)}, bf16[1024,256]{1,0:T(8,128)(2,1)S(1)}, u32[]{:S(2)}, u32[]{:S(2)}) collective-permute-start(bf16[1024,256]{1,0:T(8,128)(2,1)S(1)} %collective-permute-done.7.refs_11_), channel_id=1, source_target_pairs={{0,128},{128,0},{1,129},{129,1},{2,130},{130,2},{3,131},{131,3},{4... | collective-permute-start | bytes 1572872 | tf_op jit(solution)/shard_map/ppermute | solution.py:429
  81.5 13.1 %collective-permute-start.11 = (bf16[1024,256]{1,0:T(8,128)(2,1)S(1)}, bf16[1024,256]{1,0:T(8,128)(2,1)S(1)}, u32[]{:S(2)}, u32[]{:S(2)}) collective-permute-start(bf16[1024,256]{1,0:T(8,128)(2,1)S(1)} %collective-permute-done.1.refs_5_), channel_id=1, source_target_pairs={{0,1},{1,2},{2,3},{3,0},{4,5},{5,6},{6,7},{7,4},{8,9},{9,10},{10,1... | collective-permute-start | bytes 1572872 | tf_op jit(solution)/shard_map/ppermute | solution.py:426
  81.5 13.5 %collective-permute-start.12 = (bf16[1024,256]{1,0:T(8,128)(2,1)S(1)}, bf16[1024,256]{1,0:T(8,128)(2,1)S(1)}, u32[]{:S(2)}, u32[]{:S(2)}) collective-permute-start(bf16[1024,256]{1,0:T(8,128)(2,1)S(1)} %collective-permute-done.7.refs_11_), channel_id=1, source_target_pairs={{0,3},{1,0},{2,1},{3,2},{4,7},{5,4},{6,5},{7,6},{8,11},{9,8},{10,9... | collective-permute-start | bytes 1572872 | tf_op jit(solution)/shard_map/ppermute | solution.py:426
  84.2 20.5 %collective-permute-start.4 = (bf16[1024,256]{1,0:T(8,128)(2,1)S(1)}, bf16[1024,256]{1,0:T(8,128)(2,1)S(1)}, u32[]{:S(2)}, u32[]{:S(2)}) collective-permute-start(bf16[1024,256]{1,0:T(8,128)(2,1)S(1)} %collective-permute-done.2.refs_6_), channel_id=1, source_target_pairs={{0,128},{128,0},{1,129},{129,1},{2,130},{130,2},{3,131},{131,3},{4... | collective-permute-start | bytes 1572872 | tf_op jit(solution)/shard_map/ppermute | solution.py:429
  84.8 31.2 %collective-permute-start.8 = (bf16[1024,256]{1,0:T(8,128)(2,1)S(1)}, bf16[1024,256]{1,0:T(8,128)(2,1)S(1)}, u32[]{:S(2)}, u32[]{:S(2)}) collective-permute-start(bf16[1024,256]{1,0:T(8,128)(2,1)S(1)} %collective-permute-done.6.refs_10_), channel_id=1, source_target_pairs={{0,128},{128,0},{1,129},{129,1},{2,130},{130,2},{3,131},{131,3},{4... | collective-permute-start | bytes 1572872 | tf_op jit(solution)/shard_map/ppermute | solution.py:429
  93.4 23.1 %collective-permute-start.15 = (bf16[128,2048]{1,0:T(8,128)(2,1)S(1)}, bf16[128,2048]{1,0:T(8,128)(2,1)S(1)}, u32[]{:S(2)}, u32[]{:S(2)}) collective-permute-start(bf16[128,2048]{1,0:T(8,128)(2,1)S(1)} %slice.32), channel_id=1, source_target_pairs={{0,1},{1,2},{2,3},{3,0},{4,5},{5,6},{6,7},{7,4},{8,9},{9,10},{10,1... | collective-permute-start | bytes 1572872 | tf_op jit(solution)/shard_map/ppermute | solution.py:426
  94.6 21.9 %collective-permute-start.13 = (bf16[1024,256]{1,0:T(8,128)(2,1)S(1)}, bf16[1024,256]{1,0:T(8,128)(2,1)S(1)}, u32[]{:S(2)}, u32[]{:S(2)}) collective-permute-start(bf16[1024,256]{1,0:T(8,128)(2,1)S(1)} %collective-permute-done.3.refs_7_), channel_id=1, source_target_pairs={{0,1},{1,2},{2,3},{3,0},{4,5},{5,6},{6,7},{7,4},{8,9},{9,10},{10,1... | collective-permute-start | bytes 1572872 | tf_op jit(solution)/shard_map/ppermute | solution.py:426
  95.0 21.5 %collective-permute-start.14 = (bf16[1024,256]{1,0:T(8,128)(2,1)S(1)}, bf16[1024,256]{1,0:T(8,128)(2,1)S(1)}, u32[]{:S(2)}, u32[]{:S(2)}) collective-permute-start(bf16[1024,256]{1,0:T(8,128)(2,1)S(1)} %collective-permute-done.9.refs_13_), channel_id=1, source_target_pairs={{0,3},{1,0},{2,1},{3,2},{4,7},{5,4},{6,5},{7,6},{8,11},{9,8},{10,9... | collective-permute-start | bytes 1572872 | tf_op jit(solution)/shard_map/ppermute | solution.py:426
  104.6 14.0 %collective-permute-start.16 = (bf16[128,2048]{1,0:T(8,128)(2,1)S(1)}, bf16[128,2048]{1,0:T(8,128)(2,1)}, u32[]{:S(2)}, u32[]{:S(2)}) collective-permute-start(bf16[128,2048]{1,0:T(8,128)(2,1)S(1)} %slice.33), channel_id=1, source_target_pairs={{0,3},{1,0},{2,1},{3,2},{4,7},{5,4},{6,5},{7,6},{8,11},{9,8},{10,9... | collective-permute-start | bytes 1572872 | tf_op jit(solution)/shard_map/ppermute | solution.py:426
  128.7 70.6 %copy-start.2 = (bf16[2048,512]{1,0:T(8,128)(2,1)S(1)}, bf16[2048,512]{1,0:T(8,128)(2,1)}, u32[]{:S(2)}) copy-start(bf16[2048,512]{1,0:T(8,128)(2,1)} %weight_ref.1) | copy-start | bytes 6291460
  128.7 89.9 %all-to-all-start.1 = ((bf16[32,160,128]{2,1,0:T(8,128)(2,1)}), bf16[32,160,128]{2,1,0:T(8,128)(2,1)S(1)}, u32[]{:S(2)}, u32[]{:S(2)}) async-start(bf16[32,160,128]{2,1,0:T(8,128)(2,1)} %experts.1), calls=%async_computation.1 | async-start | bytes 2621440 | tf_op jit(solution)/shard_map/all_to_all | solution.py:465
  143.9 55.4 %copy-start.4 = (f32[2048]{0:T(1024)S(1)}, f32[2048]{0:T(1024)}, u32[]{:S(2)}) copy-start(f32[2048]{0:T(1024)} %param.14) | copy-start | bytes 24580
  145.5 53.8 %collective-permute-start = (bf16[32,2048]{1,0:T(8,128)(2,1)}, bf16[32,2048]{1,0:T(8,128)(2,1)}, u32[]{:S(2)}, u32[]{:S(2)}) collective-permute-start(bf16[32,2048]{1,0:T(8,128)(2,1)} %slice.25), channel_id=1, source_target_pairs={{0,4},{4,8},{8,12},{12,16},{16,20},{20,24},{24,28},{28,32},{32,36}... | collective-permute-start | bytes 393224 | tf_op jit(solution)/shard_map/ppermute | solution.py:442
  (15 other events, 243.6 us)

commit v5 on v4

--- a/solution.py
+++ b/solution.py
@@ -121,25 +121,38 @@
 
 def expert_kernel(*refs, sources, far, peers, capacity, blocks):
     odd_ref, message_ref = refs[0], refs[1]
-    given = refs[2 : len(far) + 2]
-    out_ref, rows_ref, hidden_ref = refs[len(far) + 2 : len(far) + 5]
-    near, signals = list(refs[len(far) + 5 : -1]), refs[-1]
+    count = sum(len(rows) for rows in far)
+    given = list(refs[2 : count + 2])
+    out_ref, rows_ref, hidden_ref = refs[count + 2 : count + 5]
+    near, signals = list(refs[count + 5 : -1]), refs[-1]
     odd = odd_ref[0] == 1
     weights, copies = [], []
-    for ref, moved in zip(given, far):
-        weights.append(near.pop(0) if moved else ref)
-        copies.append(pltpu.make_async_copy(ref, weights[-1], signals.at[len(copies)]) if moved else None)
+    used = 0
+    for rows in far:
+        pieces = [given.pop(0) for _ in rows]
+        if rows == (0,):
+            weights.append(pieces[0])
+            copies.append([])
+            continue
+        weights.append(near.pop(0))
+        moves, at = [], 0
+        for piece, size in zip(pieces, rows):
+            place = weights[-1].at[at : at + size, :]
+            moves.append(pltpu.make_async_copy(piece, place, signals.at[used]))
+            at += size
+            used += 1
+        copies.append(moves)
     waves = [[*s[0], *s[1]] for s in sources] + [[d for s in sources for d in s[2]]]
 
     def issue(wave):
         for w in wave:
-            if copies[w] is not None:
-                copies[w].start()
+            for move in copies[w]:
+                move.start()
 
     def settle(wave):
         for w in wave:
-            if copies[w] is not None:
-                copies[w].wait()
+            for move in copies[w]:
+                move.wait()
 
     issue(waves[0])
     issue(waves[1])
@@ -224,33 +237,38 @@
         out_ref[:, at_row : at_row + 16, :] = jnp.concatenate(pair, axis=1).astype(BF16)
 
 
-def experts_apply(odd, message, weights, far, sources, capacity):
+def experts_apply(odd, message, matrices, direct, sources, capacity):
     peers, lines, _ = message.shape
     blocks = lines // capacity
-    units = sum(weights[d].shape[0] for s in sources for d in s[2])
+    far = tuple((0,) if d else tuple(p.shape[0] for p in m) for m, d in zip(matrices, direct))
+    units = sum(sum(p.shape[0] for p in matrices[d]) for s in sources for d in s[2])
 
     def kernel(*refs):
         expert_kernel(*refs, sources=sources, far=far, peers=peers, capacity=capacity, blocks=blocks)
 
+    operands, specs, scratch = [], [], []
+    for pieces, rows in zip(matrices, far):
+        if rows == (0,):
+            operands.extend(pieces)
+            specs.append(whole())
+            continue
+        operands.extend(pltpu.with_memory_space_constraint(p, pltpu.HBM) for p in pieces)
+        specs.extend(pl.BlockSpec(memory_space=pltpu.HBM) for _ in pieces)
+        scratch.append(pltpu.VMEM((sum(rows), pieces[0].shape[1]), BF16))
     return pl.pallas_call(
         kernel,
-        in_specs=[pl.BlockSpec(memory_space=pltpu.SMEM), whole()]
-        + [pl.BlockSpec(memory_space=pltpu.HBM) if f else whole() for f in far],
+        in_specs=[pl.BlockSpec(memory_space=pltpu.SMEM), whole(), *specs],
         out_specs=whole(),
         out_shape=jax.ShapeDtypeStruct(message.shape, BF16),
         scratch_shapes=[
             pltpu.VMEM((peers * capacity, blocks * LANES), BF16),
             pltpu.VMEM((peers * capacity, units), BF16),
-            *(pltpu.VMEM(w.shape, BF16) for w, f in zip(weights, far) if f),
-            pltpu.SemaphoreType.DMA((len(weights),)),
+            *scratch,
+            pltpu.SemaphoreType.DMA((len(operands),)),
         ],
         compiler_params=pltpu.CompilerParams(vmem_limit_bytes=40 << 20),
         name="experts",
-    )(
-        odd,
-        message,
-        *(pltpu.with_memory_space_constraint(w, pltpu.HBM) if f else w for w, f in zip(weights, far)),
-    )
+    )(odd, message, *operands)
 
 
 def combine_kernel(
@@ -420,7 +438,7 @@
     left = [(i, (i - 1) % quarters) for i in range(quarters)]
     across = [(i, i ^ 1) for i in range(lax.axis_size("grp"))]
     gate, up, down = gate_weight[0], up_weight[0], down_weight[0]
-    rows, units = gate.shape[0] // 2, down.shape[0] // 2
+    half, part = gate.shape[0] // 2, down.shape[0] * 3 // 4
 
     def send(array, pairs):
         return lax.ppermute(array, "tp", pairs)
@@ -428,40 +446,43 @@
     def swap(array):
         return lax.ppermute(array, "grp", across)
 
-    down_r, down_l = send(down, right), send(down, left)
+    down_r = send(down, right)
+    mine_a = jnp.where(odd == 1, up[:half], gate[:half])
+    mine_b = jnp.where(odd == 1, up[half:], gate[half:])
+    mine_a_l, mine_b_l = send(mine_a, left), send(mine_b, left)
     own_ids = lax.dynamic_slice_in_dim(expert_ids, own * tokens, tokens, 0).T
     message, target = dispatch(
         own.reshape(1), moe_input, moe_gain.reshape(1, width), own_ids, ep_count, capacity
     )
     arrived = lax.all_to_all(message, EP, 0, 0, tiled=True)
-    mine_a = jnp.where(odd == 1, up[:rows], gate[:rows])
-    mine_b = jnp.where(odd == 1, up[rows:], gate[rows:])
-    mine_a_r, mine_b_l = send(mine_a, right), send(mine_b, left)
-    mine_b_r, mine_a_l = send(mine_b, right), send(mine_a, left)
+    mine_a_r, mine_b_r = send(mine_a, right), send(mine_b, right)
+    other_a_l, mine_a_far = swap(mine_a_l), send(mine_a_l, left)
+    down_l = send(down, left)
     pairs = [(i, i + 1) for i in range(ep_count - 1)]
     carried = lax.ppermute(conv_input[conv_input.shape[0] - HALO :], EP, pairs)
-    down_a_far, down_b_far = send(down_r[:units], right), send(down_l[units:], left)
-    other_a_r, other_b_l = swap(mine_a_r), swap(mine_b_l)
-    mine_a_far, mine_b_far = send(mine_a_r, right), send(mine_b_l, left)
-    other_b_r, other_a_l = swap(mine_b_r), swap(mine_a_l)
-    other_a_far, other_b_far = send(other_a_r, right), send(other_b_l, left)
+    other_b_l, mine_b_far = swap(mine_b_l), send(mine_b_l, left)
+    down_a_far = send(down_r[:part], right)
+    other_a_r = swap(mine_a_r)
+    other_b_r = swap(mine_b_r)
+    other_a_far = swap(mine_a_far)
+    other_b_far, down_b_far = send(other_b_r, right), send(down_l[part:], left)
 
     conv_out = conv_module(conv_input, carried, conv_taps, conv_gain.reshape(1, width), conv_weight)
 
-    weights = [gate, up, down]
-    sources = [((0,), (1,), (2,), False)]
-    for arrays in (
-        (mine_a_r, mine_b_r, other_a_r, other_b_r, down_r),
-        (mine_a_l, mine_b_l, other_a_l, other_b_l, down_l),
-        (mine_a_far, mine_b_far, other_a_far, other_b_far, down_a_far, down_b_far),
-    ):
-        at = len(weights)
-        weights.extend(arrays)
-        parts = tuple(range(at + 4, len(weights)))
-        sources.append(((at, at + 1), (at + 2, at + 3), parts, True))
-    late = [id(w) for w in (other_b_r, other_a_l, other_a_far, other_b_far)]
-    far = tuple(id(w) not in late for w in weights)
-    results = experts_apply(odd.reshape(1), arrived, weights, far, tuple(sources), capacity)
+    matrices = [
+        *((gate,), (up,), (down,)),
+        *((mine_a_r, mine_b_r), (other_a_r, other_b_r), (down_r,)),
+        *((mine_a_l, mine_b_l), (other_a_l, other_b_l), (down_l,)),
+        *((mine_a_far,), (mine_b_far,), (other_a_far,), (other_b_far,), (down_a_far, down_b_far)),
+    ]
+    sources = (
+        ((0,), (1,), (2,), False),
+        ((6,), (7,), (8,), True),
+        ((3,), (4,), (5,), True),
+        ((9, 10), (11, 12), (13,), True),
+    )
+    direct = tuple(n in (10, 11, 12) for n in range(len(matrices)))
+    results = experts_apply(odd.reshape(1), arrived, matrices, direct, sources, capacity)
     returned = lax.all_to_all(results, EP, 0, 0, tiled=True)
     own_weights = lax.dynamic_slice_in_dim(route_weights, own * tokens, tokens, 0)
     moe_out = combine(returned, target.T, own_weights, post_gain.reshape(1, width), capacity)

time: 223 us -> 231 us (1.036)
  waiting for transfers between devices: 114 us -> 125 us
    ppermute x12 -> x11, waiting for transfers between devices: 42.4 us -> 55 us  [send(): return lax.ppermute(array, 'tp', pairs)]
    ppermute x4 -> x5, waiting for transfers between devices: 24.3 us -> 22.5 us  [swap(): return lax.ppermute(array, 'grp', across)]
    ppermute x12 -> x11, starting transfers between devices: 14.3 us -> 12.9 us  [send(): return lax.ppermute(array, 'tp', pairs)]
    unnamed x42 -> x44, local copies, waits for them, and re-layouts: 5.73 us -> 4.95 us
    ppermute x4 -> x5, starting transfers between devices: 5.27 us -> 5.94 us  [swap(): return lax.ppermute(array, 'grp', across)]
  transfers between devices with their start and end apart: 19 -> 19, of which waited for: 10 -> 8; matrix products, arithmetic and copies ran while one was open for 2% -> 2% of each run, Pallas kernels for 8% -> 8%
where the time goes in v5:
time: 231 us
  waiting for transfers between devices  125 us (54%)
  starting transfers between devices  62.9 us (27%)
  Pallas kernels  33.7 us (15%)
  local copies, waits for them, and re-layouts  7.58 us (3%)
    ppermute x11, waiting for transfers between devices, send(): return lax.ppermute(array, 'tp', pairs)  55 us
    ppermute x1, waiting for transfers between devices, run(): carried = lax.ppermute(conv_input[conv_input.shape[0] - HALO:], EP, pairs)  47.6 us
    all_to_all x1, starting transfers between devices, run(): arrived = lax.all_to_all(message, EP, 0, 0, tiled=True)  25.6 us
    ppermute x5, waiting for transfers between devices, swap(): return lax.ppermute(array, 'grp', across)  22.5 us
    pallas_call x1, Pallas kernels, conv_module(): pl.pallas_call(conv_kernel, grid=(count // block,), in_specs=[pl.BlockSpe...  17.6 us
    all_to_all x1, starting transfers between devices, run(): returned = lax.all_to_all(results, EP, 0, 0, tiled=True)  14.9 us
    ppermute x11, starting transfers between devices, send(): return lax.ppermute(array, 'tp', pairs)  12.9 us
    pallas_call x1, Pallas kernels, experts_apply(): pl.pallas_call(kernel, in_specs=[pl.BlockSpec(memory_space=pltpu.SMEM), w...  9.16 us
  transfers between devices with their start and end apart: 19, of which 8 were waited for; matrix products, arithmetic and copies ran while one was open for 2% of the time, Pallas kernels for 8%

profile of v5, /device:TPU:33, one launch (start us, length us, event | category | flops | bytes accessed | tf_op | source)
XLA Modules:
  0.0 230.5 jit_solution(15423304971962895754)
XLA Ops:
  2.1 3.4 %dispatch.1 = (bf16[32,160,128]{2,1,0:T(8,128)(2,1)}, s32[2,160]{1,0:T(2,128)S(1)}) custom-call(s32[1]{0:T(128)} %bitcast.2.refs_0_, bf16[640,2048]{1,0:T(8,128)(2,1)} %refs_1_.1, f32[1,2048]{1,0:T(1,128)S(1)} %bitcast.19, s32[2,160]{1,0:T(2,128)S(1)} %dynamic-slice_bitcast_fusion.refs_3_), custom_call_target="tpu_custom_call" | custom-call | tf_op jit(solution)/shard_map/dispatch/pallas_call | solution.py:103
  5.6 25.6 %all-to-all-start = ((bf16[32,160,128]{2,1,0:T(8,128)(2,1)}), bf16[32,160,128]{2,1,0:T(8,128)(2,1)S(1)}, u32[]{:S(2)}, u32[]{:S(2)}) async-start(bf16[32,160,128]{2,1,0:T(8,128)(2,1)} %get-tuple-element.4), calls=%async_computation | async-start | bytes 2621440 | tf_op jit(solution)/shard_map/all_to_all | solution.py:457
  31.4 3.0 %collective-permute-start.6 = (bf16[1024,256]{1,0:T(8,128)(2,1)S(1)}, bf16[1024,256]{1,0:T(8,128)(2,1)S(1)}, u32[]{:S(2)}, u32[]{:S(2)}) collective-permute-start(bf16[1024,256]{1,0:T(8,128)(2,1)S(1)} %get-tuple-element.7), channel_id=1, source_target_pairs={{0,3},{1,0},{2,1},{3,2},{4,7},{5,4},{6,5},{7,6},{8,11},{9,8},{10,9... | collective-permute-start | bytes 1572872 | tf_op jit(solution)/shard_map/ppermute | solution.py:444
  34.4 2.7 %collective-permute-start.7 = (bf16[1024,256]{1,0:T(8,128)(2,1)S(1)}, bf16[1024,256]{1,0:T(8,128)(2,1)S(1)}, u32[]{:S(2)}, u32[]{:S(2)}) collective-permute-start(bf16[1024,256]{1,0:T(8,128)(2,1)S(1)} %get-tuple-element.6), channel_id=1, source_target_pairs={{0,3},{1,0},{2,1},{3,2},{4,7},{5,4},{6,5},{7,6},{8,11},{9,8},{10,9... | collective-permute-start | bytes 1572872 | tf_op jit(solution)/shard_map/ppermute | solution.py:444
  37.0 7.9 %collective-permute-done.6.refs_10_ = bf16[1024,256]{1,0:T(8,128)(2,1)S(1)} collective-permute-done((bf16[1024,256]{1,0:T(8,128)(2,1)S(1)}, bf16[1024,256]{1,0:T(8,128)(2,1)S(1)}, u32[]{:S(2)}, u32[]{:S(2)}) %collective-permute-start.6) | collective-permute-done | bytes 524320 | tf_op jit(solution)/shard_map/ppermute | solution.py:444
  44.9 3.4 %collective-permute-start.11 = (bf16[1024,256]{1,0:T(8,128)(2,1)S(1)}, bf16[1024,256]{1,0:T(8,128)(2,1)S(1)}, u32[]{:S(2)}, u32[]{:S(2)}) collective-permute-start(bf16[1024,256]{1,0:T(8,128)(2,1)S(1)} %collective-permute-done.6.refs_10_), channel_id=1, source_target_pairs={{0,3},{1,0},{2,1},{3,2},{4,7},{5,4},{6,5},{7,6},{8,11},{9,8},{10,9... | collective-permute-start | bytes 1572872 | tf_op jit(solution)/shard_map/ppermute | solution.py:444
  48.5 7.7 %collective-permute-done.7.refs_11_ = bf16[1024,256]{1,0:T(8,128)(2,1)S(1)} collective-permute-done((bf16[1024,256]{1,0:T(8,128)(2,1)S(1)}, bf16[1024,256]{1,0:T(8,128)(2,1)S(1)}, u32[]{:S(2)}, u32[]{:S(2)}) %collective-permute-start.7) | collective-permute-done | bytes 524320 | tf_op jit(solution)/shard_map/ppermute | solution.py:444
  56.2 1.8 collective-permute-start.4
  58.0 23.8 %collective-permute-done.1.refs_5_ = bf16[1024,256]{1,0:T(8,128)(2,1)S(1)} collective-permute-done((bf16[1024,256]{1,0:T(8,128)(2,1)S(1)}, bf16[1024,256]{1,0:T(8,128)(2,1)S(1)}, u32[]{:S(2)}, u32[]{:S(2)}) %collective-permute-start.1) | collective-permute-done | bytes 524320 | tf_op jit(solution)/shard_map/ppermute | solution.py:444
  81.8 2.0 collective-permute-start.3
  84.0 1.4 collective-permute-start.15
  85.4 15.7 %collective-permute-done.12.refs_16_ = bf16[1024,256]{1,0:T(8,128)(2,1)S(1)} collective-permute-done((bf16[1024,256]{1,0:T(8,128)(2,1)S(1)}, bf16[1024,256]{1,0:T(8,128)(2,1)S(1)}, u32[]{:S(2)}, u32[]{:S(2)}) %collective-permute-start.12) | collective-permute-done | bytes 524320 | tf_op jit(solution)/shard_map/ppermute | solution.py:444
  101.1 1.8 collective-permute-start.9
  104.0 1.4 collective-permute-done.8.refs_12_
  106.8 9.9 %collective-permute-done.9.refs_13_ = bf16[1024,256]{1,0:T(8,128)(2,1)S(1)} collective-permute-done((bf16[1024,256]{1,0:T(8,128)(2,1)S(1)}, bf16[1024,256]{1,0:T(8,128)(2,1)S(1)}, u32[]{:S(2)}, u32[]{:S(2)}) %collective-permute-start.9) | collective-permute-done | bytes 524320 | tf_op jit(solution)/shard_map/ppermute | solution.py:447
  116.7 11.2 %collective-permute-done.13.refs_17_ = bf16[1024,256]{1,0:T(8,128)(2,1)S(1)} collective-permute-done((bf16[1024,256]{1,0:T(8,128)(2,1)S(1)}, bf16[1024,256]{1,0:T(8,128)(2,1)S(1)}, u32[]{:S(2)}, u32[]{:S(2)}) %collective-permute-start.13) | collective-permute-done | bytes 524320 | tf_op jit(solution)/shard_map/ppermute | solution.py:447
  128.1 9.2 %experts.1 = bf16[32,160,128]{2,1,0:T(8,128)(2,1)} custom-call(s32[1]{0:T(128)} %bitcast.1.refs_0_, bf16[32,160,128]{2,1,0:T(8,128)(2,1)S(1)} %all-to-all-done.refs_1_, bf16[2048,256]{1,0:T(8,128)(2,1)} %bitcast.22, bf16[2048,256]{1,0:T(8,128)(2,1)} %bitcast.23, bf16[256,2048]{1,0:T(8,128)(2,1)} %bitcast.24, bf16[1024,256]{1,0:T(8,128)(2,1)} %copy-done.14, ...), custom_call_target="tpu_custom_call" | custom-call | tf_op jit(solution)/shard_map/experts/pallas_call | solution.py:258
  137.2 14.9 %all-to-all-start.1 = ((bf16[32,160,128]{2,1,0:T(8,128)(2,1)}), bf16[32,160,128]{2,1,0:T(8,128)(2,1)S(1)}, u32[]{:S(2)}, u32[]{:S(2)}) async-start(bf16[32,160,128]{2,1,0:T(8,128)(2,1)} %experts.1), calls=%async_computation.1 | async-start | bytes 2621440 | tf_op jit(solution)/shard_map/all_to_all | solution.py:486
  152.1 1.6 slice.25
  153.7 3.6 %collective-permute-start = (bf16[32,2048]{1,0:T(8,128)(2,1)}, bf16[32,2048]{1,0:T(8,128)(2,1)}, u32[]{:S(2)}, u32[]{:S(2)}) collective-permute-start(bf16[32,2048]{1,0:T(8,128)(2,1)} %slice.25), channel_id=1, source_target_pairs={{0,4},{4,8},{8,12},{12,16},{16,20},{20,24},{24,28},{28,32},{32,36}... | collective-permute-start | bytes 393224 | tf_op jit(solution)/shard_map/ppermute | solution.py:462
  159.9 47.6 %collective-permute-done.carried_ref = bf16[32,2048]{1,0:T(8,128)(2,1)} collective-permute-done((bf16[32,2048]{1,0:T(8,128)(2,1)}, bf16[32,2048]{1,0:T(8,128)(2,1)}, u32[]{:S(2)}, u32[]{:S(2)}) %collective-permute-start) | collective-permute-done | bytes 131104 | tf_op jit(solution)/shard_map/ppermute | solution.py:462
  207.5 1.7 copy-done.1
  209.3 17.6 %conv.1 = bf16[640,512]{1,0:T(8,128)(2,1)} custom-call(bf16[640,2048]{1,0:T(8,128)(2,1)S(1)} %copy-done.1, bf16[32,2048]{1,0:T(8,128)(2,1)} %collective-permute-done.carried_ref, f32[31,16,128]{2,1,0:T(8,128)S(1)} %slice.34.taps_ref, f32[1,2048]{1,0:T(1,128)S(1)} %bitcast.20, bf16[2048,512]{1,0:T(8,128)(2,1)S(1)} %copy-done.2), custom_call_target="tpu_custom_call" | custom-call | tf_op jit(solution)/shard_map/conv/pallas_call | solution.py:387
  226.8 3.5 %combine.1 = bf16[160,2048]{1,0:T(8,128)(2,1)} custom-call(bf16[32,160,128]{2,1,0:T(8,128)(2,1)S(1)} %all-to-all-done.1.refs_0_, s32[160,2]{1,0:T(8,128)S(1)} %bitcast.18, f32[160,2]{1,0:T(8,128)} %copy.16.refs_2_, f32[1,2048]{1,0:T(1,128)S(1)} %bitcast.21), custom_call_target="tpu_custom_call" | custom-call | tf_op jit(solution)/shard_map/combine/pallas_call | solution.py:322
  (70 shorter events, 7.1 us)
Async XLA Ops:
  5.6 122.5 %all-to-all-start = ((bf16[32,160,128]{2,1,0:T(8,128)(2,1)}), bf16[32,160,128]{2,1,0:T(8,128)(2,1)S(1)}, u32[]{:S(2)}, u32[]{:S(2)}) async-start(bf16[32,160,128]{2,1,0:T(8,128)(2,1)} %get-tuple-element.4), calls=%async_computation | async-start | bytes 2621440 | tf_op jit(solution)/shard_map/all_to_all | solution.py:457
  31.4 13.6 %collective-permute-start.6 = (bf16[1024,256]{1,0:T(8,128)(2,1)S(1)}, bf16[1024,256]{1,0:T(8,128)(2,1)S(1)}, u32[]{:S(2)}, u32[]{:S(2)}) collective-permute-start(bf16[1024,256]{1,0:T(8,128)(2,1)S(1)} %get-tuple-element.7), channel_id=1, source_target_pairs={{0,3},{1,0},{2,1},{3,2},{4,7},{5,4},{6,5},{7,6},{8,11},{9,8},{10,9... | collective-permute-start | bytes 1572872 | tf_op jit(solution)/shard_map/ppermute | solution.py:444
  34.3 14.0 %collective-permute-start.2 = (bf16[1024,256]{1,0:T(8,128)(2,1)S(1)}, bf16[1024,256]{1,0:T(8,128)(2,1)S(1)}, u32[]{:S(2)}, u32[]{:S(2)}) collective-permute-start(bf16[1024,256]{1,0:T(8,128)(2,1)S(1)} %get-tuple-element.6), channel_id=1, source_target_pairs={{0,1},{1,2},{2,3},{3,0},{4,5},{5,6},{6,7},{7,4},{8,9},{9,10},{10,1... | collective-permute-start | bytes 1572872 | tf_op jit(solution)/shard_map/ppermute | solution.py:444
  34.4 49.4 %collective-permute-start.5 = (bf16[256,2048]{1,0:T(8,128)(2,1)S(1)}, bf16[256,2048]{1,0:T(8,128)(2,1)S(1)}, u32[]{:S(2)}, u32[]{:S(2)}) collective-permute-start(bf16[256,2048]{1,0:T(8,128)(2,1)S(1)} %bitcast.25), channel_id=1, source_target_pairs={{0,1},{1,2},{2,3},{3,0},{4,5},{5,6},{6,7},{7,4},{8,9},{9,10},{10,1... | collective-permute-start | bytes 3145736 | tf_op jit(solution)/shard_map/ppermute | solution.py:444
  34.4 21.8 %collective-permute-start.7 = (bf16[1024,256]{1,0:T(8,128)(2,1)S(1)}, bf16[1024,256]{1,0:T(8,128)(2,1)S(1)}, u32[]{:S(2)}, u32[]{:S(2)}) collective-permute-start(bf16[1024,256]{1,0:T(8,128)(2,1)S(1)} %get-tuple-element.6), channel_id=1, source_target_pairs={{0,3},{1,0},{2,1},{3,2},{4,7},{5,4},{6,5},{7,6},{8,11},{9,8},{10,9... | collective-permute-start | bytes 1572872 | tf_op jit(solution)/shard_map/ppermute | solution.py:444
  37.0 44.7 %collective-permute-start.1 = (bf16[1024,256]{1,0:T(8,128)(2,1)S(1)}, bf16[1024,256]{1,0:T(8,128)(2,1)S(1)}, u32[]{:S(2)}, u32[]{:S(2)}) collective-permute-start(bf16[1024,256]{1,0:T(8,128)(2,1)S(1)} %get-tuple-element.7), channel_id=1, source_target_pairs={{0,1},{1,2},{2,3},{3,0},{4,5},{5,6},{6,7},{7,4},{8,9},{9,10},{10,1... | collective-permute-start | bytes 1572872 | tf_op jit(solution)/shard_map/ppermute | solution.py:444
  44.9 83.1 %copy-start.11 = (bf16[1024,256]{1,0:T(8,128)(2,1)}, bf16[1024,256]{1,0:T(8,128)(2,1)S(1)}, u32[]{:S(2)}) copy-start(bf16[1024,256]{1,0:T(8,128)(2,1)S(1)} %collective-permute-done.6.refs_10_) | copy-start | bytes 1572868
  44.9 36.8 %collective-permute-start.11 = (bf16[1024,256]{1,0:T(8,128)(2,1)S(1)}, bf16[1024,256]{1,0:T(8,128)(2,1)S(1)}, u32[]{:S(2)}, u32[]{:S(2)}) collective-permute-start(bf16[1024,256]{1,0:T(8,128)(2,1)S(1)} %collective-permute-done.6.refs_10_), channel_id=1, source_target_pairs={{0,3},{1,0},{2,1},{3,2},{4,7},{5,4},{6,5},{7,6},{8,11},{9,8},{10,9... | collective-permute-start | bytes 1572872 | tf_op jit(solution)/shard_map/ppermute | solution.py:444
  48.3 79.6 %copy-start.12 = (bf16[1024,256]{1,0:T(8,128)(2,1)}, bf16[1024,256]{1,0:T(8,128)(2,1)S(1)}, u32[]{:S(2)}) copy-start(bf16[1024,256]{1,0:T(8,128)(2,1)S(1)} %collective-permute-done.2.refs_6_) | copy-start | bytes 1572868
  48.3 54.8 %collective-permute-start.10 = (bf16[256,2048]{1,0:T(8,128)(2,1)S(1)}, bf16[256,2048]{1,0:T(8,128)(2,1)S(1)}, u32[]{:S(2)}, u32[]{:S(2)}) collective-permute-start(bf16[256,2048]{1,0:T(8,128)(2,1)S(1)} %bitcast.26), channel_id=1, source_target_pairs={{0,3},{1,0},{2,1},{3,2},{4,7},{5,4},{6,5},{7,6},{8,11},{9,8},{10,9... | collective-permute-start | bytes 3145736 | tf_op jit(solution)/shard_map/ppermute | solution.py:444
  56.2 71.8 %copy-start.13 = (bf16[1024,256]{1,0:T(8,128)(2,1)}, bf16[1024,256]{1,0:T(8,128)(2,1)S(1)}, u32[]{:S(2)}) copy-start(bf16[1024,256]{1,0:T(8,128)(2,1)S(1)} %collective-permute-done.7.refs_11_) | copy-start | bytes 1572868
  56.2 27.8 %collective-permute-start.4 = (bf16[1024,256]{1,0:T(8,128)(2,1)S(1)}, bf16[1024,256]{1,0:T(8,128)(2,1)S(1)}, u32[]{:S(2)}, u32[]{:S(2)}) collective-permute-start(bf16[1024,256]{1,0:T(8,128)(2,1)S(1)} %collective-permute-done.2.refs_6_), channel_id=1, source_target_pairs={{0,128},{128,0},{1,129},{129,1},{2,130},{130,2},{3,131},{131,3},{4... | collective-permute-start | bytes 1572872 | tf_op jit(solution)/shard_map/ppermute | solution.py:447
  81.8 19.3 %collective-permute-start.12 = (bf16[1024,256]{1,0:T(8,128)(2,1)S(1)}, bf16[1024,256]{1,0:T(8,128)(2,1)S(1)}, u32[]{:S(2)}, u32[]{:S(2)}) collective-permute-start(bf16[1024,256]{1,0:T(8,128)(2,1)S(1)} %collective-permute-done.7.refs_11_), channel_id=1, source_target_pairs={{0,3},{1,0},{2,1},{3,2},{4,7},{5,4},{6,5},{7,6},{8,11},{9,8},{10,9... | collective-permute-start | bytes 1572872 | tf_op jit(solution)/shard_map/ppermute | solution.py:444
  81.8 21.2 %collective-permute-start.3 = (bf16[1024,256]{1,0:T(8,128)(2,1)S(1)}, bf16[1024,256]{1,0:T(8,128)(2,1)S(1)}, u32[]{:S(2)}, u32[]{:S(2)}) collective-permute-start(bf16[1024,256]{1,0:T(8,128)(2,1)S(1)} %collective-permute-done.1.refs_5_), channel_id=1, source_target_pairs={{0,128},{128,0},{1,129},{129,1},{2,130},{130,2},{3,131},{131,3},{4... | collective-permute-start | bytes 1572872 | tf_op jit(solution)/shard_map/ppermute | solution.py:447
  83.8 21.7 %collective-permute-start.8 = (bf16[1024,256]{1,0:T(8,128)(2,1)S(1)}, bf16[1024,256]{1,0:T(8,128)(2,1)S(1)}, u32[]{:S(2)}, u32[]{:S(2)}) collective-permute-start(bf16[1024,256]{1,0:T(8,128)(2,1)S(1)} %collective-permute-done.6.refs_10_), channel_id=1, source_target_pairs={{0,128},{128,0},{1,129},{129,1},{2,130},{130,2},{3,131},{131,3},{4... | collective-permute-start | bytes 1572872 | tf_op jit(solution)/shard_map/ppermute | solution.py:447
  84.0 44.0 %collective-permute-start.15 = (bf16[192,2048]{1,0:T(8,128)(2,1)S(1)}, bf16[192,2048]{1,0:T(8,128)(2,1)}, u32[]{:S(2)}, u32[]{:S(2)}) collective-permute-start(bf16[192,2048]{1,0:T(8,128)(2,1)S(1)} %slice.32), channel_id=1, source_target_pairs={{0,1},{1,2},{2,3},{3,0},{4,5},{5,6},{6,7},{7,4},{8,9},{9,10},{10,1... | collective-permute-start | bytes 2359304 | tf_op jit(solution)/shard_map/ppermute | solution.py:444
  101.1 15.6 %collective-permute-start.9 = (bf16[1024,256]{1,0:T(8,128)(2,1)S(1)}, bf16[1024,256]{1,0:T(8,128)(2,1)S(1)}, u32[]{:S(2)}, u32[]{:S(2)}) collective-permute-start(bf16[1024,256]{1,0:T(8,128)(2,1)S(1)} %collective-permute-done.7.refs_11_), channel_id=1, source_target_pairs={{0,128},{128,0},{1,129},{129,1},{2,130},{130,2},{3,131},{131,3},{4... | collective-permute-start | bytes 1572872 | tf_op jit(solution)/shard_map/ppermute | solution.py:447
  103.0 25.0 %collective-permute-start.13 = (bf16[1024,256]{1,0:T(8,128)(2,1)S(1)}, bf16[1024,256]{1,0:T(8,128)(2,1)S(1)}, u32[]{:S(2)}, u32[]{:S(2)}) collective-permute-start(bf16[1024,256]{1,0:T(8,128)(2,1)S(1)} %collective-permute-done.11.refs_15_), channel_id=1, source_target_pairs={{0,128},{128,0},{1,129},{129,1},{2,130},{130,2},{3,131},{131,3},{4... | collective-permute-start | bytes 1572872 | tf_op jit(solution)/shard_map/ppermute | solution.py:447
  103.1 24.8 %collective-permute-start.14 = (bf16[1024,256]{1,0:T(8,128)(2,1)S(1)}, bf16[1024,256]{1,0:T(8,128)(2,1)S(1)}, u32[]{:S(2)}, u32[]{:S(2)}) collective-permute-start(bf16[1024,256]{1,0:T(8,128)(2,1)S(1)} %collective-permute-done.4.refs_8_), channel_id=1, source_target_pairs={{0,1},{1,2},{2,3},{3,0},{4,5},{5,6},{6,7},{7,4},{8,9},{9,10},{10,1... | collective-permute-start | bytes 1572872 | tf_op jit(solution)/shard_map/ppermute | solution.py:444
  105.5 11.2 %collective-permute-start.16 = (bf16[64,2048]{1,0:T(8,128)(2,1)S(1)}, bf16[64,2048]{1,0:T(8,128)(2,1)S(1)}, u32[]{:S(2)}, u32[]{:S(2)}) collective-permute-start(bf16[64,2048]{1,0:T(8,128)(2,1)S(1)} %slice.33), channel_id=1, source_target_pairs={{0,3},{1,0},{2,1},{3,2},{4,7},{5,4},{6,5},{7,6},{8,11},{9,8},{10,9... | collective-permute-start | bytes 786440 | tf_op jit(solution)/shard_map/ppermute | solution.py:444
  137.2 70.3 %copy-start.2 = (bf16[2048,512]{1,0:T(8,128)(2,1)S(1)}, bf16[2048,512]{1,0:T(8,128)(2,1)}, u32[]{:S(2)}) copy-start(bf16[2048,512]{1,0:T(8,128)(2,1)} %weight_ref.1) | copy-start | bytes 6291460
  137.2 89.6 %all-to-all-start.1 = ((bf16[32,160,128]{2,1,0:T(8,128)(2,1)}), bf16[32,160,128]{2,1,0:T(8,128)(2,1)S(1)}, u32[]{:S(2)}, u32[]{:S(2)}) async-start(bf16[32,160,128]{2,1,0:T(8,128)(2,1)} %experts.1), calls=%async_computation.1 | async-start | bytes 2621440 | tf_op jit(solution)/shard_map/all_to_all | solution.py:486
  152.1 55.4 %copy-start.4 = (f32[2048]{0:T(1024)S(1)}, f32[2048]{0:T(1024)}, u32[]{:S(2)}) copy-start(f32[2048]{0:T(1024)} %param.14) | copy-start | bytes 24580
  153.7 53.8 %collective-permute-start = (bf16[32,2048]{1,0:T(8,128)(2,1)}, bf16[32,2048]{1,0:T(8,128)(2,1)}, u32[]{:S(2)}, u32[]{:S(2)}) collective-permute-start(bf16[32,2048]{1,0:T(8,128)(2,1)} %slice.25), channel_id=1, source_target_pairs={{0,4},{4,8},{8,12},{12,16},{16,20},{20,24},{24,28},{28,32},{32,36}... | collective-permute-start | bytes 393224 | tf_op jit(solution)/shard_map/ppermute | solution.py:462
  (16 other events, 325.7 us)

commit v6 on v5

--- a/solution.py
+++ b/solution.py
@@ -45,16 +45,46 @@
 
 
 def dispatch_kernel(
-    own_ref, all_ref, gain_ref, ids_ref, out_ref, target_ref, rows_ref, signal, *, experts, capacity
+    own_ref,
+    all_ref,
+    far_gain_ref,
+    ids_ref,
+    gate_ref,
+    up_ref,
+    out_ref,
+    target_ref,
+    *rest,
+    experts,
+    capacity,
 ):
+    picked, (rows_ref, gain_ref, signals) = rest[:-3], rest[-3:]
     tokens, width = rows_ref.shape
-    copy = pltpu.make_async_copy(
-        all_ref.at[pl.ds(pl.multiple_of(own_ref[0] * tokens, 16), tokens), :], rows_ref, signal
-    )
-    copy.start()
     blocks = width // LANES
     head, tail = split_rows(capacity)
     per = 8 // tail
+    copy = pltpu.make_async_copy(
+        all_ref.at[pl.ds(pl.multiple_of(own_ref[0] * tokens, 16), tokens), :],
+        rows_ref,
+        signals.at[0],
+    )
+    copy.start()
+    gain_copy = pltpu.make_async_copy(far_gain_ref, gain_ref, signals.at[1])
+    gain_copy.start()
+
+    def moves(source_ref):
+        at = 0
+        for i, ref in enumerate(picked):
+            rows = source_ref.at[at : at + ref.shape[0], :]
+            yield pltpu.make_async_copy(rows, ref, signals.at[2 + i])
+            at += ref.shape[0]
+
+    for odd, source_ref in ((0, gate_ref), (1, up_ref)):
+
+        @pl.when(own_ref[1] == odd)
+        def _(source_ref=source_ref):
+            for move in moves(source_ref):
+                move.start()
+
     ids = ids_ref[...]
     onehot = [
         (ids[k : k + 1, :] == lax.broadcasted_iota(jnp.int32, (experts, tokens), 0)).astype(F32)
@@ -80,6 +110,7 @@
     pick = pick.astype(BF16)
     picks = jnp.concatenate(picks, axis=1).astype(BF16)
     copy.wait()
+    gain_copy.wait()
     rows = rows_ref[...].astype(F32)
     mean_square = jnp.mean(rows * rows, axis=-1, keepdims=True)
     normed = (rows * lax.rsqrt(mean_square + EPSILON) * gain_ref[...]).astype(BF16)
@@ -91,32 +122,42 @@
     put_message(
         out_ref, lambda c: dot(pick, col(normed, c)), tail_of, experts, head, tail, blocks
     )
-
-
-def dispatch(own, rows, gain, ids, experts, capacity):
+    for odd, source_ref in ((0, gate_ref), (1, up_ref)):
+
+        @pl.when(own_ref[1] == odd)
+        def _(source_ref=source_ref):
+            for move in moves(source_ref):
+                move.wait()
+
+
+def dispatch(own, rows, gain, ids, gate, up, cuts, experts, capacity):
     tokens = ids.shape[1]
     width = rows.shape[1]
+    hbm = pl.BlockSpec(memory_space=pltpu.HBM)
 
     def kernel(*refs):
         dispatch_kernel(*refs, experts=experts, capacity=capacity)
 
+    def held(array):
+        return pltpu.with_memory_space_constraint(array, pltpu.HBM)
+
     return pl.pallas_call(
         kernel,
-        in_specs=[
-            pl.BlockSpec(memory_space=pltpu.SMEM),
-            pl.BlockSpec(memory_space=pltpu.HBM),
-            whole(),
-            whole(),
+        in_specs=[pl.BlockSpec(memory_space=pltpu.SMEM), hbm, hbm, whole(), hbm, hbm],
+        out_specs=[whole(), whole(), *(hbm for _ in cuts)],
+        scratch_shapes=[
+            pltpu.VMEM((tokens, width), BF16),
+            pltpu.VMEM(gain.shape, F32),
+            pltpu.SemaphoreType.DMA((2 + len(cuts),)),
         ],
-        out_specs=[whole(), whole()],
-        scratch_shapes=[pltpu.VMEM((tokens, width), BF16), pltpu.SemaphoreType.DMA],
         out_shape=[
             jax.ShapeDtypeStruct((experts, capacity * width // LANES, LANES), BF16),
             jax.ShapeDtypeStruct((2, tokens), jnp.int32),
+            *(pltpu.HBM((cut, gate.shape[1]), BF16) for cut in cuts),
         ],
         compiler_params=pltpu.CompilerParams(vmem_limit_bytes=24 << 20),
         name="dispatch",
-    )(own, pltpu.with_memory_space_constraint(rows, pltpu.HBM), gain, ids)
+    )(own, held(rows), held(gain), ids, held(gate), held(up))
 
 
 def expert_kernel(*refs, sources, far, peers, capacity, blocks):
@@ -133,6 +174,14 @@
         if rows == (0,):
             weights.append(pieces[0])
             copies.append([])
+            continue
+        if rows[0] < 0:
+            weights.append(near.pop(0))
+            copies.append([])
+            at = 0
+            for piece in pieces:
+                weights[-1][at : at + piece.shape[0], :] = piece[...]
+                at += piece.shape[0]
             continue
         weights.append(near.pop(0))
         moves, at = [], 0
@@ -240,7 +289,10 @@
 def experts_apply(odd, message, matrices, direct, sources, capacity):
     peers, lines, _ = message.shape
     blocks = lines // capacity
-    far = tuple((0,) if d else tuple(p.shape[0] for p in m) for m, d in zip(matrices, direct))
+    far = []
+    for pieces, held in zip(matrices, direct):
+        rows = tuple(p.shape[0] for p in pieces)
+        far.append(rows if not held else (0,) if len(rows) == 1 else tuple(-r for r in rows))
     units = sum(sum(p.shape[0] for p in matrices[d]) for s in sources for d in s[2])
 
     def kernel(*refs):
@@ -252,9 +304,13 @@
             operands.extend(pieces)
             specs.append(whole())
             continue
+        scratch.append(pltpu.VMEM((abs(sum(rows)), pieces[0].shape[1]), BF16))
+        if rows[0] < 0:
+            operands.extend(pieces)
+            specs.extend(whole() for _ in pieces)
+            continue
         operands.extend(pltpu.with_memory_space_constraint(p, pltpu.HBM) for p in pieces)
         specs.extend(pl.BlockSpec(memory_space=pltpu.HBM) for _ in pieces)
-        scratch.append(pltpu.VMEM((sum(rows), pieces[0].shape[1]), BF16))
     return pl.pallas_call(
         kernel,
         in_specs=[pl.BlockSpec(memory_space=pltpu.SMEM), whole(), *specs],
@@ -438,7 +494,7 @@
     left = [(i, (i - 1) % quarters) for i in range(quarters)]
     across = [(i, i ^ 1) for i in range(lax.axis_size("grp"))]
     gate, up, down = gate_weight[0], up_weight[0], down_weight[0]
-    half, part = gate.shape[0] // 2, down.shape[0] * 3 // 4
+    half, part = gate.shape[0] // 2, down.shape[0] * 7 // 8
 
     def send(array, pairs):
         return lax.ppermute(array, "tp", pairs)
@@ -447,13 +503,19 @@
         return lax.ppermute(array, "grp", across)
 
     down_r = send(down, right)
-    mine_a = jnp.where(odd == 1, up[:half], gate[:half])
-    mine_b = jnp.where(odd == 1, up[half:], gate[half:])
+    own_ids = lax.dynamic_slice_in_dim(expert_ids, own * tokens, tokens, 0).T
+    message, target, mine_a, mine_b = dispatch(
+        jnp.stack([own, odd]),
+        moe_input,
+        moe_gain.reshape(1, width),
+        own_ids,
+        gate,
+        up,
+        (half, gate.shape[0] - half),
+        ep_count,
+        capacity,
+    )
     mine_a_l, mine_b_l = send(mine_a, left), send(mine_b, left)
-    own_ids = lax.dynamic_slice_in_dim(expert_ids, own * tokens, tokens, 0).T
-    message, target = dispatch(
-        own.reshape(1), moe_input, moe_gain.reshape(1, width), own_ids, ep_count, capacity
-    )
     arrived = lax.all_to_all(message, EP, 0, 0, tiled=True)
     mine_a_r, mine_b_r = send(mine_a, right), send(mine_b, right)
     other_a_l, mine_a_far = swap(mine_a_l), send(mine_a_l, left)
@@ -481,7 +543,7 @@
         ((3,), (4,), (5,), True),
         ((9, 10), (11, 12), (13,), True),
     )
-    direct = tuple(n in (10, 11, 12) for n in range(len(matrices)))
+    direct = tuple(n in (11, 12, 13) for n in range(len(matrices)))
     results = experts_apply(odd.reshape(1), arrived, matrices, direct, sources, capacity)
     returned = lax.all_to_all(results, EP, 0, 0, tiled=True)
     own_weights = lax.dynamic_slice_in_dim(route_weights, own * tokens, tokens, 0)

time: 231 us -> 260 us (1.13)
  Pallas kernels: 33.7 us -> 64.7 us
  waiting for transfers between devices: 125 us -> 119 us
  starting transfers between devices: 62.9 us -> 67.8 us
    pallas_call x1, Pallas kernels: 3.44 us -> 34.5 us  [dispatch(): pl.pallas_call(kernel, in_specs=[pl.BlockSpec(memory_space=pltpu.SMEM), h...]
    ppermute x11, starting transfers between devices: 12.9 us -> 16.2 us  [send(): return lax.ppermute(array, 'tp', pairs)]
    ppermute x11, waiting for transfers between devices: 55 us -> 51.7 us  [send(): return lax.ppermute(array, 'tp', pairs)]
  transfers between devices with their start and end apart: 19 -> 19, of which waited for: 8 -> 8; matrix products, arithmetic and copies ran while one was open for 2% -> 2% of each run, Pallas kernels for 8% -> 7%
where the time goes in v6:
time: 260 us
  waiting for transfers between devices  119 us (46%)
  starting transfers between devices  67.8 us (26%)
  Pallas kernels  64.7 us (25%)
  local copies, waits for them, and re-layouts  6.8 us (3%)
    ppermute x11, waiting for transfers between devices, send(): return lax.ppermute(array, 'tp', pairs)  51.7 us
    ppermute x1, waiting for transfers between devices, run(): carried = lax.ppermute(conv_input[conv_input.shape[0] - HALO:], EP, pairs)  47.6 us
    pallas_call x1, Pallas kernels, dispatch(): pl.pallas_call(kernel, in_specs=[pl.BlockSpec(memory_space=pltpu.SMEM), h...  34.5 us
    all_to_all x1, starting transfers between devices, run(): arrived = lax.all_to_all(message, EP, 0, 0, tiled=True)  25.6 us
    ppermute x5, waiting for transfers between devices, swap(): return lax.ppermute(array, 'grp', across)  20.1 us
    pallas_call x1, Pallas kernels, conv_module(): pl.pallas_call(conv_kernel, grid=(count // block,), in_specs=[pl.BlockSpe...  17.8 us
    ppermute x11, starting transfers between devices, send(): return lax.ppermute(array, 'tp', pairs)  16.2 us
    all_to_all x1, starting transfers between devices, run(): returned = lax.all_to_all(results, EP, 0, 0, tiled=True)  14.9 us
  transfers between devices with their start and end apart: 19, of which 8 were waited for; matrix products, arithmetic and copies ran while one was open for 2% of the time, Pallas kernels for 7%

profile of v6, /device:TPU:33, one launch (start us, length us, event | category | flops | bytes accessed | tf_op | source)
XLA Modules:
  0.0 259.8 jit_solution(11683276264978863357)
XLA Ops:
  1.4 34.5 %dispatch.1 = (bf16[32,160,128]{2,1,0:T(8,128)(2,1)}, s32[2,160]{1,0:T(2,128)S(1)}, bf16[1024,256]{1,0:T(8,128)(2,1)}, bf16[1024,256]{1,0:T(8,128)(2,1)}) custom-call(s32[2]{0:T(128)S(1)} %pad_add_fusion.refs_0_, bf16[640,2048]{1,0:T(8,128)(2,1)} %refs_1_.1, f32[1,2048]{1,0:T(1,128)} %bitcast.23, s32[2,160]{1,0:T(2,128)S(1)} %dynamic-slice_bitcast_fusion.refs_3_, ...), custom_call_target="tpu_custom_call" | custom-call | tf_op jit(solution)/shard_map/dispatch/pallas_call | solution.py:144
  36.0 25.6 %all-to-all-start = ((bf16[32,160,128]{2,1,0:T(8,128)(2,1)}), bf16[32,160,128]{2,1,0:T(8,128)(2,1)S(1)}, u32[]{:S(2)}, u32[]{:S(2)}) async-start(bf16[32,160,128]{2,1,0:T(8,128)(2,1)} %get-tuple-element.6), calls=%async_computation | async-start | bytes 2621440 | tf_op jit(solution)/shard_map/all_to_all | solution.py:519
  63.0 1.7 collective-permute-start.6
  64.7 2.7 %collective-permute-start.7 = (bf16[1024,256]{1,0:T(8,128)(2,1)S(1)}, bf16[1024,256]{1,0:T(8,128)(2,1)S(1)}, u32[]{:S(2)}, u32[]{:S(2)}) collective-permute-start(bf16[1024,256]{1,0:T(8,128)(2,1)S(1)} %copy-done.18), channel_id=1, source_target_pairs={{0,3},{1,0},{2,1},{3,2},{4,7},{5,4},{6,5},{7,6},{8,11},{9,8},{10,9... | collective-permute-start | bytes 1572872 | tf_op jit(solution)/shard_map/ppermute | solution.py:500
  67.4 8.1 %collective-permute-done.6.refs_10_ = bf16[1024,256]{1,0:T(8,128)(2,1)S(1)} collective-permute-done((bf16[1024,256]{1,0:T(8,128)(2,1)S(1)}, bf16[1024,256]{1,0:T(8,128)(2,1)S(1)}, u32[]{:S(2)}, u32[]{:S(2)}) %collective-permute-start.6) | collective-permute-done | bytes 524320 | tf_op jit(solution)/shard_map/ppermute | solution.py:500
  75.5 3.2 %collective-permute-start.10 = (bf16[256,2048]{1,0:T(8,128)(2,1)}, bf16[256,2048]{1,0:T(8,128)(2,1)S(1)}, u32[]{:S(2)}, u32[]{:S(2)}) collective-permute-start(bf16[256,2048]{1,0:T(8,128)(2,1)} %bitcast.7.refs_4_), channel_id=1, source_target_pairs={{0,3},{1,0},{2,1},{3,2},{4,7},{5,4},{6,5},{7,6},{8,11},{9,8},{10,9... | collective-permute-start | bytes 3145736 | tf_op jit(solution)/shard_map/ppermute | solution.py:500
  78.7 20.1 %collective-permute-done.2.refs_6_ = bf16[1024,256]{1,0:T(8,128)(2,1)S(1)} collective-permute-done((bf16[1024,256]{1,0:T(8,128)(2,1)S(1)}, bf16[1024,256]{1,0:T(8,128)(2,1)S(1)}, u32[]{:S(2)}, u32[]{:S(2)}) %collective-permute-start.2) | collective-permute-done | bytes 524320 | tf_op jit(solution)/shard_map/ppermute | solution.py:500
  100.0 1.8 collective-permute-start.4
  101.9 8.2 %collective-permute-done.1.refs_5_ = bf16[1024,256]{1,0:T(8,128)(2,1)S(1)} collective-permute-done((bf16[1024,256]{1,0:T(8,128)(2,1)S(1)}, bf16[1024,256]{1,0:T(8,128)(2,1)S(1)}, u32[]{:S(2)}, u32[]{:S(2)}) %collective-permute-start.1) | collective-permute-done | bytes 524320 | tf_op jit(solution)/shard_map/ppermute | solution.py:500
  111.3 1.8 collective-permute-start.3
  113.2 7.3 %collective-permute-done.11.refs_15_ = bf16[1024,256]{1,0:T(8,128)(2,1)S(1)} collective-permute-done((bf16[1024,256]{1,0:T(8,128)(2,1)S(1)}, bf16[1024,256]{1,0:T(8,128)(2,1)S(1)}, u32[]{:S(2)}, u32[]{:S(2)}) %collective-permute-start.11) | collective-permute-done | bytes 524320 | tf_op jit(solution)/shard_map/ppermute | solution.py:500
  121.8 1.8 collective-permute-start.8
  123.7 8.0 %collective-permute-done.12.refs_16_ = bf16[1024,256]{1,0:T(8,128)(2,1)S(1)} collective-permute-done((bf16[1024,256]{1,0:T(8,128)(2,1)S(1)}, bf16[1024,256]{1,0:T(8,128)(2,1)S(1)}, u32[]{:S(2)}, u32[]{:S(2)}) %collective-permute-start.12) | collective-permute-done | bytes 524320 | tf_op jit(solution)/shard_map/ppermute | solution.py:500
  131.7 1.8 collective-permute-start.9
  135.2 2.0 collective-permute-start.16
  137.2 8.8 %collective-permute-done.9.refs_13_ = bf16[1024,256]{1,0:T(8,128)(2,1)S(1)} collective-permute-done((bf16[1024,256]{1,0:T(8,128)(2,1)S(1)}, bf16[1024,256]{1,0:T(8,128)(2,1)S(1)}, u32[]{:S(2)}, u32[]{:S(2)}) %collective-permute-start.9) | collective-permute-done | bytes 524320 | tf_op jit(solution)/shard_map/ppermute | solution.py:503
  146.0 11.2 %collective-permute-done.13.refs_17_ = bf16[1024,256]{1,0:T(8,128)(2,1)S(1)} collective-permute-done((bf16[1024,256]{1,0:T(8,128)(2,1)S(1)}, bf16[1024,256]{1,0:T(8,128)(2,1)S(1)}, u32[]{:S(2)}, u32[]{:S(2)}) %collective-permute-start.13) | collective-permute-done | bytes 524320 | tf_op jit(solution)/shard_map/ppermute | solution.py:503
  157.4 8.9 %experts.1 = bf16[32,160,128]{2,1,0:T(8,128)(2,1)} custom-call(s32[1]{0:T(128)} %bitcast.1.refs_0_, bf16[32,160,128]{2,1,0:T(8,128)(2,1)S(1)} %all-to-all-done.refs_1_, bf16[2048,256]{1,0:T(8,128)(2,1)} %bitcast.18, bf16[2048,256]{1,0:T(8,128)(2,1)} %bitcast.20, bf16[256,2048]{1,0:T(8,128)(2,1)} %bitcast.7.refs_4_, bf16[1024,256]{1,0:T(8,128)(2,1)} %copy-done.10, ...), custom_call_target="tpu_custom_call" | custom-call | tf_op jit(solution)/shard_map/experts/pallas_call | solution.py:314
  166.3 14.9 %all-to-all-start.1 = ((bf16[32,160,128]{2,1,0:T(8,128)(2,1)}), bf16[32,160,128]{2,1,0:T(8,128)(2,1)S(1)}, u32[]{:S(2)}, u32[]{:S(2)}) async-start(bf16[32,160,128]{2,1,0:T(8,128)(2,1)} %experts.1), calls=%async_computation.1 | async-start | bytes 2621440 | tf_op jit(solution)/shard_map/all_to_all | solution.py:548
  182.8 3.6 %collective-permute-start = (bf16[32,2048]{1,0:T(8,128)(2,1)}, bf16[32,2048]{1,0:T(8,128)(2,1)}, u32[]{:S(2)}, u32[]{:S(2)}) collective-permute-start(bf16[32,2048]{1,0:T(8,128)(2,1)} %slice.9), channel_id=1, source_target_pairs={{0,4},{4,8},{8,12},{12,16},{16,20},{20,24},{24,28},{28,32},{32,36}... | collective-permute-start | bytes 393224 | tf_op jit(solution)/shard_map/ppermute | solution.py:524
  189.0 47.6 %collective-permute-done.carried_ref = bf16[32,2048]{1,0:T(8,128)(2,1)} collective-permute-done((bf16[32,2048]{1,0:T(8,128)(2,1)}, bf16[32,2048]{1,0:T(8,128)(2,1)}, u32[]{:S(2)}, u32[]{:S(2)}) %collective-permute-start) | collective-permute-done | bytes 131104 | tf_op jit(solution)/shard_map/ppermute | solution.py:524
  236.6 1.7 copy-done.1
  238.3 17.8 %conv.1 = bf16[640,512]{1,0:T(8,128)(2,1)} custom-call(bf16[640,2048]{1,0:T(8,128)(2,1)S(1)} %copy-done.1, bf16[32,2048]{1,0:T(8,128)(2,1)} %collective-permute-done.carried_ref, f32[31,16,128]{2,1,0:T(8,128)S(1)} %slice.14.taps_ref, f32[1,2048]{1,0:T(1,128)S(1)} %bitcast.15, bf16[2048,512]{1,0:T(8,128)(2,1)S(1)} %copy-done.2), custom_call_target="tpu_custom_call" | custom-call | tf_op jit(solution)/shard_map/conv/pallas_call | solution.py:443
  256.1 3.5 %combine.1 = bf16[160,2048]{1,0:T(8,128)(2,1)} custom-call(bf16[32,160,128]{2,1,0:T(8,128)(2,1)S(1)} %all-to-all-done.1.refs_0_, s32[160,2]{1,0:T(8,128)S(1)} %bitcast.14, f32[160,2]{1,0:T(8,128)} %copy.16.refs_2_, f32[1,2048]{1,0:T(1,128)S(1)} %bitcast.16), custom_call_target="tpu_custom_call" | custom-call | tf_op jit(solution)/shard_map/combine/pallas_call | solution.py:378
  (66 shorter events, 12.0 us)
Async XLA Ops:
  36.0 121.4 %all-to-all-start = ((bf16[32,160,128]{2,1,0:T(8,128)(2,1)}), bf16[32,160,128]{2,1,0:T(8,128)(2,1)S(1)}, u32[]{:S(2)}, u32[]{:S(2)}) async-start(bf16[32,160,128]{2,1,0:T(8,128)(2,1)} %get-tuple-element.6), calls=%async_computation | async-start | bytes 2621440 | tf_op jit(solution)/shard_map/all_to_all | solution.py:519
  61.6 49.7 %collective-permute-start.5 = (bf16[256,2048]{1,0:T(8,128)(2,1)}, bf16[256,2048]{1,0:T(8,128)(2,1)S(1)}, u32[]{:S(2)}, u32[]{:S(2)}) collective-permute-start(bf16[256,2048]{1,0:T(8,128)(2,1)} %bitcast.7.refs_4_), channel_id=1, source_target_pairs={{0,1},{1,2},{2,3},{3,0},{4,5},{5,6},{6,7},{7,4},{8,9},{9,10},{10,1... | collective-permute-start | bytes 3145736 | tf_op jit(solution)/shard_map/ppermute | solution.py:500
  63.0 12.5 %collective-permute-start.6 = (bf16[1024,256]{1,0:T(8,128)(2,1)S(1)}, bf16[1024,256]{1,0:T(8,128)(2,1)S(1)}, u32[]{:S(2)}, u32[]{:S(2)}) collective-permute-start(bf16[1024,256]{1,0:T(8,128)(2,1)S(1)} %copy-done.17), channel_id=1, source_target_pairs={{0,3},{1,0},{2,1},{3,2},{4,7},{5,4},{6,5},{7,6},{8,11},{9,8},{10,9... | collective-permute-start | bytes 1572872 | tf_op jit(solution)/shard_map/ppermute | solution.py:500
  64.7 34.1 %collective-permute-start.2 = (bf16[1024,256]{1,0:T(8,128)(2,1)S(1)}, bf16[1024,256]{1,0:T(8,128)(2,1)S(1)}, u32[]{:S(2)}, u32[]{:S(2)}) collective-permute-start(bf16[1024,256]{1,0:T(8,128)(2,1)S(1)} %copy-done.18), channel_id=1, source_target_pairs={{0,1},{1,2},{2,3},{3,0},{4,5},{5,6},{6,7},{7,4},{8,9},{9,10},{10,1... | collective-permute-start | bytes 1572872 | tf_op jit(solution)/shard_map/ppermute | solution.py:500
  64.7 35.3 %collective-permute-start.7 = (bf16[1024,256]{1,0:T(8,128)(2,1)S(1)}, bf16[1024,256]{1,0:T(8,128)(2,1)S(1)}, u32[]{:S(2)}, u32[]{:S(2)}) collective-permute-start(bf16[1024,256]{1,0:T(8,128)(2,1)S(1)} %copy-done.18), channel_id=1, source_target_pairs={{0,3},{1,0},{2,1},{3,2},{4,7},{5,4},{6,5},{7,6},{8,11},{9,8},{10,9... | collective-permute-start | bytes 1572872 | tf_op jit(solution)/shard_map/ppermute | solution.py:500
  67.4 42.7 %collective-permute-start.1 = (bf16[1024,256]{1,0:T(8,128)(2,1)S(1)}, bf16[1024,256]{1,0:T(8,128)(2,1)S(1)}, u32[]{:S(2)}, u32[]{:S(2)}) collective-permute-start(bf16[1024,256]{1,0:T(8,128)(2,1)S(1)} %copy-done.17), channel_id=1, source_target_pairs={{0,1},{1,2},{2,3},{3,0},{4,5},{5,6},{6,7},{7,4},{8,9},{9,10},{10,1... | collective-permute-start | bytes 1572872 | tf_op jit(solution)/shard_map/ppermute | solution.py:500
  75.5 81.7 %copy-start.7 = (bf16[1024,256]{1,0:T(8,128)(2,1)}, bf16[1024,256]{1,0:T(8,128)(2,1)S(1)}, u32[]{:S(2)}) copy-start(bf16[1024,256]{1,0:T(8,128)(2,1)S(1)} %collective-permute-done.6.refs_10_) | copy-start | bytes 1572868
  75.5 58.2 %collective-permute-start.10 = (bf16[256,2048]{1,0:T(8,128)(2,1)}, bf16[256,2048]{1,0:T(8,128)(2,1)S(1)}, u32[]{:S(2)}, u32[]{:S(2)}) collective-permute-start(bf16[256,2048]{1,0:T(8,128)(2,1)} %bitcast.7.refs_4_), channel_id=1, source_target_pairs={{0,3},{1,0},{2,1},{3,2},{4,7},{5,4},{6,5},{7,6},{8,11},{9,8},{10,9... | collective-permute-start | bytes 3145736 | tf_op jit(solution)/shard_map/ppermute | solution.py:500
  98.8 21.7 %collective-permute-start.11 = (bf16[1024,256]{1,0:T(8,128)(2,1)S(1)}, bf16[1024,256]{1,0:T(8,128)(2,1)S(1)}, u32[]{:S(2)}, u32[]{:S(2)}) collective-permute-start(bf16[1024,256]{1,0:T(8,128)(2,1)S(1)} %collective-permute-done.6.refs_10_), channel_id=1, source_target_pairs={{0,3},{1,0},{2,1},{3,2},{4,7},{5,4},{6,5},{7,6},{8,11},{9,8},{10,9... | collective-permute-start | bytes 1572872 | tf_op jit(solution)/shard_map/ppermute | solution.py:500
  100.0 57.2 %copy-start.9 = (bf16[1024,256]{1,0:T(8,128)(2,1)}, bf16[1024,256]{1,0:T(8,128)(2,1)S(1)}, u32[]{:S(2)}) copy-start(bf16[1024,256]{1,0:T(8,128)(2,1)S(1)} %collective-permute-done.7.refs_11_) | copy-start | bytes 1572868
  100.0 21.8 %collective-permute-start.4 = (bf16[1024,256]{1,0:T(8,128)(2,1)S(1)}, bf16[1024,256]{1,0:T(8,128)(2,1)S(1)}, u32[]{:S(2)}, u32[]{:S(2)}) collective-permute-start(bf16[1024,256]{1,0:T(8,128)(2,1)S(1)} %collective-permute-done.2.refs_6_), channel_id=1, source_target_pairs={{0,128},{128,0},{1,129},{129,1},{2,130},{130,2},{3,131},{131,3},{4... | collective-permute-start | bytes 1572872 | tf_op jit(solution)/shard_map/ppermute | solution.py:503
  110.1 21.7 %collective-permute-start.12 = (bf16[1024,256]{1,0:T(8,128)(2,1)S(1)}, bf16[1024,256]{1,0:T(8,128)(2,1)S(1)}, u32[]{:S(2)}, u32[]{:S(2)}) collective-permute-start(bf16[1024,256]{1,0:T(8,128)(2,1)S(1)} %collective-permute-done.7.refs_11_), channel_id=1, source_target_pairs={{0,3},{1,0},{2,1},{3,2},{4,7},{5,4},{6,5},{7,6},{8,11},{9,8},{10,9... | collective-permute-start | bytes 1572872 | tf_op jit(solution)/shard_map/ppermute | solution.py:500
  111.3 22.3 %collective-permute-start.3 = (bf16[1024,256]{1,0:T(8,128)(2,1)S(1)}, bf16[1024,256]{1,0:T(8,128)(2,1)S(1)}, u32[]{:S(2)}, u32[]{:S(2)}) collective-permute-start(bf16[1024,256]{1,0:T(8,128)(2,1)S(1)} %collective-permute-done.1.refs_5_), channel_id=1, source_target_pairs={{0,128},{128,0},{1,129},{129,1},{2,130},{130,2},{3,131},{131,3},{4... | collective-permute-start | bytes 1572872 | tf_op jit(solution)/shard_map/ppermute | solution.py:503
  120.5 36.8 %copy-start.11 = (bf16[1024,256]{1,0:T(8,128)(2,1)}, bf16[1024,256]{1,0:T(8,128)(2,1)S(1)}, u32[]{:S(2)}) copy-start(bf16[1024,256]{1,0:T(8,128)(2,1)S(1)} %collective-permute-done.11.refs_15_) | copy-start | bytes 1572868
  120.5 36.9 %collective-permute-start.15 = (bf16[224,2048]{1,0:T(8,128)(2,1)S(1)}, bf16[224,2048]{1,0:T(8,128)(2,1)S(1)}, u32[]{:S(2)}, u32[]{:S(2)}) collective-permute-start(bf16[224,2048]{1,0:T(8,128)(2,1)S(1)} %slice.12), channel_id=1, source_target_pairs={{0,1},{1,2},{2,3},{3,0},{4,5},{5,6},{6,7},{7,4},{8,9},{9,10},{10,1... | collective-permute-start | bytes 2752520 | tf_op jit(solution)/shard_map/ppermute | solution.py:500
  121.8 13.4 %collective-permute-start.8 = (bf16[1024,256]{1,0:T(8,128)(2,1)S(1)}, bf16[1024,256]{1,0:T(8,128)(2,1)S(1)}, u32[]{:S(2)}, u32[]{:S(2)}) collective-permute-start(bf16[1024,256]{1,0:T(8,128)(2,1)S(1)} %collective-permute-done.6.refs_10_), channel_id=1, source_target_pairs={{0,128},{128,0},{1,129},{129,1},{2,130},{130,2},{3,131},{131,3},{4... | collective-permute-start | bytes 1572872 | tf_op jit(solution)/shard_map/ppermute | solution.py:503
  131.7 14.3 %collective-permute-start.9 = (bf16[1024,256]{1,0:T(8,128)(2,1)S(1)}, bf16[1024,256]{1,0:T(8,128)(2,1)S(1)}, u32[]{:S(2)}, u32[]{:S(2)}) collective-permute-start(bf16[1024,256]{1,0:T(8,128)(2,1)S(1)} %collective-permute-done.7.refs_11_), channel_id=1, source_target_pairs={{0,128},{128,0},{1,129},{129,1},{2,130},{130,2},{3,131},{131,3},{4... | collective-permute-start | bytes 1572872 | tf_op jit(solution)/shard_map/ppermute | solution.py:503
  133.6 23.7 %collective-permute-start.13 = (bf16[1024,256]{1,0:T(8,128)(2,1)S(1)}, bf16[1024,256]{1,0:T(8,128)(2,1)S(1)}, u32[]{:S(2)}, u32[]{:S(2)}) collective-permute-start(bf16[1024,256]{1,0:T(8,128)(2,1)S(1)} %collective-permute-done.11.refs_15_), channel_id=1, source_target_pairs={{0,128},{128,0},{1,129},{129,1},{2,130},{130,2},{3,131},{131,3},{4... | collective-permute-start | bytes 1572872 | tf_op jit(solution)/shard_map/ppermute | solution.py:503
  133.7 23.5 %collective-permute-start.14 = (bf16[1024,256]{1,0:T(8,128)(2,1)S(1)}, bf16[1024,256]{1,0:T(8,128)(2,1)S(1)}, u32[]{:S(2)}, u32[]{:S(2)}) collective-permute-start(bf16[1024,256]{1,0:T(8,128)(2,1)S(1)} %collective-permute-done.4.refs_8_), channel_id=1, source_target_pairs={{0,1},{1,2},{2,3},{3,0},{4,5},{5,6},{6,7},{7,4},{8,9},{9,10},{10,1... | collective-permute-start | bytes 1572872 | tf_op jit(solution)/shard_map/ppermute | solution.py:500
  135.2 10.8 %collective-permute-start.16 = (bf16[32,2048]{1,0:T(8,128)(2,1)S(1)}, bf16[32,2048]{1,0:T(8,128)(2,1)S(1)}, u32[]{:S(2)}, u32[]{:S(2)}) collective-permute-start(bf16[32,2048]{1,0:T(8,128)(2,1)S(1)} %slice.13), channel_id=1, source_target_pairs={{0,3},{1,0},{2,1},{3,2},{4,7},{5,4},{6,5},{7,6},{8,11},{9,8},{10,9... | collective-permute-start | bytes 393224 | tf_op jit(solution)/shard_map/ppermute | solution.py:500
  166.3 70.3 %copy-start.2 = (bf16[2048,512]{1,0:T(8,128)(2,1)S(1)}, bf16[2048,512]{1,0:T(8,128)(2,1)}, u32[]{:S(2)}) copy-start(bf16[2048,512]{1,0:T(8,128)(2,1)} %weight_ref.1) | copy-start | bytes 6291460
  166.3 89.8 %all-to-all-start.1 = ((bf16[32,160,128]{2,1,0:T(8,128)(2,1)}), bf16[32,160,128]{2,1,0:T(8,128)(2,1)S(1)}, u32[]{:S(2)}, u32[]{:S(2)}) async-start(bf16[32,160,128]{2,1,0:T(8,128)(2,1)} %experts.1), calls=%async_computation.1 | async-start | bytes 2621440 | tf_op jit(solution)/shard_map/all_to_all | solution.py:548
  181.2 55.4 %copy-start.3 = (f32[2048]{0:T(1024)S(1)}, f32[2048]{0:T(1024)}, u32[]{:S(2)}) copy-start(f32[2048]{0:T(1024)} %param.14) | copy-start | bytes 24580
  182.8 53.8 %collective-permute-start = (bf16[32,2048]{1,0:T(8,128)(2,1)}, bf16[32,2048]{1,0:T(8,128)(2,1)}, u32[]{:S(2)}, u32[]{:S(2)}) collective-permute-start(bf16[32,2048]{1,0:T(8,128)(2,1)} %slice.9), channel_id=1, source_target_pairs={{0,4},{4,8},{8,12},{12,16},{16,20},{20,24},{24,28},{28,32},{32,36}... | collective-permute-start | bytes 393224 | tf_op jit(solution)/shard_map/ppermute | solution.py:524
  (14 other events, 278.3 us)

commit v7 on v6

--- a/solution.py
+++ b/solution.py
@@ -144,7 +144,7 @@
     return pl.pallas_call(
         kernel,
         in_specs=[pl.BlockSpec(memory_space=pltpu.SMEM), hbm, hbm, whole(), hbm, hbm],
-        out_specs=[whole(), whole(), *(hbm for _ in cuts)],
+        out_specs=[whole()] * (2 + len(cuts)),
         scratch_shapes=[
             pltpu.VMEM((tokens, width), BF16),
             pltpu.VMEM(gain.shape, F32),
@@ -153,7 +153,7 @@
         out_shape=[
             jax.ShapeDtypeStruct((experts, capacity * width // LANES, LANES), BF16),
             jax.ShapeDtypeStruct((2, tokens), jnp.int32),
-            *(pltpu.HBM((cut, gate.shape[1]), BF16) for cut in cuts),
+            *(jax.ShapeDtypeStruct((cut, gate.shape[1]), BF16) for cut in cuts),
         ],
         compiler_params=pltpu.CompilerParams(vmem_limit_bytes=24 << 20),
         name="dispatch",
@@ -503,7 +503,14 @@
         return lax.ppermute(array, "grp", across)
 
     down_r = send(down, right)
+    turn = ep_count - ep_count // 4 - 1
+    order = [(turn - i) % ep_count for i in range(ep_count)]
+
+    def exchange(array):
+        return lax.all_to_all(array, EP, 0, 0, axis_index_groups=[order], tiled=True)
+
     own_ids = lax.dynamic_slice_in_dim(expert_ids, own * tokens, tokens, 0).T
+    own_ids = (turn + ep_count - own_ids) % ep_count
     message, target, mine_a, mine_b = dispatch(
         jnp.stack([own, odd]),
         moe_input,
@@ -516,7 +523,7 @@
         capacity,
     )
     mine_a_l, mine_b_l = send(mine_a, left), send(mine_b, left)
-    arrived = lax.all_to_all(message, EP, 0, 0, tiled=True)
+    arrived = exchange(message)
     mine_a_r, mine_b_r = send(mine_a, right), send(mine_b, right)
     other_a_l, mine_a_far = swap(mine_a_l), send(mine_a_l, left)
     down_l = send(down, left)
@@ -545,7 +552,7 @@
     )
     direct = tuple(n in (11, 12, 13) for n in range(len(matrices)))
     results = experts_apply(odd.reshape(1), arrived, matrices, direct, sources, capacity)
-    returned = lax.all_to_all(results, EP, 0, 0, tiled=True)
+    returned = exchange(results)
     own_weights = lax.dynamic_slice_in_dim(route_weights, own * tokens, tokens, 0)
     moe_out = combine(returned, target.T, own_weights, post_gain.reshape(1, width), capacity)
     return (conv_out, moe_out)

time: 260 us -> 237 us (0.912)
  Pallas kernels: 64.7 us -> 34.2 us
  waiting for transfers between devices: 119 us -> 123 us
  starting transfers between devices: 67.8 us -> 71.7 us
    pallas_call x1, Pallas kernels: 34.5 us -> 3.99 us  [dispatch(): pl.pallas_call(kernel, in_specs=[pl.BlockSpec(memory_space=pltpu.SMEM), h...]
    all_to_all x2, starting transfers between devices: 40.5 us -> 44.6 us  [exchange(): lax.all_to_all(array, EP, 0, 0, axis_index_groups=[order], tiled=True)]
    ppermute x1, waiting for transfers between devices: 47.6 us -> 51.1 us  [run(): carried = lax.ppermute(conv_input[conv_input.shape[0] - HALO:], EP, pairs)]
  transfers between devices with their start and end apart: 19 -> 19, of which waited for: 8 -> 8; matrix products, arithmetic and copies ran while one was open for 2% -> 2% of each run, Pallas kernels for 7% -> 8%
where the time goes in v7:
time: 237 us; the launch traced here: 236 us
  waiting for transfers between devices  123 us (52%)
  starting transfers between devices  71.7 us (30%)
  Pallas kernels  34.2 us (14%)
  local copies, waits for them, and re-layouts  5.44 us (2%)
    ppermute x11, waiting for transfers between devices, send(): return lax.ppermute(array, 'tp', pairs)  52 us
    ppermute x1, waiting for transfers between devices, run(): carried = lax.ppermute(conv_input[conv_input.shape[0] - HALO:], EP, pairs)  51.1 us
    all_to_all x2, starting transfers between devices, exchange(): lax.all_to_all(array, EP, 0, 0, axis_index_groups=[order], tiled=True)  44.6 us
    ppermute x5, waiting for transfers between devices, swap(): return lax.ppermute(array, 'grp', across)  20.1 us
    pallas_call x1, Pallas kernels, conv_module(): pl.pallas_call(conv_kernel, grid=(count // block,), in_specs=[pl.BlockSpe...  17.8 us
    ppermute x11, starting transfers between devices, send(): return lax.ppermute(array, 'tp', pairs)  16.2 us
    pallas_call x1, Pallas kernels, experts_apply(): pl.pallas_call(kernel, in_specs=[pl.BlockSpec(memory_space=pltpu.SMEM), w...  8.86 us
    ppermute x5, starting transfers between devices, swap(): return lax.ppermute(array, 'grp', across)  7.5 us
  transfers between devices with their start and end apart: 19, of which 8 were waited for; matrix products, arithmetic and copies ran while one was open for 2% of the time, Pallas kernels for 8%

profile of v7, /device:TPU:33, one launch (start us, length us, event | category | flops | bytes accessed | tf_op | source)
XLA Modules:
  0.0 236.4 jit_solution(3584946656570035036)
XLA Ops:
  1.5 4.0 %dispatch.1 = (bf16[32,160,128]{2,1,0:T(8,128)(2,1)}, s32[2,160]{1,0:T(2,128)S(1)}, bf16[1024,256]{1,0:T(8,128)(2,1)S(1)}, bf16[1024,256]{1,0:T(8,128)(2,1)S(1)}) custom-call(s32[2]{0:T(128)S(1)} %pad_add_fusion.refs_0_, bf16[640,2048]{1,0:T(8,128)(2,1)} %refs_1_.1, f32[1,2048]{1,0:T(1,128)} %bitcast.23, s32[2,160]{1,0:T(2,128)S(1)} %and_select_fusion.refs_3_, ...), custom_call_target="tpu_custom_call" | custom-call | tf_op jit(solution)/shard_map/dispatch/pallas_call | solution.py:144
  5.5 30.3 %all-to-all-start = ((bf16[32,160,128]{2,1,0:T(8,128)(2,1)}), bf16[32,160,128]{2,1,0:T(8,128)(2,1)S(1)}, u32[]{:S(2)}, u32[]{:S(2)}) async-start(bf16[32,160,128]{2,1,0:T(8,128)(2,1)} %get-tuple-element.6), calls=%async_computation | async-start | bytes 2621440 | tf_op jit(solution)/shard_map/all_to_all | solution.py:510
  37.2 1.7 collective-permute-start.6
  38.9 2.7 %collective-permute-start.7 = (bf16[1024,256]{1,0:T(8,128)(2,1)S(1)}, bf16[1024,256]{1,0:T(8,128)(2,1)S(1)}, u32[]{:S(2)}, u32[]{:S(2)}) collective-permute-start(bf16[1024,256]{1,0:T(8,128)(2,1)S(1)} %get-tuple-element.8), channel_id=1, source_target_pairs={{0,3},{1,0},{2,1},{3,2},{4,7},{5,4},{6,5},{7,6},{8,11},{9,8},{10,9... | collective-permute-start | bytes 1572872 | tf_op jit(solution)/shard_map/ppermute | solution.py:500
  41.6 8.4 %collective-permute-done.6.refs_10_ = bf16[1024,256]{1,0:T(8,128)(2,1)S(1)} collective-permute-done((bf16[1024,256]{1,0:T(8,128)(2,1)S(1)}, bf16[1024,256]{1,0:T(8,128)(2,1)S(1)}, u32[]{:S(2)}, u32[]{:S(2)}) %collective-permute-start.6) | collective-permute-done | bytes 524320 | tf_op jit(solution)/shard_map/ppermute | solution.py:500
  50.0 3.2 %collective-permute-start.10 = (bf16[256,2048]{1,0:T(8,128)(2,1)}, bf16[256,2048]{1,0:T(8,128)(2,1)S(1)}, u32[]{:S(2)}, u32[]{:S(2)}) collective-permute-start(bf16[256,2048]{1,0:T(8,128)(2,1)} %bitcast.7.refs_4_), channel_id=1, source_target_pairs={{0,3},{1,0},{2,1},{3,2},{4,7},{5,4},{6,5},{7,6},{8,11},{9,8},{10,9... | collective-permute-start | bytes 3145736 | tf_op jit(solution)/shard_map/ppermute | solution.py:500
  53.2 20.1 %collective-permute-done.2.refs_6_ = bf16[1024,256]{1,0:T(8,128)(2,1)S(1)} collective-permute-done((bf16[1024,256]{1,0:T(8,128)(2,1)S(1)}, bf16[1024,256]{1,0:T(8,128)(2,1)S(1)}, u32[]{:S(2)}, u32[]{:S(2)}) %collective-permute-start.2) | collective-permute-done | bytes 524320 | tf_op jit(solution)/shard_map/ppermute | solution.py:500
  74.5 1.8 collective-permute-start.4
  76.4 8.2 %collective-permute-done.1.refs_5_ = bf16[1024,256]{1,0:T(8,128)(2,1)S(1)} collective-permute-done((bf16[1024,256]{1,0:T(8,128)(2,1)S(1)}, bf16[1024,256]{1,0:T(8,128)(2,1)S(1)}, u32[]{:S(2)}, u32[]{:S(2)}) %collective-permute-start.1) | collective-permute-done | bytes 524320 | tf_op jit(solution)/shard_map/ppermute | solution.py:500
  85.7 1.8 collective-permute-start.3
  87.7 7.3 %collective-permute-done.11.refs_15_ = bf16[1024,256]{1,0:T(8,128)(2,1)S(1)} collective-permute-done((bf16[1024,256]{1,0:T(8,128)(2,1)S(1)}, bf16[1024,256]{1,0:T(8,128)(2,1)S(1)}, u32[]{:S(2)}, u32[]{:S(2)}) %collective-permute-start.11) | collective-permute-done | bytes 524320 | tf_op jit(solution)/shard_map/ppermute | solution.py:500
  96.3 1.8 collective-permute-start.8
  98.1 8.0 %collective-permute-done.12.refs_16_ = bf16[1024,256]{1,0:T(8,128)(2,1)S(1)} collective-permute-done((bf16[1024,256]{1,0:T(8,128)(2,1)S(1)}, bf16[1024,256]{1,0:T(8,128)(2,1)S(1)}, u32[]{:S(2)}, u32[]{:S(2)}) %collective-permute-start.12) | collective-permute-done | bytes 524320 | tf_op jit(solution)/shard_map/ppermute | solution.py:500
  106.2 1.8 collective-permute-start.9
  109.7 2.0 collective-permute-start.16
  111.7 8.8 %collective-permute-done.9.refs_13_ = bf16[1024,256]{1,0:T(8,128)(2,1)S(1)} collective-permute-done((bf16[1024,256]{1,0:T(8,128)(2,1)S(1)}, bf16[1024,256]{1,0:T(8,128)(2,1)S(1)}, u32[]{:S(2)}, u32[]{:S(2)}) %collective-permute-start.9) | collective-permute-done | bytes 524320 | tf_op jit(solution)/shard_map/ppermute | solution.py:503
  120.5 11.2 %collective-permute-done.13.refs_17_ = bf16[1024,256]{1,0:T(8,128)(2,1)S(1)} collective-permute-done((bf16[1024,256]{1,0:T(8,128)(2,1)S(1)}, bf16[1024,256]{1,0:T(8,128)(2,1)S(1)}, u32[]{:S(2)}, u32[]{:S(2)}) %collective-permute-start.13) | collective-permute-done | bytes 524320 | tf_op jit(solution)/shard_map/ppermute | solution.py:503
  131.9 8.9 %experts.1 = bf16[32,160,128]{2,1,0:T(8,128)(2,1)} custom-call(s32[1]{0:T(128)} %bitcast.1.refs_0_, bf16[32,160,128]{2,1,0:T(8,128)(2,1)S(1)} %all-to-all-done.refs_1_, bf16[2048,256]{1,0:T(8,128)(2,1)} %bitcast.18, bf16[2048,256]{1,0:T(8,128)(2,1)} %bitcast.20, bf16[256,2048]{1,0:T(8,128)(2,1)} %bitcast.7.refs_4_, bf16[1024,256]{1,0:T(8,128)(2,1)} %copy-done.10, ...), custom_call_target="tpu_custom_call" | custom-call | tf_op jit(solution)/shard_map/experts/pallas_call | solution.py:314
  140.7 14.3 %all-to-all-start.1 = ((bf16[32,160,128]{2,1,0:T(8,128)(2,1)}), bf16[32,160,128]{2,1,0:T(8,128)(2,1)S(1)}, u32[]{:S(2)}, u32[]{:S(2)}) async-start(bf16[32,160,128]{2,1,0:T(8,128)(2,1)} %experts.1), calls=%async_computation.1 | async-start | bytes 2621440 | tf_op jit(solution)/shard_map/all_to_all | solution.py:510
  156.7 3.4 %collective-permute-start = (bf16[32,2048]{1,0:T(8,128)(2,1)}, bf16[32,2048]{1,0:T(8,128)(2,1)}, u32[]{:S(2)}, u32[]{:S(2)}) collective-permute-start(bf16[32,2048]{1,0:T(8,128)(2,1)} %slice.9), channel_id=1, source_target_pairs={{0,4},{4,8},{8,12},{12,16},{16,20},{20,24},{24,28},{28,32},{32,36}... | collective-permute-start | bytes 393224 | tf_op jit(solution)/shard_map/ppermute | solution.py:531
  162.0 51.1 %collective-permute-done.carried_ref = bf16[32,2048]{1,0:T(8,128)(2,1)} collective-permute-done((bf16[32,2048]{1,0:T(8,128)(2,1)}, bf16[32,2048]{1,0:T(8,128)(2,1)}, u32[]{:S(2)}, u32[]{:S(2)}) %collective-permute-start) | collective-permute-done | bytes 131104 | tf_op jit(solution)/shard_map/ppermute | solution.py:531
  213.2 1.7 copy-done.1
  214.9 17.8 %conv.1 = bf16[640,512]{1,0:T(8,128)(2,1)} custom-call(bf16[640,2048]{1,0:T(8,128)(2,1)S(1)} %copy-done.1, bf16[32,2048]{1,0:T(8,128)(2,1)} %collective-permute-done.carried_ref, f32[31,16,128]{2,1,0:T(8,128)S(1)} %slice.14.taps_ref, f32[1,2048]{1,0:T(1,128)S(1)} %bitcast.15, bf16[2048,512]{1,0:T(8,128)(2,1)S(1)} %copy-done.2), custom_call_target="tpu_custom_call" | custom-call | tf_op jit(solution)/shard_map/conv/pallas_call | solution.py:443
  232.7 3.5 %combine.1 = bf16[160,2048]{1,0:T(8,128)(2,1)} custom-call(bf16[32,160,128]{2,1,0:T(8,128)(2,1)S(1)} %all-to-all-done.1.refs_0_, s32[160,2]{1,0:T(8,128)S(1)} %bitcast.14, f32[160,2]{1,0:T(8,128)} %copy.16.refs_2_, f32[1,2048]{1,0:T(1,128)S(1)} %bitcast.16), custom_call_target="tpu_custom_call" | custom-call | tf_op jit(solution)/shard_map/combine/pallas_call | solution.py:378
  (62 shorter events, 11.4 us)
Async XLA Ops:
  0.6 159.5 %copy-start = (f32[640,2]{0,1:T(2,128)S(1)}, f32[640,2]{0,1:T(2,128)}, u32[]{:S(2)}) copy-start(f32[640,2]{0,1:T(2,128)} %param.19) | copy-start | bytes 15364
  5.5 126.4 %all-to-all-start = ((bf16[32,160,128]{2,1,0:T(8,128)(2,1)}), bf16[32,160,128]{2,1,0:T(8,128)(2,1)S(1)}, u32[]{:S(2)}, u32[]{:S(2)}) async-start(bf16[32,160,128]{2,1,0:T(8,128)(2,1)} %get-tuple-element.6), calls=%async_computation | async-start | bytes 2621440 | tf_op jit(solution)/shard_map/all_to_all | solution.py:510
  35.8 50.0 %collective-permute-start.5 = (bf16[256,2048]{1,0:T(8,128)(2,1)}, bf16[256,2048]{1,0:T(8,128)(2,1)S(1)}, u32[]{:S(2)}, u32[]{:S(2)}) collective-permute-start(bf16[256,2048]{1,0:T(8,128)(2,1)} %bitcast.7.refs_4_), channel_id=1, source_target_pairs={{0,1},{1,2},{2,3},{3,0},{4,5},{5,6},{6,7},{7,4},{8,9},{9,10},{10,1... | collective-permute-start | bytes 3145736 | tf_op jit(solution)/shard_map/ppermute | solution.py:500
  37.2 12.8 %collective-permute-start.6 = (bf16[1024,256]{1,0:T(8,128)(2,1)S(1)}, bf16[1024,256]{1,0:T(8,128)(2,1)S(1)}, u32[]{:S(2)}, u32[]{:S(2)}) collective-permute-start(bf16[1024,256]{1,0:T(8,128)(2,1)S(1)} %get-tuple-element.7), channel_id=1, source_target_pairs={{0,3},{1,0},{2,1},{3,2},{4,7},{5,4},{6,5},{7,6},{8,11},{9,8},{10,9... | collective-permute-start | bytes 1572872 | tf_op jit(solution)/shard_map/ppermute | solution.py:500
  38.9 34.4 %collective-permute-start.2 = (bf16[1024,256]{1,0:T(8,128)(2,1)S(1)}, bf16[1024,256]{1,0:T(8,128)(2,1)S(1)}, u32[]{:S(2)}, u32[]{:S(2)}) collective-permute-start(bf16[1024,256]{1,0:T(8,128)(2,1)S(1)} %get-tuple-element.8), channel_id=1, source_target_pairs={{0,1},{1,2},{2,3},{3,0},{4,5},{5,6},{6,7},{7,4},{8,9},{9,10},{10,1... | collective-permute-start | bytes 1572872 | tf_op jit(solution)/shard_map/ppermute | solution.py:500
  38.9 35.6 %collective-permute-start.7 = (bf16[1024,256]{1,0:T(8,128)(2,1)S(1)}, bf16[1024,256]{1,0:T(8,128)(2,1)S(1)}, u32[]{:S(2)}, u32[]{:S(2)}) collective-permute-start(bf16[1024,256]{1,0:T(8,128)(2,1)S(1)} %get-tuple-element.8), channel_id=1, source_target_pairs={{0,3},{1,0},{2,1},{3,2},{4,7},{5,4},{6,5},{7,6},{8,11},{9,8},{10,9... | collective-permute-start | bytes 1572872 | tf_op jit(solution)/shard_map/ppermute | solution.py:500
  41.6 42.9 %collective-permute-start.1 = (bf16[1024,256]{1,0:T(8,128)(2,1)S(1)}, bf16[1024,256]{1,0:T(8,128)(2,1)S(1)}, u32[]{:S(2)}, u32[]{:S(2)}) collective-permute-start(bf16[1024,256]{1,0:T(8,128)(2,1)S(1)} %get-tuple-element.7), channel_id=1, source_target_pairs={{0,1},{1,2},{2,3},{3,0},{4,5},{5,6},{6,7},{7,4},{8,9},{9,10},{10,1... | collective-permute-start | bytes 1572872 | tf_op jit(solution)/shard_map/ppermute | solution.py:500
  50.0 81.7 %copy-start.7 = (bf16[1024,256]{1,0:T(8,128)(2,1)}, bf16[1024,256]{1,0:T(8,128)(2,1)S(1)}, u32[]{:S(2)}) copy-start(bf16[1024,256]{1,0:T(8,128)(2,1)S(1)} %collective-permute-done.6.refs_10_) | copy-start | bytes 1572868
  50.0 58.2 %collective-permute-start.10 = (bf16[256,2048]{1,0:T(8,128)(2,1)}, bf16[256,2048]{1,0:T(8,128)(2,1)S(1)}, u32[]{:S(2)}, u32[]{:S(2)}) collective-permute-start(bf16[256,2048]{1,0:T(8,128)(2,1)} %bitcast.7.refs_4_), channel_id=1, source_target_pairs={{0,3},{1,0},{2,1},{3,2},{4,7},{5,4},{6,5},{7,6},{8,11},{9,8},{10,9... | collective-permute-start | bytes 3145736 | tf_op jit(solution)/shard_map/ppermute | solution.py:500
  73.3 58.5 %copy-start.8 = (bf16[1024,256]{1,0:T(8,128)(2,1)}, bf16[1024,256]{1,0:T(8,128)(2,1)S(1)}, u32[]{:S(2)}) copy-start(bf16[1024,256]{1,0:T(8,128)(2,1)S(1)} %collective-permute-done.2.refs_6_) | copy-start | bytes 1572868
  73.3 21.7 %collective-permute-start.11 = (bf16[1024,256]{1,0:T(8,128)(2,1)S(1)}, bf16[1024,256]{1,0:T(8,128)(2,1)S(1)}, u32[]{:S(2)}, u32[]{:S(2)}) collective-permute-start(bf16[1024,256]{1,0:T(8,128)(2,1)S(1)} %collective-permute-done.6.refs_10_), channel_id=1, source_target_pairs={{0,3},{1,0},{2,1},{3,2},{4,7},{5,4},{6,5},{7,6},{8,11},{9,8},{10,9... | collective-permute-start | bytes 1572872 | tf_op jit(solution)/shard_map/ppermute | solution.py:500
  74.5 21.8 %collective-permute-start.4 = (bf16[1024,256]{1,0:T(8,128)(2,1)S(1)}, bf16[1024,256]{1,0:T(8,128)(2,1)S(1)}, u32[]{:S(2)}, u32[]{:S(2)}) collective-permute-start(bf16[1024,256]{1,0:T(8,128)(2,1)S(1)} %collective-permute-done.2.refs_6_), channel_id=1, source_target_pairs={{0,128},{128,0},{1,129},{129,1},{2,130},{130,2},{3,131},{131,3},{4... | collective-permute-start | bytes 1572872 | tf_op jit(solution)/shard_map/ppermute | solution.py:503
  84.5 21.7 %collective-permute-start.12 = (bf16[1024,256]{1,0:T(8,128)(2,1)S(1)}, bf16[1024,256]{1,0:T(8,128)(2,1)S(1)}, u32[]{:S(2)}, u32[]{:S(2)}) collective-permute-start(bf16[1024,256]{1,0:T(8,128)(2,1)S(1)} %collective-permute-done.7.refs_11_), channel_id=1, source_target_pairs={{0,3},{1,0},{2,1},{3,2},{4,7},{5,4},{6,5},{7,6},{8,11},{9,8},{10,9... | collective-permute-start | bytes 1572872 | tf_op jit(solution)/shard_map/ppermute | solution.py:500
  85.7 22.3 %collective-permute-start.3 = (bf16[1024,256]{1,0:T(8,128)(2,1)S(1)}, bf16[1024,256]{1,0:T(8,128)(2,1)S(1)}, u32[]{:S(2)}, u32[]{:S(2)}) collective-permute-start(bf16[1024,256]{1,0:T(8,128)(2,1)S(1)} %collective-permute-done.1.refs_5_), channel_id=1, source_target_pairs={{0,128},{128,0},{1,129},{129,1},{2,130},{130,2},{3,131},{131,3},{4... | collective-permute-start | bytes 1572872 | tf_op jit(solution)/shard_map/ppermute | solution.py:503
  94.9 36.9 %collective-permute-start.15 = (bf16[224,2048]{1,0:T(8,128)(2,1)S(1)}, bf16[224,2048]{1,0:T(8,128)(2,1)S(1)}, u32[]{:S(2)}, u32[]{:S(2)}) collective-permute-start(bf16[224,2048]{1,0:T(8,128)(2,1)S(1)} %slice.12), channel_id=1, source_target_pairs={{0,1},{1,2},{2,3},{3,0},{4,5},{5,6},{6,7},{7,4},{8,9},{9,10},{10,1... | collective-permute-start | bytes 2752520 | tf_op jit(solution)/shard_map/ppermute | solution.py:500
  96.3 13.4 %collective-permute-start.8 = (bf16[1024,256]{1,0:T(8,128)(2,1)S(1)}, bf16[1024,256]{1,0:T(8,128)(2,1)S(1)}, u32[]{:S(2)}, u32[]{:S(2)}) collective-permute-start(bf16[1024,256]{1,0:T(8,128)(2,1)S(1)} %collective-permute-done.6.refs_10_), channel_id=1, source_target_pairs={{0,128},{128,0},{1,129},{129,1},{2,130},{130,2},{3,131},{131,3},{4... | collective-permute-start | bytes 1572872 | tf_op jit(solution)/shard_map/ppermute | solution.py:503
  106.2 14.3 %collective-permute-start.9 = (bf16[1024,256]{1,0:T(8,128)(2,1)S(1)}, bf16[1024,256]{1,0:T(8,128)(2,1)S(1)}, u32[]{:S(2)}, u32[]{:S(2)}) collective-permute-start(bf16[1024,256]{1,0:T(8,128)(2,1)S(1)} %collective-permute-done.7.refs_11_), channel_id=1, source_target_pairs={{0,128},{128,0},{1,129},{129,1},{2,130},{130,2},{3,131},{131,3},{4... | collective-permute-start | bytes 1572872 | tf_op jit(solution)/shard_map/ppermute | solution.py:503
  108.0 23.7 %collective-permute-start.13 = (bf16[1024,256]{1,0:T(8,128)(2,1)S(1)}, bf16[1024,256]{1,0:T(8,128)(2,1)S(1)}, u32[]{:S(2)}, u32[]{:S(2)}) collective-permute-start(bf16[1024,256]{1,0:T(8,128)(2,1)S(1)} %collective-permute-done.11.refs_15_), channel_id=1, source_target_pairs={{0,128},{128,0},{1,129},{129,1},{2,130},{130,2},{3,131},{131,3},{4... | collective-permute-start | bytes 1572872 | tf_op jit(solution)/shard_map/ppermute | solution.py:503
  108.2 23.5 %collective-permute-start.14 = (bf16[1024,256]{1,0:T(8,128)(2,1)S(1)}, bf16[1024,256]{1,0:T(8,128)(2,1)S(1)}, u32[]{:S(2)}, u32[]{:S(2)}) collective-permute-start(bf16[1024,256]{1,0:T(8,128)(2,1)S(1)} %collective-permute-done.4.refs_8_), channel_id=1, source_target_pairs={{0,1},{1,2},{2,3},{3,0},{4,5},{5,6},{6,7},{7,4},{8,9},{9,10},{10,1... | collective-permute-start | bytes 1572872 | tf_op jit(solution)/shard_map/ppermute | solution.py:500
  109.7 10.8 %collective-permute-start.16 = (bf16[32,2048]{1,0:T(8,128)(2,1)S(1)}, bf16[32,2048]{1,0:T(8,128)(2,1)S(1)}, u32[]{:S(2)}, u32[]{:S(2)}) collective-permute-start(bf16[32,2048]{1,0:T(8,128)(2,1)S(1)} %slice.13), channel_id=1, source_target_pairs={{0,3},{1,0},{2,1},{3,2},{4,7},{5,4},{6,5},{7,6},{8,11},{9,8},{10,9... | collective-permute-start | bytes 393224 | tf_op jit(solution)/shard_map/ppermute | solution.py:500
  140.7 72.4 %copy-start.2 = (bf16[2048,512]{1,0:T(8,128)(2,1)S(1)}, bf16[2048,512]{1,0:T(8,128)(2,1)}, u32[]{:S(2)}) copy-start(bf16[2048,512]{1,0:T(8,128)(2,1)} %weight_ref.1) | copy-start | bytes 6291460
  140.7 91.9 %all-to-all-start.1 = ((bf16[32,160,128]{2,1,0:T(8,128)(2,1)}), bf16[32,160,128]{2,1,0:T(8,128)(2,1)S(1)}, u32[]{:S(2)}, u32[]{:S(2)}) async-start(bf16[32,160,128]{2,1,0:T(8,128)(2,1)} %experts.1), calls=%async_computation.1 | async-start | bytes 2621440 | tf_op jit(solution)/shard_map/all_to_all | solution.py:510
  155.1 58.1 %copy-start.3 = (f32[2048]{0:T(1024)S(1)}, f32[2048]{0:T(1024)}, u32[]{:S(2)}) copy-start(f32[2048]{0:T(1024)} %param.14) | copy-start | bytes 24580
  156.7 56.5 %collective-permute-start = (bf16[32,2048]{1,0:T(8,128)(2,1)}, bf16[32,2048]{1,0:T(8,128)(2,1)}, u32[]{:S(2)}, u32[]{:S(2)}) collective-permute-start(bf16[32,2048]{1,0:T(8,128)(2,1)} %slice.9), channel_id=1, source_target_pairs={{0,4},{4,8},{8,12},{12,16},{16,20},{20,24},{24,28},{28,32},{32,36}... | collective-permute-start | bytes 393224 | tf_op jit(solution)/shard_map/ppermute | solution.py:531
  (12 other events, 325.1 us)

commit v8 on v7

--- a/solution.py
+++ b/solution.py
@@ -54,6 +54,7 @@
     out_ref,
     target_ref,
     *rest,
+    turn,
     experts,
     capacity,
 ):
@@ -85,7 +86,8 @@
             for move in moves(source_ref):
                 move.start()
 
-    ids = ids_ref[...]
+    ids = turn - ids_ref[...]
+    ids = jnp.where(ids < 0, ids + experts, ids)
     onehot = [
         (ids[k : k + 1, :] == lax.broadcasted_iota(jnp.int32, (experts, tokens), 0)).astype(F32)
         for k in range(2)
@@ -130,13 +132,13 @@
                 move.wait()
 
 
-def dispatch(own, rows, gain, ids, gate, up, cuts, experts, capacity):
+def dispatch(own, rows, gain, ids, gate, up, cuts, turn, experts, capacity):
     tokens = ids.shape[1]
     width = rows.shape[1]
     hbm = pl.BlockSpec(memory_space=pltpu.HBM)
 
     def kernel(*refs):
-        dispatch_kernel(*refs, experts=experts, capacity=capacity)
+        dispatch_kernel(*refs, turn=turn, experts=experts, capacity=capacity)
 
     def held(array):
         return pltpu.with_memory_space_constraint(array, pltpu.HBM)
@@ -510,7 +512,6 @@
         return lax.all_to_all(array, EP, 0, 0, axis_index_groups=[order], tiled=True)
 
     own_ids = lax.dynamic_slice_in_dim(expert_ids, own * tokens, tokens, 0).T
-    own_ids = (turn + ep_count - own_ids) % ep_count
     message, target, mine_a, mine_b = dispatch(
         jnp.stack([own, odd]),
         moe_input,
@@ -519,13 +520,14 @@
         gate,
         up,
         (half, gate.shape[0] - half),
+        turn,
         ep_count,
         capacity,
     )
     mine_a_l, mine_b_l = send(mine_a, left), send(mine_b, left)
     arrived = exchange(message)
+    other_a_l, mine_a_far = swap(mine_a_l), send(mine_a_l, left)
     mine_a_r, mine_b_r = send(mine_a, right), send(mine_b, right)
-    other_a_l, mine_a_far = swap(mine_a_l), send(mine_a_l, left)
     down_l = send(down, left)
     pairs = [(i, i + 1) for i in range(ep_count - 1)]
     carried = lax.ppermute(conv_input[conv_input.shape[0] - HALO :], EP, pairs)

time: 237 us -> 237 us (level)
  no operation moved by 1% of the time
where the time goes in v8:
time: 237 us; the launch traced here: 236 us
  waiting for transfers between devices  123 us (52%)
  starting transfers between devices  71.7 us (30%)
  Pallas kernels  34.2 us (14%)
  local copies, waits for them, and re-layouts  6.79 us (3%)
    ppermute x11, waiting for transfers between devices, send(): return lax.ppermute(array, 'tp', pairs)  52 us
    ppermute x1, waiting for transfers between devices, run(): carried = lax.ppermute(conv_input[conv_input.shape[0] - HALO:], EP, pairs)  50.4 us
    all_to_all x2, starting transfers between devices, exchange(): lax.all_to_all(array, EP, 0, 0, axis_index_groups=[order], tiled=True)  44.6 us
    ppermute x5, waiting for transfers between devices, swap(): return lax.ppermute(array, 'grp', across)  20.1 us
    pallas_call x1, Pallas kernels, conv_module(): pl.pallas_call(conv_kernel, grid=(count // block,), in_specs=[pl.BlockSpe...  17.8 us
    ppermute x11, starting transfers between devices, send(): return lax.ppermute(array, 'tp', pairs)  16.2 us
    pallas_call x1, Pallas kernels, experts_apply(): pl.pallas_call(kernel, in_specs=[pl.BlockSpec(memory_space=pltpu.SMEM), w...  8.86 us
    ppermute x5, starting transfers between devices, swap(): return lax.ppermute(array, 'grp', across)  7.51 us
  transfers between devices with their start and end apart: 19, of which 8 were waited for; matrix products, arithmetic and copies ran while one was open for 2% of the time, Pallas kernels for 8%

profile of v8, /device:TPU:33, one launch (start us, length us, event | category | flops | bytes accessed | tf_op | source)
XLA Modules:
  0.0 236.3 jit_solution(9756525414286330918)
XLA Ops:
  1.4 4.0 %dispatch.1 = (bf16[32,160,128]{2,1,0:T(8,128)(2,1)}, s32[2,160]{1,0:T(2,128)S(1)}, bf16[1024,256]{1,0:T(8,128)(2,1)S(1)}, bf16[1024,256]{1,0:T(8,128)(2,1)S(1)}) custom-call(s32[2]{0:T(128)S(1)} %pad_add_fusion.refs_0_, bf16[640,2048]{1,0:T(8,128)(2,1)} %refs_1_.1, f32[1,2048]{1,0:T(1,128)} %bitcast.23, s32[2,160]{1,0:T(2,128)S(1)} %dynamic-slice_bitcast_fusion.refs_3_, ...), custom_call_target="tpu_custom_call" | custom-call | tf_op jit(solution)/shard_map/dispatch/pallas_call | solution.py:146
  5.4 30.3 %all-to-all-start = ((bf16[32,160,128]{2,1,0:T(8,128)(2,1)}), bf16[32,160,128]{2,1,0:T(8,128)(2,1)S(1)}, u32[]{:S(2)}, u32[]{:S(2)}) async-start(bf16[32,160,128]{2,1,0:T(8,128)(2,1)} %get-tuple-element.6), calls=%async_computation | async-start | bytes 2621440 | tf_op jit(solution)/shard_map/all_to_all | solution.py:512
  37.1 1.7 collective-permute-start.6
  38.8 2.7 %collective-permute-start.7 = (bf16[1024,256]{1,0:T(8,128)(2,1)S(1)}, bf16[1024,256]{1,0:T(8,128)(2,1)S(1)}, u32[]{:S(2)}, u32[]{:S(2)}) collective-permute-start(bf16[1024,256]{1,0:T(8,128)(2,1)S(1)} %get-tuple-element.8), channel_id=1, source_target_pairs={{0,3},{1,0},{2,1},{3,2},{4,7},{5,4},{6,5},{7,6},{8,11},{9,8},{10,9... | collective-permute-start | bytes 1572872 | tf_op jit(solution)/shard_map/ppermute | solution.py:502
  41.5 8.4 %collective-permute-done.6.refs_10_ = bf16[1024,256]{1,0:T(8,128)(2,1)S(1)} collective-permute-done((bf16[1024,256]{1,0:T(8,128)(2,1)S(1)}, bf16[1024,256]{1,0:T(8,128)(2,1)S(1)}, u32[]{:S(2)}, u32[]{:S(2)}) %collective-permute-start.6) | collective-permute-done | bytes 524320 | tf_op jit(solution)/shard_map/ppermute | solution.py:502
  49.9 3.2 %collective-permute-start.10 = (bf16[256,2048]{1,0:T(8,128)(2,1)}, bf16[256,2048]{1,0:T(8,128)(2,1)S(1)}, u32[]{:S(2)}, u32[]{:S(2)}) collective-permute-start(bf16[256,2048]{1,0:T(8,128)(2,1)} %bitcast.7.refs_4_), channel_id=1, source_target_pairs={{0,3},{1,0},{2,1},{3,2},{4,7},{5,4},{6,5},{7,6},{8,11},{9,8},{10,9... | collective-permute-start | bytes 3145736 | tf_op jit(solution)/shard_map/ppermute | solution.py:502
  53.1 20.1 %collective-permute-done.2.refs_6_ = bf16[1024,256]{1,0:T(8,128)(2,1)S(1)} collective-permute-done((bf16[1024,256]{1,0:T(8,128)(2,1)S(1)}, bf16[1024,256]{1,0:T(8,128)(2,1)S(1)}, u32[]{:S(2)}, u32[]{:S(2)}) %collective-permute-start.2) | collective-permute-done | bytes 524320 | tf_op jit(solution)/shard_map/ppermute | solution.py:502
  74.4 1.8 collective-permute-start.4
  76.3 8.2 %collective-permute-done.1.refs_5_ = bf16[1024,256]{1,0:T(8,128)(2,1)S(1)} collective-permute-done((bf16[1024,256]{1,0:T(8,128)(2,1)S(1)}, bf16[1024,256]{1,0:T(8,128)(2,1)S(1)}, u32[]{:S(2)}, u32[]{:S(2)}) %collective-permute-start.1) | collective-permute-done | bytes 524320 | tf_op jit(solution)/shard_map/ppermute | solution.py:502
  85.6 1.8 collective-permute-start.3
  87.6 7.3 %collective-permute-done.11.refs_15_ = bf16[1024,256]{1,0:T(8,128)(2,1)S(1)} collective-permute-done((bf16[1024,256]{1,0:T(8,128)(2,1)S(1)}, bf16[1024,256]{1,0:T(8,128)(2,1)S(1)}, u32[]{:S(2)}, u32[]{:S(2)}) %collective-permute-start.11) | collective-permute-done | bytes 524320 | tf_op jit(solution)/shard_map/ppermute | solution.py:502
  96.2 1.8 collective-permute-start.8
  98.0 8.0 %collective-permute-done.12.refs_16_ = bf16[1024,256]{1,0:T(8,128)(2,1)S(1)} collective-permute-done((bf16[1024,256]{1,0:T(8,128)(2,1)S(1)}, bf16[1024,256]{1,0:T(8,128)(2,1)S(1)}, u32[]{:S(2)}, u32[]{:S(2)}) %collective-permute-start.12) | collective-permute-done | bytes 524320 | tf_op jit(solution)/shard_map/ppermute | solution.py:502
  106.1 1.8 collective-permute-start.9
  109.6 2.0 collective-permute-start.16
  111.6 8.8 %collective-permute-done.9.refs_13_ = bf16[1024,256]{1,0:T(8,128)(2,1)S(1)} collective-permute-done((bf16[1024,256]{1,0:T(8,128)(2,1)S(1)}, bf16[1024,256]{1,0:T(8,128)(2,1)S(1)}, u32[]{:S(2)}, u32[]{:S(2)}) %collective-permute-start.9) | collective-permute-done | bytes 524320 | tf_op jit(solution)/shard_map/ppermute | solution.py:505
  120.4 11.2 %collective-permute-done.13.refs_17_ = bf16[1024,256]{1,0:T(8,128)(2,1)S(1)} collective-permute-done((bf16[1024,256]{1,0:T(8,128)(2,1)S(1)}, bf16[1024,256]{1,0:T(8,128)(2,1)S(1)}, u32[]{:S(2)}, u32[]{:S(2)}) %collective-permute-start.13) | collective-permute-done | bytes 524320 | tf_op jit(solution)/shard_map/ppermute | solution.py:505
  131.8 8.9 %experts.1 = bf16[32,160,128]{2,1,0:T(8,128)(2,1)} custom-call(s32[1]{0:T(128)} %bitcast.1.refs_0_, bf16[32,160,128]{2,1,0:T(8,128)(2,1)S(1)} %all-to-all-done.refs_1_, bf16[2048,256]{1,0:T(8,128)(2,1)} %bitcast.18, bf16[2048,256]{1,0:T(8,128)(2,1)} %bitcast.20, bf16[256,2048]{1,0:T(8,128)(2,1)} %bitcast.7.refs_4_, bf16[1024,256]{1,0:T(8,128)(2,1)} %copy-done.10, ...), custom_call_target="tpu_custom_call" | custom-call | tf_op jit(solution)/shard_map/experts/pallas_call | solution.py:316
  140.6 14.3 %all-to-all-start.1 = ((bf16[32,160,128]{2,1,0:T(8,128)(2,1)}), bf16[32,160,128]{2,1,0:T(8,128)(2,1)S(1)}, u32[]{:S(2)}, u32[]{:S(2)}) async-start(bf16[32,160,128]{2,1,0:T(8,128)(2,1)} %experts.1), calls=%async_computation.1 | async-start | bytes 2621440 | tf_op jit(solution)/shard_map/all_to_all | solution.py:512
  156.6 3.4 %collective-permute-start = (bf16[32,2048]{1,0:T(8,128)(2,1)}, bf16[32,2048]{1,0:T(8,128)(2,1)}, u32[]{:S(2)}, u32[]{:S(2)}) collective-permute-start(bf16[32,2048]{1,0:T(8,128)(2,1)} %slice.9), channel_id=1, source_target_pairs={{0,4},{4,8},{8,12},{12,16},{16,20},{20,24},{24,28},{28,32},{32,36}... | collective-permute-start | bytes 393224 | tf_op jit(solution)/shard_map/ppermute | solution.py:533
  162.6 50.4 %collective-permute-done.carried_ref = bf16[32,2048]{1,0:T(8,128)(2,1)} collective-permute-done((bf16[32,2048]{1,0:T(8,128)(2,1)}, bf16[32,2048]{1,0:T(8,128)(2,1)}, u32[]{:S(2)}, u32[]{:S(2)}) %collective-permute-start) | collective-permute-done | bytes 131104 | tf_op jit(solution)/shard_map/ppermute | solution.py:533
  213.1 1.7 copy-done.1
  214.8 17.8 %conv.1 = bf16[640,512]{1,0:T(8,128)(2,1)} custom-call(bf16[640,2048]{1,0:T(8,128)(2,1)S(1)} %copy-done.1, bf16[32,2048]{1,0:T(8,128)(2,1)} %collective-permute-done.carried_ref, f32[31,16,128]{2,1,0:T(8,128)S(1)} %slice.14.taps_ref, f32[1,2048]{1,0:T(1,128)S(1)} %bitcast.15, bf16[2048,512]{1,0:T(8,128)(2,1)S(1)} %copy-done.2), custom_call_target="tpu_custom_call" | custom-call | tf_op jit(solution)/shard_map/conv/pallas_call | solution.py:445
  232.6 3.5 %combine.1 = bf16[160,2048]{1,0:T(8,128)(2,1)} custom-call(bf16[32,160,128]{2,1,0:T(8,128)(2,1)S(1)} %all-to-all-done.1.refs_0_, s32[160,2]{1,0:T(8,128)S(1)} %bitcast.14, f32[160,2]{1,0:T(8,128)} %copy.16.refs_2_, f32[1,2048]{1,0:T(1,128)S(1)} %bitcast.16), custom_call_target="tpu_custom_call" | custom-call | tf_op jit(solution)/shard_map/combine/pallas_call | solution.py:380
  (62 shorter events, 12.0 us)
Async XLA Ops:
  5.4 126.4 %all-to-all-start = ((bf16[32,160,128]{2,1,0:T(8,128)(2,1)}), bf16[32,160,128]{2,1,0:T(8,128)(2,1)S(1)}, u32[]{:S(2)}, u32[]{:S(2)}) async-start(bf16[32,160,128]{2,1,0:T(8,128)(2,1)} %get-tuple-element.6), calls=%async_computation | async-start | bytes 2621440 | tf_op jit(solution)/shard_map/all_to_all | solution.py:512
  35.7 50.0 %collective-permute-start.5 = (bf16[256,2048]{1,0:T(8,128)(2,1)}, bf16[256,2048]{1,0:T(8,128)(2,1)S(1)}, u32[]{:S(2)}, u32[]{:S(2)}) collective-permute-start(bf16[256,2048]{1,0:T(8,128)(2,1)} %bitcast.7.refs_4_), channel_id=1, source_target_pairs={{0,1},{1,2},{2,3},{3,0},{4,5},{5,6},{6,7},{7,4},{8,9},{9,10},{10,1... | collective-permute-start | bytes 3145736 | tf_op jit(solution)/shard_map/ppermute | solution.py:502
  37.1 12.8 %collective-permute-start.6 = (bf16[1024,256]{1,0:T(8,128)(2,1)S(1)}, bf16[1024,256]{1,0:T(8,128)(2,1)S(1)}, u32[]{:S(2)}, u32[]{:S(2)}) collective-permute-start(bf16[1024,256]{1,0:T(8,128)(2,1)S(1)} %get-tuple-element.7), channel_id=1, source_target_pairs={{0,3},{1,0},{2,1},{3,2},{4,7},{5,4},{6,5},{7,6},{8,11},{9,8},{10,9... | collective-permute-start | bytes 1572872 | tf_op jit(solution)/shard_map/ppermute | solution.py:502
  38.8 34.4 %collective-permute-start.2 = (bf16[1024,256]{1,0:T(8,128)(2,1)S(1)}, bf16[1024,256]{1,0:T(8,128)(2,1)S(1)}, u32[]{:S(2)}, u32[]{:S(2)}) collective-permute-start(bf16[1024,256]{1,0:T(8,128)(2,1)S(1)} %get-tuple-element.8), channel_id=1, source_target_pairs={{0,1},{1,2},{2,3},{3,0},{4,5},{5,6},{6,7},{7,4},{8,9},{9,10},{10,1... | collective-permute-start | bytes 1572872 | tf_op jit(solution)/shard_map/ppermute | solution.py:502
  38.8 35.6 %collective-permute-start.7 = (bf16[1024,256]{1,0:T(8,128)(2,1)S(1)}, bf16[1024,256]{1,0:T(8,128)(2,1)S(1)}, u32[]{:S(2)}, u32[]{:S(2)}) collective-permute-start(bf16[1024,256]{1,0:T(8,128)(2,1)S(1)} %get-tuple-element.8), channel_id=1, source_target_pairs={{0,3},{1,0},{2,1},{3,2},{4,7},{5,4},{6,5},{7,6},{8,11},{9,8},{10,9... | collective-permute-start | bytes 1572872 | tf_op jit(solution)/shard_map/ppermute | solution.py:502
  41.5 42.9 %collective-permute-start.1 = (bf16[1024,256]{1,0:T(8,128)(2,1)S(1)}, bf16[1024,256]{1,0:T(8,128)(2,1)S(1)}, u32[]{:S(2)}, u32[]{:S(2)}) collective-permute-start(bf16[1024,256]{1,0:T(8,128)(2,1)S(1)} %get-tuple-element.7), channel_id=1, source_target_pairs={{0,1},{1,2},{2,3},{3,0},{4,5},{5,6},{6,7},{7,4},{8,9},{9,10},{10,1... | collective-permute-start | bytes 1572872 | tf_op jit(solution)/shard_map/ppermute | solution.py:502
  49.9 81.7 %copy-start.7 = (bf16[1024,256]{1,0:T(8,128)(2,1)}, bf16[1024,256]{1,0:T(8,128)(2,1)S(1)}, u32[]{:S(2)}) copy-start(bf16[1024,256]{1,0:T(8,128)(2,1)S(1)} %collective-permute-done.6.refs_10_) | copy-start | bytes 1572868
  49.9 58.2 %collective-permute-start.10 = (bf16[256,2048]{1,0:T(8,128)(2,1)}, bf16[256,2048]{1,0:T(8,128)(2,1)S(1)}, u32[]{:S(2)}, u32[]{:S(2)}) collective-permute-start(bf16[256,2048]{1,0:T(8,128)(2,1)} %bitcast.7.refs_4_), channel_id=1, source_target_pairs={{0,3},{1,0},{2,1},{3,2},{4,7},{5,4},{6,5},{7,6},{8,11},{9,8},{10,9... | collective-permute-start | bytes 3145736 | tf_op jit(solution)/shard_map/ppermute | solution.py:502
  73.2 58.5 %copy-start.8 = (bf16[1024,256]{1,0:T(8,128)(2,1)}, bf16[1024,256]{1,0:T(8,128)(2,1)S(1)}, u32[]{:S(2)}) copy-start(bf16[1024,256]{1,0:T(8,128)(2,1)S(1)} %collective-permute-done.2.refs_6_) | copy-start | bytes 1572868
  73.2 21.7 %collective-permute-start.11 = (bf16[1024,256]{1,0:T(8,128)(2,1)S(1)}, bf16[1024,256]{1,0:T(8,128)(2,1)S(1)}, u32[]{:S(2)}, u32[]{:S(2)}) collective-permute-start(bf16[1024,256]{1,0:T(8,128)(2,1)S(1)} %collective-permute-done.6.refs_10_), channel_id=1, source_target_pairs={{0,3},{1,0},{2,1},{3,2},{4,7},{5,4},{6,5},{7,6},{8,11},{9,8},{10,9... | collective-permute-start | bytes 1572872 | tf_op jit(solution)/shard_map/ppermute | solution.py:502
  74.4 57.2 %copy-start.9 = (bf16[1024,256]{1,0:T(8,128)(2,1)}, bf16[1024,256]{1,0:T(8,128)(2,1)S(1)}, u32[]{:S(2)}) copy-start(bf16[1024,256]{1,0:T(8,128)(2,1)S(1)} %collective-permute-done.7.refs_11_) | copy-start | bytes 1572868
  74.4 21.8 %collective-permute-start.4 = (bf16[1024,256]{1,0:T(8,128)(2,1)S(1)}, bf16[1024,256]{1,0:T(8,128)(2,1)S(1)}, u32[]{:S(2)}, u32[]{:S(2)}) collective-permute-start(bf16[1024,256]{1,0:T(8,128)(2,1)S(1)} %collective-permute-done.2.refs_6_), channel_id=1, source_target_pairs={{0,128},{128,0},{1,129},{129,1},{2,130},{130,2},{3,131},{131,3},{4... | collective-permute-start | bytes 1572872 | tf_op jit(solution)/shard_map/ppermute | solution.py:505
  84.4 21.7 %collective-permute-start.12 = (bf16[1024,256]{1,0:T(8,128)(2,1)S(1)}, bf16[1024,256]{1,0:T(8,128)(2,1)S(1)}, u32[]{:S(2)}, u32[]{:S(2)}) collective-permute-start(bf16[1024,256]{1,0:T(8,128)(2,1)S(1)} %collective-permute-done.7.refs_11_), channel_id=1, source_target_pairs={{0,3},{1,0},{2,1},{3,2},{4,7},{5,4},{6,5},{7,6},{8,11},{9,8},{10,9... | collective-permute-start | bytes 1572872 | tf_op jit(solution)/shard_map/ppermute | solution.py:502
  85.6 22.3 %collective-permute-start.3 = (bf16[1024,256]{1,0:T(8,128)(2,1)S(1)}, bf16[1024,256]{1,0:T(8,128)(2,1)S(1)}, u32[]{:S(2)}, u32[]{:S(2)}) collective-permute-start(bf16[1024,256]{1,0:T(8,128)(2,1)S(1)} %collective-permute-done.1.refs_5_), channel_id=1, source_target_pairs={{0,128},{128,0},{1,129},{129,1},{2,130},{130,2},{3,131},{131,3},{4... | collective-permute-start | bytes 1572872 | tf_op jit(solution)/shard_map/ppermute | solution.py:505
  94.8 36.9 %collective-permute-start.15 = (bf16[224,2048]{1,0:T(8,128)(2,1)S(1)}, bf16[224,2048]{1,0:T(8,128)(2,1)S(1)}, u32[]{:S(2)}, u32[]{:S(2)}) collective-permute-start(bf16[224,2048]{1,0:T(8,128)(2,1)S(1)} %slice.12), channel_id=1, source_target_pairs={{0,1},{1,2},{2,3},{3,0},{4,5},{5,6},{6,7},{7,4},{8,9},{9,10},{10,1... | collective-permute-start | bytes 2752520 | tf_op jit(solution)/shard_map/ppermute | solution.py:502
  96.2 13.4 %collective-permute-start.8 = (bf16[1024,256]{1,0:T(8,128)(2,1)S(1)}, bf16[1024,256]{1,0:T(8,128)(2,1)S(1)}, u32[]{:S(2)}, u32[]{:S(2)}) collective-permute-start(bf16[1024,256]{1,0:T(8,128)(2,1)S(1)} %collective-permute-done.6.refs_10_), channel_id=1, source_target_pairs={{0,128},{128,0},{1,129},{129,1},{2,130},{130,2},{3,131},{131,3},{4... | collective-permute-start | bytes 1572872 | tf_op jit(solution)/shard_map/ppermute | solution.py:505
  106.1 14.3 %collective-permute-start.9 = (bf16[1024,256]{1,0:T(8,128)(2,1)S(1)}, bf16[1024,256]{1,0:T(8,128)(2,1)S(1)}, u32[]{:S(2)}, u32[]{:S(2)}) collective-permute-start(bf16[1024,256]{1,0:T(8,128)(2,1)S(1)} %collective-permute-done.7.refs_11_), channel_id=1, source_target_pairs={{0,128},{128,0},{1,129},{129,1},{2,130},{130,2},{3,131},{131,3},{4... | collective-permute-start | bytes 1572872 | tf_op jit(solution)/shard_map/ppermute | solution.py:505
  107.9 23.7 %collective-permute-start.13 = (bf16[1024,256]{1,0:T(8,128)(2,1)S(1)}, bf16[1024,256]{1,0:T(8,128)(2,1)S(1)}, u32[]{:S(2)}, u32[]{:S(2)}) collective-permute-start(bf16[1024,256]{1,0:T(8,128)(2,1)S(1)} %collective-permute-done.11.refs_15_), channel_id=1, source_target_pairs={{0,128},{128,0},{1,129},{129,1},{2,130},{130,2},{3,131},{131,3},{4... | collective-permute-start | bytes 1572872 | tf_op jit(solution)/shard_map/ppermute | solution.py:505
  108.1 23.5 %collective-permute-start.14 = (bf16[1024,256]{1,0:T(8,128)(2,1)S(1)}, bf16[1024,256]{1,0:T(8,128)(2,1)S(1)}, u32[]{:S(2)}, u32[]{:S(2)}) collective-permute-start(bf16[1024,256]{1,0:T(8,128)(2,1)S(1)} %collective-permute-done.4.refs_8_), channel_id=1, source_target_pairs={{0,1},{1,2},{2,3},{3,0},{4,5},{5,6},{6,7},{7,4},{8,9},{9,10},{10,1... | collective-permute-start | bytes 1572872 | tf_op jit(solution)/shard_map/ppermute | solution.py:502
  109.6 10.8 %collective-permute-start.16 = (bf16[32,2048]{1,0:T(8,128)(2,1)S(1)}, bf16[32,2048]{1,0:T(8,128)(2,1)S(1)}, u32[]{:S(2)}, u32[]{:S(2)}) collective-permute-start(bf16[32,2048]{1,0:T(8,128)(2,1)S(1)} %slice.13), channel_id=1, source_target_pairs={{0,3},{1,0},{2,1},{3,2},{4,7},{5,4},{6,5},{7,6},{8,11},{9,8},{10,9... | collective-permute-start | bytes 393224 | tf_op jit(solution)/shard_map/ppermute | solution.py:502
  140.6 72.4 %copy-start.2 = (bf16[2048,512]{1,0:T(8,128)(2,1)S(1)}, bf16[2048,512]{1,0:T(8,128)(2,1)}, u32[]{:S(2)}) copy-start(bf16[2048,512]{1,0:T(8,128)(2,1)} %weight_ref.1) | copy-start | bytes 6291460
  140.6 91.9 %all-to-all-start.1 = ((bf16[32,160,128]{2,1,0:T(8,128)(2,1)}), bf16[32,160,128]{2,1,0:T(8,128)(2,1)S(1)}, u32[]{:S(2)}, u32[]{:S(2)}) async-start(bf16[32,160,128]{2,1,0:T(8,128)(2,1)} %experts.1), calls=%async_computation.1 | async-start | bytes 2621440 | tf_op jit(solution)/shard_map/all_to_all | solution.py:512
  155.0 58.1 %copy-start.3 = (f32[2048]{0:T(1024)S(1)}, f32[2048]{0:T(1024)}, u32[]{:S(2)}) copy-start(f32[2048]{0:T(1024)} %param.14) | copy-start | bytes 24580
  156.6 56.5 %collective-permute-start = (bf16[32,2048]{1,0:T(8,128)(2,1)}, bf16[32,2048]{1,0:T(8,128)(2,1)}, u32[]{:S(2)}, u32[]{:S(2)}) collective-permute-start(bf16[32,2048]{1,0:T(8,128)(2,1)} %slice.9), channel_id=1, source_target_pairs={{0,4},{4,8},{8,12},{12,16},{16,20},{20,24},{24,28},{28,32},{32,36}... | collective-permute-start | bytes 393224 | tf_op jit(solution)/shard_map/ppermute | solution.py:533
  (12 other events, 268.5 us)

commit v9 on v8

--- a/solution.py
+++ b/solution.py
@@ -531,12 +531,12 @@
     down_l = send(down, left)
     pairs = [(i, i + 1) for i in range(ep_count - 1)]
     carried = lax.ppermute(conv_input[conv_input.shape[0] - HALO :], EP, pairs)
-    other_b_l, mine_b_far = swap(mine_b_l), send(mine_b_l, left)
+    other_b_l = swap(mine_b_l)
     down_a_far = send(down_r[:part], right)
     other_a_r = swap(mine_a_r)
-    other_b_r = swap(mine_b_r)
+    other_b_r, mine_b_far = swap(mine_b_r), send(mine_b_r, right)
     other_a_far = swap(mine_a_far)
-    other_b_far, down_b_far = send(other_b_r, right), send(down_l[part:], left)
+    other_b_far, down_b_far = send(other_b_l, left), send(down_l[part:], left)
 
     conv_out = conv_module(conv_input, carried, conv_taps, conv_gain.reshape(1, width), conv_weight)
 

time: 237 us -> 236 us (level)
    ppermute x11, waiting for transfers between devices: 52 us -> 44.3 us  [send(): return lax.ppermute(array, 'tp', pairs)]
    ppermute x5, waiting for transfers between devices: 20.1 us -> 26.5 us  [swap(): return lax.ppermute(array, 'grp', across)]
  transfers between devices with their start and end apart: 19 -> 19, of which waited for: 8 -> 9; matrix products, arithmetic and copies ran while one was open for 2% -> 2% of each run, Pallas kernels for 8% -> 8%
where the time goes in v9:
time: 236 us
  waiting for transfers between devices  121 us (51%)
  starting transfers between devices  72.3 us (31%)
  Pallas kernels  34.2 us (14%)
  local copies, waits for them, and re-layouts  6.79 us (3%)
    ppermute x1, waiting for transfers between devices, run(): carried = lax.ppermute(conv_input[conv_input.shape[0] - HALO:], EP, pairs)  50.4 us
    all_to_all x2, starting transfers between devices, exchange(): lax.all_to_all(array, EP, 0, 0, axis_index_groups=[order], tiled=True)  44.6 us
    ppermute x11, waiting for transfers between devices, send(): return lax.ppermute(array, 'tp', pairs)  44.3 us
    ppermute x5, waiting for transfers between devices, swap(): return lax.ppermute(array, 'grp', across)  26.5 us
    pallas_call x1, Pallas kernels, conv_module(): pl.pallas_call(conv_kernel, grid=(count // block,), in_specs=[pl.BlockSpe...  17.8 us
    ppermute x11, starting transfers between devices, send(): return lax.ppermute(array, 'tp', pairs)  16.7 us
    pallas_call x1, Pallas kernels, experts_apply(): pl.pallas_call(kernel, in_specs=[pl.BlockSpec(memory_space=pltpu.SMEM), w...  8.86 us
    ppermute x5, starting transfers between devices, swap(): return lax.ppermute(array, 'grp', across)  7.66 us
  transfers between devices with their start and end apart: 19, of which 9 were waited for; matrix products, arithmetic and copies ran while one was open for 2% of the time, Pallas kernels for 8%

profile of v9, /device:TPU:33, one launch (start us, length us, event | category | flops | bytes accessed | tf_op | source)
XLA Modules:
  0.0 235.6 jit_solution(17373928155449242880)
XLA Ops:
  1.4 4.0 %dispatch.1 = (bf16[32,160,128]{2,1,0:T(8,128)(2,1)}, s32[2,160]{1,0:T(2,128)S(1)}, bf16[1024,256]{1,0:T(8,128)(2,1)S(1)}, bf16[1024,256]{1,0:T(8,128)(2,1)S(1)}) custom-call(s32[2]{0:T(128)S(1)} %pad_add_fusion.refs_0_, bf16[640,2048]{1,0:T(8,128)(2,1)} %refs_1_.1, f32[1,2048]{1,0:T(1,128)} %bitcast.23, s32[2,160]{1,0:T(2,128)S(1)} %dynamic-slice_bitcast_fusion.refs_3_, ...), custom_call_target="tpu_custom_call" | custom-call | tf_op jit(solution)/shard_map/dispatch/pallas_call | solution.py:146
  5.4 30.3 %all-to-all-start = ((bf16[32,160,128]{2,1,0:T(8,128)(2,1)}), bf16[32,160,128]{2,1,0:T(8,128)(2,1)S(1)}, u32[]{:S(2)}, u32[]{:S(2)}) async-start(bf16[32,160,128]{2,1,0:T(8,128)(2,1)} %get-tuple-element.6), calls=%async_computation | async-start | bytes 2621440 | tf_op jit(solution)/shard_map/all_to_all | solution.py:512
  40.3 9.6 %collective-permute-done.6.refs_10_ = bf16[1024,256]{1,0:T(8,128)(2,1)S(1)} collective-permute-done((bf16[1024,256]{1,0:T(8,128)(2,1)S(1)}, bf16[1024,256]{1,0:T(8,128)(2,1)S(1)}, u32[]{:S(2)}, u32[]{:S(2)}) %collective-permute-start.6) | collective-permute-done | bytes 524320 | tf_op jit(solution)/shard_map/ppermute | solution.py:502
  49.9 3.2 %collective-permute-start.10 = (bf16[256,2048]{1,0:T(8,128)(2,1)}, bf16[256,2048]{1,0:T(8,128)(2,1)S(1)}, u32[]{:S(2)}, u32[]{:S(2)}) collective-permute-start(bf16[256,2048]{1,0:T(8,128)(2,1)} %bitcast.7.refs_4_), channel_id=1, source_target_pairs={{0,3},{1,0},{2,1},{3,2},{4,7},{5,4},{6,5},{7,6},{8,11},{9,8},{10,9... | collective-permute-start | bytes 3145736 | tf_op jit(solution)/shard_map/ppermute | solution.py:502
  53.1 8.1 %collective-permute-done.7.refs_11_ = bf16[1024,256]{1,0:T(8,128)(2,1)S(1)} collective-permute-done((bf16[1024,256]{1,0:T(8,128)(2,1)S(1)}, bf16[1024,256]{1,0:T(8,128)(2,1)S(1)}, u32[]{:S(2)}, u32[]{:S(2)}) %collective-permute-start.7) | collective-permute-done | bytes 524320 | tf_op jit(solution)/shard_map/ppermute | solution.py:502
  61.1 3.2 %collective-permute-start.11 = (bf16[1024,256]{1,0:T(8,128)(2,1)S(1)}, bf16[1024,256]{1,0:T(8,128)(2,1)S(1)}, u32[]{:S(2)}, u32[]{:S(2)}) collective-permute-start(bf16[1024,256]{1,0:T(8,128)(2,1)S(1)} %collective-permute-done.6.refs_10_), channel_id=1, source_target_pairs={{0,3},{1,0},{2,1},{3,2},{4,7},{5,4},{6,5},{7,6},{8,11},{9,8},{10,9... | collective-permute-start | bytes 1572872 | tf_op jit(solution)/shard_map/ppermute | solution.py:502
  64.3 8.9 %collective-permute-done.2.refs_6_ = bf16[1024,256]{1,0:T(8,128)(2,1)S(1)} collective-permute-done((bf16[1024,256]{1,0:T(8,128)(2,1)S(1)}, bf16[1024,256]{1,0:T(8,128)(2,1)S(1)}, u32[]{:S(2)}, u32[]{:S(2)}) %collective-permute-start.2) | collective-permute-done | bytes 524320 | tf_op jit(solution)/shard_map/ppermute | solution.py:502
  73.2 1.8 collective-permute-start.9
  75.0 9.4 %collective-permute-done.1.refs_5_ = bf16[1024,256]{1,0:T(8,128)(2,1)S(1)} collective-permute-done((bf16[1024,256]{1,0:T(8,128)(2,1)S(1)}, bf16[1024,256]{1,0:T(8,128)(2,1)S(1)}, u32[]{:S(2)}, u32[]{:S(2)}) %collective-permute-start.1) | collective-permute-done | bytes 524320 | tf_op jit(solution)/shard_map/ppermute | solution.py:502
  84.4 2.0 collective-permute-start.3
  86.5 8.3 %collective-permute-done.11.refs_15_ = bf16[1024,256]{1,0:T(8,128)(2,1)S(1)} collective-permute-done((bf16[1024,256]{1,0:T(8,128)(2,1)S(1)}, bf16[1024,256]{1,0:T(8,128)(2,1)S(1)}, u32[]{:S(2)}, u32[]{:S(2)}) %collective-permute-start.11) | collective-permute-done | bytes 524320 | tf_op jit(solution)/shard_map/ppermute | solution.py:502
  96.2 1.8 collective-permute-start.4
  98.1 1.9 collective-permute-start.8
  101.6 6.9 %collective-permute-done.4.refs_8_ = bf16[1024,256]{1,0:T(8,128)(2,1)S(1)} collective-permute-done((bf16[1024,256]{1,0:T(8,128)(2,1)S(1)}, bf16[1024,256]{1,0:T(8,128)(2,1)S(1)}, u32[]{:S(2)}, u32[]{:S(2)}) %collective-permute-start.4) | collective-permute-done | bytes 524320 | tf_op jit(solution)/shard_map/ppermute | solution.py:505
  108.5 2.9 %collective-permute-start.16 = (bf16[32,2048]{1,0:T(8,128)(2,1)S(1)}, bf16[32,2048]{1,0:T(8,128)(2,1)S(1)}, u32[]{:S(2)}, u32[]{:S(2)}) collective-permute-start(bf16[32,2048]{1,0:T(8,128)(2,1)S(1)} %slice.13), channel_id=1, source_target_pairs={{0,3},{1,0},{2,1},{3,2},{4,7},{5,4},{6,5},{7,6},{8,11},{9,8},{10,9... | collective-permute-start | bytes 393224 | tf_op jit(solution)/shard_map/ppermute | solution.py:502
  111.4 8.3 %collective-permute-done.8.refs_12_ = bf16[1024,256]{1,0:T(8,128)(2,1)S(1)} collective-permute-done((bf16[1024,256]{1,0:T(8,128)(2,1)S(1)}, bf16[1024,256]{1,0:T(8,128)(2,1)S(1)}, u32[]{:S(2)}, u32[]{:S(2)}) %collective-permute-start.8) | collective-permute-done | bytes 524320 | tf_op jit(solution)/shard_map/ppermute | solution.py:505
  119.8 11.2 %collective-permute-done.13.refs_17_ = bf16[1024,256]{1,0:T(8,128)(2,1)S(1)} collective-permute-done((bf16[1024,256]{1,0:T(8,128)(2,1)S(1)}, bf16[1024,256]{1,0:T(8,128)(2,1)S(1)}, u32[]{:S(2)}, u32[]{:S(2)}) %collective-permute-start.13) | collective-permute-done | bytes 524320 | tf_op jit(solution)/shard_map/ppermute | solution.py:505
  131.1 8.9 %experts.1 = bf16[32,160,128]{2,1,0:T(8,128)(2,1)} custom-call(s32[1]{0:T(128)} %bitcast.1.refs_0_, bf16[32,160,128]{2,1,0:T(8,128)(2,1)S(1)} %all-to-all-done.refs_1_, bf16[2048,256]{1,0:T(8,128)(2,1)} %bitcast.18, bf16[2048,256]{1,0:T(8,128)(2,1)} %bitcast.20, bf16[256,2048]{1,0:T(8,128)(2,1)} %bitcast.7.refs_4_, bf16[1024,256]{1,0:T(8,128)(2,1)} %copy-done.10, ...), custom_call_target="tpu_custom_call" | custom-call | tf_op jit(solution)/shard_map/experts/pallas_call | solution.py:316
  140.0 14.3 %all-to-all-start.1 = ((bf16[32,160,128]{2,1,0:T(8,128)(2,1)}), bf16[32,160,128]{2,1,0:T(8,128)(2,1)S(1)}, u32[]{:S(2)}, u32[]{:S(2)}) async-start(bf16[32,160,128]{2,1,0:T(8,128)(2,1)} %experts.1), calls=%async_computation.1 | async-start | bytes 2621440 | tf_op jit(solution)/shard_map/all_to_all | solution.py:512
  155.9 3.4 %collective-permute-start = (bf16[32,2048]{1,0:T(8,128)(2,1)}, bf16[32,2048]{1,0:T(8,128)(2,1)}, u32[]{:S(2)}, u32[]{:S(2)}) collective-permute-start(bf16[32,2048]{1,0:T(8,128)(2,1)} %slice.9), channel_id=1, source_target_pairs={{0,4},{4,8},{8,12},{12,16},{16,20},{20,24},{24,28},{28,32},{32,36}... | collective-permute-start | bytes 393224 | tf_op jit(solution)/shard_map/ppermute | solution.py:533
  161.9 50.4 %collective-permute-done.carried_ref = bf16[32,2048]{1,0:T(8,128)(2,1)} collective-permute-done((bf16[32,2048]{1,0:T(8,128)(2,1)}, bf16[32,2048]{1,0:T(8,128)(2,1)}, u32[]{:S(2)}, u32[]{:S(2)}) %collective-permute-start) | collective-permute-done | bytes 131104 | tf_op jit(solution)/shard_map/ppermute | solution.py:533
  212.4 1.7 copy-done.1
  214.1 17.8 %conv.1 = bf16[640,512]{1,0:T(8,128)(2,1)} custom-call(bf16[640,2048]{1,0:T(8,128)(2,1)S(1)} %copy-done.1, bf16[32,2048]{1,0:T(8,128)(2,1)} %collective-permute-done.carried_ref, f32[31,16,128]{2,1,0:T(8,128)S(1)} %slice.14.taps_ref, f32[1,2048]{1,0:T(1,128)S(1)} %bitcast.15, bf16[2048,512]{1,0:T(8,128)(2,1)S(1)} %copy-done.2), custom_call_target="tpu_custom_call" | custom-call | tf_op jit(solution)/shard_map/conv/pallas_call | solution.py:445
  231.9 3.5 %combine.1 = bf16[160,2048]{1,0:T(8,128)(2,1)} custom-call(bf16[32,160,128]{2,1,0:T(8,128)(2,1)S(1)} %all-to-all-done.1.refs_0_, s32[160,2]{1,0:T(8,128)S(1)} %bitcast.14, f32[160,2]{1,0:T(8,128)} %copy.16.refs_2_, f32[1,2048]{1,0:T(1,128)S(1)} %bitcast.16), custom_call_target="tpu_custom_call" | custom-call | tf_op jit(solution)/shard_map/combine/pallas_call | solution.py:380
  (62 shorter events, 12.8 us)
Async XLA Ops:
  5.4 125.7 %all-to-all-start = ((bf16[32,160,128]{2,1,0:T(8,128)(2,1)}), bf16[32,160,128]{2,1,0:T(8,128)(2,1)S(1)}, u32[]{:S(2)}, u32[]{:S(2)}) async-start(bf16[32,160,128]{2,1,0:T(8,128)(2,1)} %get-tuple-element.6), calls=%async_computation | async-start | bytes 2621440 | tf_op jit(solution)/shard_map/all_to_all | solution.py:512
  35.7 48.8 %collective-permute-start.5 = (bf16[256,2048]{1,0:T(8,128)(2,1)}, bf16[256,2048]{1,0:T(8,128)(2,1)S(1)}, u32[]{:S(2)}, u32[]{:S(2)}) collective-permute-start(bf16[256,2048]{1,0:T(8,128)(2,1)} %bitcast.7.refs_4_), channel_id=1, source_target_pairs={{0,1},{1,2},{2,3},{3,0},{4,5},{5,6},{6,7},{7,4},{8,9},{9,10},{10,1... | collective-permute-start | bytes 3145736 | tf_op jit(solution)/shard_map/ppermute | solution.py:502
  37.1 12.8 %collective-permute-start.6 = (bf16[1024,256]{1,0:T(8,128)(2,1)S(1)}, bf16[1024,256]{1,0:T(8,128)(2,1)S(1)}, u32[]{:S(2)}, u32[]{:S(2)}) collective-permute-start(bf16[1024,256]{1,0:T(8,128)(2,1)S(1)} %get-tuple-element.7), channel_id=1, source_target_pairs={{0,3},{1,0},{2,1},{3,2},{4,7},{5,4},{6,5},{7,6},{8,11},{9,8},{10,9... | collective-permute-start | bytes 1572872 | tf_op jit(solution)/shard_map/ppermute | solution.py:502
  38.8 22.3 %collective-permute-start.7 = (bf16[1024,256]{1,0:T(8,128)(2,1)S(1)}, bf16[1024,256]{1,0:T(8,128)(2,1)S(1)}, u32[]{:S(2)}, u32[]{:S(2)}) collective-permute-start(bf16[1024,256]{1,0:T(8,128)(2,1)S(1)} %get-tuple-element.8), channel_id=1, source_target_pairs={{0,3},{1,0},{2,1},{3,2},{4,7},{5,4},{6,5},{7,6},{8,11},{9,8},{10,9... | collective-permute-start | bytes 1572872 | tf_op jit(solution)/shard_map/ppermute | solution.py:502
  40.1 33.1 %collective-permute-start.2 = (bf16[1024,256]{1,0:T(8,128)(2,1)S(1)}, bf16[1024,256]{1,0:T(8,128)(2,1)S(1)}, u32[]{:S(2)}, u32[]{:S(2)}) collective-permute-start(bf16[1024,256]{1,0:T(8,128)(2,1)S(1)} %get-tuple-element.8), channel_id=1, source_target_pairs={{0,1},{1,2},{2,3},{3,0},{4,5},{5,6},{6,7},{7,4},{8,9},{9,10},{10,1... | collective-permute-start | bytes 1572872 | tf_op jit(solution)/shard_map/ppermute | solution.py:502
  40.3 44.2 %collective-permute-start.1 = (bf16[1024,256]{1,0:T(8,128)(2,1)S(1)}, bf16[1024,256]{1,0:T(8,128)(2,1)S(1)}, u32[]{:S(2)}, u32[]{:S(2)}) collective-permute-start(bf16[1024,256]{1,0:T(8,128)(2,1)S(1)} %get-tuple-element.7), channel_id=1, source_target_pairs={{0,1},{1,2},{2,3},{3,0},{4,5},{5,6},{6,7},{7,4},{8,9},{9,10},{10,1... | collective-permute-start | bytes 1572872 | tf_op jit(solution)/shard_map/ppermute | solution.py:502
  49.9 81.1 %copy-start.7 = (bf16[1024,256]{1,0:T(8,128)(2,1)}, bf16[1024,256]{1,0:T(8,128)(2,1)S(1)}, u32[]{:S(2)}) copy-start(bf16[1024,256]{1,0:T(8,128)(2,1)S(1)} %collective-permute-done.6.refs_10_) | copy-start | bytes 1572868
  49.9 50.2 %collective-permute-start.10 = (bf16[256,2048]{1,0:T(8,128)(2,1)}, bf16[256,2048]{1,0:T(8,128)(2,1)S(1)}, u32[]{:S(2)}, u32[]{:S(2)}) collective-permute-start(bf16[256,2048]{1,0:T(8,128)(2,1)} %bitcast.7.refs_4_), channel_id=1, source_target_pairs={{0,3},{1,0},{2,1},{3,2},{4,7},{5,4},{6,5},{7,6},{8,11},{9,8},{10,9... | collective-permute-start | bytes 3145736 | tf_op jit(solution)/shard_map/ppermute | solution.py:502
  61.1 69.8 %copy-start.8 = (bf16[1024,256]{1,0:T(8,128)(2,1)}, bf16[1024,256]{1,0:T(8,128)(2,1)S(1)}, u32[]{:S(2)}) copy-start(bf16[1024,256]{1,0:T(8,128)(2,1)S(1)} %collective-permute-done.7.refs_11_) | copy-start | bytes 1572868
  61.1 33.7 %collective-permute-start.11 = (bf16[1024,256]{1,0:T(8,128)(2,1)S(1)}, bf16[1024,256]{1,0:T(8,128)(2,1)S(1)}, u32[]{:S(2)}, u32[]{:S(2)}) collective-permute-start(bf16[1024,256]{1,0:T(8,128)(2,1)S(1)} %collective-permute-done.6.refs_10_), channel_id=1, source_target_pairs={{0,3},{1,0},{2,1},{3,2},{4,7},{5,4},{6,5},{7,6},{8,11},{9,8},{10,9... | collective-permute-start | bytes 1572872 | tf_op jit(solution)/shard_map/ppermute | solution.py:502
  73.2 57.8 %copy-start.9 = (bf16[1024,256]{1,0:T(8,128)(2,1)}, bf16[1024,256]{1,0:T(8,128)(2,1)S(1)}, u32[]{:S(2)}) copy-start(bf16[1024,256]{1,0:T(8,128)(2,1)S(1)} %collective-permute-done.2.refs_6_) | copy-start | bytes 1572868
  73.2 23.0 %collective-permute-start.9 = (bf16[1024,256]{1,0:T(8,128)(2,1)S(1)}, bf16[1024,256]{1,0:T(8,128)(2,1)S(1)}, u32[]{:S(2)}, u32[]{:S(2)}) collective-permute-start(bf16[1024,256]{1,0:T(8,128)(2,1)S(1)} %collective-permute-done.7.refs_11_), channel_id=1, source_target_pairs={{0,128},{128,0},{1,129},{129,1},{2,130},{130,2},{3,131},{131,3},{4... | collective-permute-start | bytes 1572872 | tf_op jit(solution)/shard_map/ppermute | solution.py:505
  84.4 13.7 %collective-permute-start.12 = (bf16[1024,256]{1,0:T(8,128)(2,1)S(1)}, bf16[1024,256]{1,0:T(8,128)(2,1)S(1)}, u32[]{:S(2)}, u32[]{:S(2)}) collective-permute-start(bf16[1024,256]{1,0:T(8,128)(2,1)S(1)} %collective-permute-done.2.refs_6_), channel_id=1, source_target_pairs={{0,1},{1,2},{2,3},{3,0},{4,5},{5,6},{6,7},{7,4},{8,9},{9,10},{10,1... | collective-permute-start | bytes 1572872 | tf_op jit(solution)/shard_map/ppermute | solution.py:502
  84.4 15.5 %collective-permute-start.3 = (bf16[1024,256]{1,0:T(8,128)(2,1)S(1)}, bf16[1024,256]{1,0:T(8,128)(2,1)S(1)}, u32[]{:S(2)}, u32[]{:S(2)}) collective-permute-start(bf16[1024,256]{1,0:T(8,128)(2,1)S(1)} %collective-permute-done.1.refs_5_), channel_id=1, source_target_pairs={{0,128},{128,0},{1,129},{129,1},{2,130},{130,2},{3,131},{131,3},{4... | collective-permute-start | bytes 1572872 | tf_op jit(solution)/shard_map/ppermute | solution.py:505
  94.8 36.2 %collective-permute-start.15 = (bf16[224,2048]{1,0:T(8,128)(2,1)S(1)}, bf16[224,2048]{1,0:T(8,128)(2,1)S(1)}, u32[]{:S(2)}, u32[]{:S(2)}) collective-permute-start(bf16[224,2048]{1,0:T(8,128)(2,1)S(1)} %slice.12), channel_id=1, source_target_pairs={{0,1},{1,2},{2,3},{3,0},{4,5},{5,6},{6,7},{7,4},{8,9},{9,10},{10,1... | collective-permute-start | bytes 2752520 | tf_op jit(solution)/shard_map/ppermute | solution.py:502
  96.2 12.3 %collective-permute-start.4 = (bf16[1024,256]{1,0:T(8,128)(2,1)S(1)}, bf16[1024,256]{1,0:T(8,128)(2,1)S(1)}, u32[]{:S(2)}, u32[]{:S(2)}) collective-permute-start(bf16[1024,256]{1,0:T(8,128)(2,1)S(1)} %collective-permute-done.2.refs_6_), channel_id=1, source_target_pairs={{0,128},{128,0},{1,129},{129,1},{2,130},{130,2},{3,131},{131,3},{4... | collective-permute-start | bytes 1572872 | tf_op jit(solution)/shard_map/ppermute | solution.py:505
  98.1 21.7 %collective-permute-start.8 = (bf16[1024,256]{1,0:T(8,128)(2,1)S(1)}, bf16[1024,256]{1,0:T(8,128)(2,1)S(1)}, u32[]{:S(2)}, u32[]{:S(2)}) collective-permute-start(bf16[1024,256]{1,0:T(8,128)(2,1)S(1)} %collective-permute-done.6.refs_10_), channel_id=1, source_target_pairs={{0,128},{128,0},{1,129},{129,1},{2,130},{130,2},{3,131},{131,3},{4... | collective-permute-start | bytes 1572872 | tf_op jit(solution)/shard_map/ppermute | solution.py:505
  99.9 31.0 %collective-permute-start.13 = (bf16[1024,256]{1,0:T(8,128)(2,1)S(1)}, bf16[1024,256]{1,0:T(8,128)(2,1)S(1)}, u32[]{:S(2)}, u32[]{:S(2)}) collective-permute-start(bf16[1024,256]{1,0:T(8,128)(2,1)S(1)} %collective-permute-done.11.refs_15_), channel_id=1, source_target_pairs={{0,128},{128,0},{1,129},{129,1},{2,130},{130,2},{3,131},{131,3},{4... | collective-permute-start | bytes 1572872 | tf_op jit(solution)/shard_map/ppermute | solution.py:505
  100.1 30.9 %collective-permute-start.14 = (bf16[1024,256]{1,0:T(8,128)(2,1)S(1)}, bf16[1024,256]{1,0:T(8,128)(2,1)S(1)}, u32[]{:S(2)}, u32[]{:S(2)}) collective-permute-start(bf16[1024,256]{1,0:T(8,128)(2,1)S(1)} %collective-permute-done.9.refs_13_), channel_id=1, source_target_pairs={{0,3},{1,0},{2,1},{3,2},{4,7},{5,4},{6,5},{7,6},{8,11},{9,8},{10,9... | collective-permute-start | bytes 1572872 | tf_op jit(solution)/shard_map/ppermute | solution.py:502
  108.5 11.2 %collective-permute-start.16 = (bf16[32,2048]{1,0:T(8,128)(2,1)S(1)}, bf16[32,2048]{1,0:T(8,128)(2,1)S(1)}, u32[]{:S(2)}, u32[]{:S(2)}) collective-permute-start(bf16[32,2048]{1,0:T(8,128)(2,1)S(1)} %slice.13), channel_id=1, source_target_pairs={{0,3},{1,0},{2,1},{3,2},{4,7},{5,4},{6,5},{7,6},{8,11},{9,8},{10,9... | collective-permute-start | bytes 393224 | tf_op jit(solution)/shard_map/ppermute | solution.py:502
  140.0 72.4 %copy-start.2 = (bf16[2048,512]{1,0:T(8,128)(2,1)S(1)}, bf16[2048,512]{1,0:T(8,128)(2,1)}, u32[]{:S(2)}) copy-start(bf16[2048,512]{1,0:T(8,128)(2,1)} %weight_ref.1) | copy-start | bytes 6291460
  140.0 91.9 %all-to-all-start.1 = ((bf16[32,160,128]{2,1,0:T(8,128)(2,1)}), bf16[32,160,128]{2,1,0:T(8,128)(2,1)S(1)}, u32[]{:S(2)}, u32[]{:S(2)}) async-start(bf16[32,160,128]{2,1,0:T(8,128)(2,1)} %experts.1), calls=%async_computation.1 | async-start | bytes 2621440 | tf_op jit(solution)/shard_map/all_to_all | solution.py:512
  154.3 58.1 %copy-start.3 = (f32[2048]{0:T(1024)S(1)}, f32[2048]{0:T(1024)}, u32[]{:S(2)}) copy-start(f32[2048]{0:T(1024)} %param.14) | copy-start | bytes 24580
  155.9 56.5 %collective-permute-start = (bf16[32,2048]{1,0:T(8,128)(2,1)}, bf16[32,2048]{1,0:T(8,128)(2,1)}, u32[]{:S(2)}, u32[]{:S(2)}) collective-permute-start(bf16[32,2048]{1,0:T(8,128)(2,1)} %slice.9), channel_id=1, source_target_pairs={{0,4},{4,8},{8,12},{12,16},{16,20},{20,24},{24,28},{28,32},{32,36}... | collective-permute-start | bytes 393224 | tf_op jit(solution)/shard_map/ppermute | solution.py:533
  (12 other events, 282.2 us)
